TPU v7x, 32 devices: a whole 2x2x4 slice. The times are simulated.
32 devices in a mesh: grp: 2 (over x), ep: 16 (over z, y, core).
Axes of the slice: x: 2, y: 2, z: 4, core: 2. Of those that a mesh axis runs over, the one named last changes fastest.
Arguments:
- hidden_in: bfloat16 [512, 2048], P(('grp', 'ep')), parts along dimension 0, may hold values from -6 to 6
- state_in: float32 [512, 64, 1024], P(('grp', 'ep')), parts along dimension 0, may hold values from -3 to 3
- norm_gain: float32 [2048], replicated, may hold values from 0.1 to 1.9
- w_recept: bfloat16 [2048, 1024], P(None, 'ep'), may hold values from -0.125 to 0.125
- w_key: bfloat16 [2048, 1024], P(None, 'ep'), may hold values from -0.125 to 0.125
- w_value: bfloat16 [2048, 1024], P(None, 'ep'), may hold values from -0.125 to 0.125
- decay_base: float32 [1024], replicated, may hold values from -4 to 2
- w_decay_down: bfloat16 [2048, 128], replicated, may hold values from -0.125 to 0.125
- w_decay_up: bfloat16 [128, 1024], replicated, may hold values from -0.5 to 0.5
- w_remove_down: bfloat16 [2048, 128], replicated, may hold values from -0.125 to 0.125
- w_remove_up: bfloat16 [128, 1024], replicated, may hold values from -1 to 1
- group_gain: float32 [1024], replicated, may hold values from 0.1 to 1.9
- w_out: bfloat16 [1024, 2048], replicated, may hold values from -0.1875 to 0.1875
- ffn_gain: float32 [2048], replicated, may hold values from 0.1 to 1.9
- routes: int32 [512, 2], P(('grp', 'ep')), parts along dimension 0, may hold values from 0 to 3, all different within a row; in each aligned block of 16 rows (0 to 15, 16 to 31, ...) at most 16 rows name the same one
- route_gate: float32 [512, 2], P(('grp', 'ep')), parts along dimension 0, may hold values from 0.1 to 1
- w_gate: bfloat16 [2048, 11264], P(None, 'ep'), may hold values from -0.125 to 0.125
- w_up: bfloat16 [2048, 11264], P(None, 'ep'), may hold values from -0.125 to 0.125
- w_down: bfloat16 [11264, 2048], P('ep'), may hold values from -0.109375 to 0.109375
Outputs:
- mixed_out: bfloat16 [512, 2048], P(('grp', 'ep')), parts along dimension 0
- state_out: float32 [512, 64, 1024], P(('grp', 'ep')), parts along dimension 0
There are 2 independent parts, one for each index of `grp`. A program takes and returns all parts, laid end to end along the dimension named above; an argument that names none is the same for every part. Nothing has to cross between parts.
Inputs may be any that keep to these rules, and one draw needn't show every extreme that they name: `routes`: each row names 2 different experts; in each aligned block of 16 rows (the rows of one device) no expert is named more than 16 times.
All inputs are finite; a program needn't handle non-finite values.
Results may differ from a plain program's by a relative error of at most 0.015.
Values may be sent and summed in bfloat16 or wider, within the bound.
No kernel may reach another device: no remote copies, remote signals or barrier semaphores. Data moves between devices by JAX's collectives and lax.ppermute only.
A program may use at most 128 MiB of HBM per device.

v0:
```python
import jax
import jax.numpy as jnp
from jax import lax
from jax.sharding import PartitionSpec as P

EXP_SPLIT = 4


norm_eps = 1e-06
group_eps = 0.00064


def scaled_rows(values, scale_gain):
    floats = values.astype(jnp.float32)
    return (
        floats
        * lax.rsqrt(jnp.mean(floats * floats, axis=-1, keepdims=True) + norm_eps)
        * scale_gain
    )


def update_state(state_in, receptance, new_keys, new_values, decay_rate, removal):
    seq_count = state_in.shape[0]
    head_size = state_in.shape[1]
    head_count = state_in.shape[2] // head_size
    shape_heads = (seq_count, head_count, head_size)
    recept_heads = receptance.astype(jnp.float32).reshape(shape_heads)
    key_heads = new_keys.astype(jnp.float32).reshape(shape_heads)
    value_heads = new_values.astype(jnp.float32).reshape(shape_heads)
    unit_keys = key_heads * lax.rsqrt(
        jnp.sum(key_heads * key_heads, axis=-1, keepdims=True) + norm_eps
    )
    blocks = state_in.reshape(seq_count, head_size, head_count, head_size)
    recalled = jnp.einsum("svhk,shk->svh", blocks, unit_keys, precision=lax.Precision.HIGHEST)
    removed = unit_keys * removal.reshape(shape_heads)
    updated = (
        blocks * decay_rate.reshape(seq_count, 1, head_count, head_size)
        - recalled[..., None] * removed[:, None]
        + jnp.swapaxes(value_heads, 1, 2)[..., None] * key_heads[:, None]
    )
    readout = jnp.einsum("svhk,shk->shv", updated, recept_heads, precision=lax.Precision.HIGHEST)
    return (updated.reshape(state_in.shape), readout)


def group_scale(readout, scale_gain):
    center = readout - jnp.mean(readout, axis=-1, keepdims=True)
    spread = jnp.mean(center * center, axis=-1, keepdims=True)
    normed = center * lax.rsqrt(spread + group_eps)
    return (normed.reshape(readout.shape[0], -1) * scale_gain).astype(jnp.bfloat16)


def decay_of(normed, w_decay_down, w_decay_up, decay_base):
    decay_low = jnp.dot(normed, w_decay_down, preferred_element_type=jnp.float32).astype(
        jnp.bfloat16
    )
    decay_act = jnp.tanh(decay_low.astype(jnp.float32)).astype(jnp.bfloat16)
    decay_pre = decay_base + jnp.dot(decay_act, w_decay_up, preferred_element_type=jnp.float32)
    return jnp.exp(-jnp.exp(-jax.nn.softplus(-decay_pre) - 0.5))


def removal_of(normed, w_remove_down, w_remove_up):
    remove_low = jnp.dot(normed, w_remove_down, preferred_element_type=jnp.float32).astype(
        jnp.bfloat16
    )
    return jax.nn.sigmoid(jnp.dot(remove_low, w_remove_up, preferred_element_type=jnp.float32))


def shards(
    hidden_in,
    state_in,
    norm_gain,
    w_recept,
    w_key,
    w_value,
    decay_base,
    w_decay_down,
    w_decay_up,
    w_remove_down,
    w_remove_up,
    group_gain,
    w_out,
    ffn_gain,
    routes,
    route_gate,
    w_gate,
    w_up,
    w_down,
):
    normed = scaled_rows(hidden_in, norm_gain).astype(jnp.bfloat16)
    shard_rows = lax.all_gather(normed, "ep", axis=0, tiled=True)
    spread = jnp.stack(
        [
            jnp.dot(shard_rows, matrix, preferred_element_type=jnp.float32).astype(jnp.bfloat16)
            for matrix in (w_recept, w_key, w_value)
        ]
    )
    joined = lax.all_to_all(spread, "ep", split_axis=1, concat_axis=2, tiled=True)
    receptance, new_keys, new_values = (joined[0], joined[1], joined[2])
    decay_rate = decay_of(normed, w_decay_down, w_decay_up, decay_base)
    removal = removal_of(normed, w_remove_down, w_remove_up)
    state_out, readout = update_state(
        state_in, receptance, new_keys, new_values, decay_rate, removal
    )
    grouped = group_scale(readout, group_gain)
    residual = hidden_in.astype(jnp.float32) + jnp.dot(
        grouped, w_out, preferred_element_type=jnp.float32
    )
    expert_in = scaled_rows(residual, ffn_gain).astype(jnp.bfloat16)
    ep_size = lax.axis_size("ep")
    experts = ep_size // EXP_SPLIT
    seq_count, model_width = expert_in.shape
    top_count = routes.shape[1]
    capacity = max(2, 2 * seq_count * top_count // experts)
    chosen = routes.reshape(-1)
    hit_table = (chosen[:, None] == jnp.arange(experts, dtype=jnp.int32)[None, :]).astype(jnp.int32)
    slot_index = jnp.sum((jnp.cumsum(hit_table, axis=0) - 1) * hit_table, axis=1)
    slot_table = (slot_index[:, None] == jnp.arange(capacity, dtype=jnp.int32)[None, :]).astype(
        jnp.float32
    )
    placed = hit_table.astype(jnp.float32)[:, :, None] * slot_table[:, None, :]
    placed = placed.reshape(seq_count, top_count, experts * capacity)
    dispatch = jnp.sum(placed, axis=1).astype(jnp.bfloat16)
    combine = jnp.sum(placed * route_gate[:, :, None], axis=1)
    outgoing = jnp.einsum(
        "sm,sd->md", dispatch, expert_in, preferred_element_type=jnp.float32
    ).astype(jnp.bfloat16)
    send_buffer = jnp.broadcast_to(
        outgoing.reshape(experts, 1, capacity, model_width),
        (experts, EXP_SPLIT, capacity, model_width),
    )
    send_buffer = send_buffer.reshape(ep_size, capacity, model_width)
    columns = lax.all_to_all(send_buffer, "ep", split_axis=0, concat_axis=0, tiled=True)
    flat_rows = columns.reshape(-1, model_width)
    gate_pre = jnp.dot(flat_rows, w_gate, preferred_element_type=jnp.float32)
    up_pre = jnp.dot(flat_rows, w_up, preferred_element_type=jnp.float32)
    hidden = (jax.nn.silu(gate_pre) * up_pre).astype(jnp.bfloat16)
    partial_out = jnp.dot(hidden, w_down, preferred_element_type=jnp.float32).astype(jnp.bfloat16)
    partial_out = partial_out.reshape(columns.shape[0], columns.shape[1], model_width)
    returned = lax.all_to_all(partial_out, "ep", split_axis=0, concat_axis=0, tiled=True)
    summed = jnp.sum(
        returned.reshape(experts, EXP_SPLIT, capacity, model_width).astype(jnp.float32), axis=1
    )
    routed = jnp.dot(
        combine, summed.reshape(experts * capacity, model_width), precision=lax.Precision.HIGHEST
    )
    mixed_out = (residual + routed).astype(jnp.bfloat16)
    return (mixed_out, state_out)


def solution(mesh):
    placed = (
        P(("grp", "ep"), None),
        P(("grp", "ep"), None, None),
        P(),
        P(None, "ep"),
        P(None, "ep"),
        P(None, "ep"),
        P(),
        P(),
        P(),
        P(),
        P(),
        P(),
        P(),
        P(),
        P(("grp", "ep"), None),
        P(("grp", "ep"), None),
        P(None, "ep"),
        P(None, "ep"),
        P("ep", None),
    )
    return jax.shard_map(
        shards,
        mesh=mesh,
        in_specs=placed,
        out_specs=(P(("grp", "ep"), None), P(("grp", "ep"), None, None)),
        check_vma=False,
    )
```

profile of v0, /device:TPU:0, one launch (start us, length us, event | category | flops | bytes accessed | tf_op | source)
XLA Modules:
  0.0 197.7 jit_solution(5547005113535397011)
XLA Ops:
  7.2 0.0 copy-start
  7.2 0.0 all-gather.2.cloned.1.call-start
  7.2 1.1 fusion.15
  8.4 1.6 fusion.17
  9.9 0.0 all-gather.2.cloned.1.call-update
  9.9 0.8 copy.54
  10.7 0.1 eq.36
  10.8 0.1 fusion.30
  10.9 0.1 reduce_window_sum.11
  10.9 0.2 select_reduce_fusion
  11.1 0.1 fusion.29
  11.2 1.5 fusion.23
  12.7 38.6 %all-gather.2.cloned.1.call-done = bf16[256,2048]{1,0:T(8,128)(2,1)} async-done(((bf16[16,2048]{1,0:T(8,128)(2,1)}), bf16[256,2048]{1,0:T(8,128)(2,1)}) %all-gather.2.cloned.1.call-update) | async-done | bytes 1048592 | tf_op jit(solution)/shard_map/all_gather | solution.py:90
  51.4 1.7 fusion.10
  53.1 1.7 fusion.9
  54.8 1.7 fusion.8
  56.5 0.2 copy.48
  56.7 0.8 reshape.183
  57.5 3.7 %all-to-all-start = ((bf16[16,2,1536]{2,1,0:T(2,128)(2,1)}), bf16[16,2,1536]{2,1,0:T(2,128)(2,1)S(1)}, u32[]{:S(2)}, u32[]{:S(2)}) async-start(bf16[16,2,1536]{2,1,0:T(2,128)(2,1)} %reshape.183), calls=%async_computation | async-start | bytes 196608 | tf_op jit(solution)/shard_map/all_to_all | solution.py:97
  61.2 0.1 broadcast_multiply_fusion.1
  61.3 0.1 copy.55
  61.4 0.1 mul.204
  61.5 0.1 mul.182
  61.6 7.3 %reshape.167 = f32[16,64,16,64]{3,2,1,0:T(8,128)} reshape(f32[16,64,1024]{2,1,0:T(8,128)} %param.20) | data formatting | bytes 8388608 | tf_op jit(solution)/shard_map/reshape | solution.py:33
  68.9 0.6 fusion.33
  69.5 0.2 reshape.184
  69.8 0.1 multiply_reduce_fusion.3
  69.9 0.7 slice_convert_fusion
  70.6 0.1 copy.68
  70.7 0.7 mul.186.clone
  71.4 1.0 mul.217
  72.4 1.6 copy.56
  74.0 1.0 reshape.177
  75.0 2.1 %multiply_multiply_fusion = (f32[16,1024]{1,0:T(8,128)}, f32[16,1024]{1,0:T(8,128)}) fusion(f32[16,1024]{1,0:T(8,128)S(1)} %reshape.177, f32[16,1024]{1,0:T(8,128)S(1)} %mul.217, bf16[128,1024]{1,0:T(8,128)(2,1)} %param.29, bf16[16,2048]{1,0:T(8,128)(2,1)S(1)} %copy-done.4, bf16[2048,128]{1,0:T(8,128)(2,1)} %param.28), kind=kOutput, calls=%fused_computation.54 | convolution fusion | flops 12666880 | bytes 1114112 | tf_op jit(solution)/shard_map/dot_general | solution.py:65
  77.1 1.6 reshape.168
  78.7 1.0 broadcast_multiply_fusion
  79.7 0.7 copy.67
  80.4 0.7 copy.51
  81.1 0.7 copy.53
  81.8 1.1 copy.52
  83.0 0.0 copy-start.12
  83.0 5.8 %multiply_reduce_fusion = f32[16,16,64]{1,2,0:T(8,128)S(1)} fusion(f32[16,64,16,64]{3,2,1,0:T(8,128)} %reshape.167, f32[16,16,64]{2,1,0:T(8,128)} %copy.67), kind=kLoop, calls=%fused_computation.2 | loop fusion | flops 2080768 | bytes 4325376 | tf_op jit(solution)/shard_map/svhk,shk->svh/dot_general | solution.py:34
  88.8 5.1 %multiply_add_fusion = f32[16,64,16,64]{3,2,1,0:T(8,128)S(1)} fusion(f32[16,64,16,64]{3,2,1,0:T(8,128)S(1)} %copy-done.2, f32[16,16,64]{2,1,0:T(8,128)S(1)} %copy-done.12, f32[16,64,16]{2,1,0:T(8,128)S(1)} %copy.52, f32[16,16,64]{2,1,0:T(8,128)S(1)} %copy-done.11, f32[16,64,16]{2,1,0:T(8,128)S(1)} %bitcast.69, f32[16,16,64]{2,1,0:T(8,128)S(1)} %mul.182), kind=kLoop, calls=%fused_computation.3 | loop fusion | flops 5242880 | bytes 8716288 | tf_op jit(solution)/shard_map/add | solution.py:37
  94.0 8.5 %fusion = f32[16,16,1,64]{3,2,1,0:T(1,128)S(1)} fusion(f32[16,64,16,64]{3,2,1,0:T(8,128)S(1)} %multiply_add_fusion, bf16[16,16,64,1]{2,0,1,3:T(8,128)(2,1)S(1)} %copy-done.6), kind=kOutput, calls=%fused_computation | convolution fusion | flops 12582912 | bytes 4292608 | tf_op jit(solution)/shard_map/svhk,shk->shv/dot_general | solution.py:41
  102.5 0.1 reduce_sum.83
  102.6 0.2 multiply_reduce_fusion.2
  102.8 0.8 subtract_multiply_fusion
  103.6 1.6 reshape.170
  105.2 3.2 %multiply_reduce_fusion.1 = (f32[16]{0:T(128)S(1)}, f32[16,2048]{1,0:T(8,128)S(1)}) fusion(bf16[1024,2048]{1,0:T(8,128)(2,1)} %param.31, f32[16,1024]{1,0:T(8,128)} %reshape.170, f32[1024]{0:T(1024)} %param.30, bf16[16,2048]{1,0:T(8,128)(2,1)} %param.19), kind=kOutput, calls=%fused_computation.41 | convolution fusion | flops 67272688 | bytes 4460608 | tf_op jit(solution)/shard_map/dot_general | solution.py:105
  108.4 0.3 convolution_convert_fusion.1
  108.7 0.1 broadcast_in_dim.5
  108.8 30.5 %all_to_all.25 = bf16[16,16,2048]{2,1,0:T(8,128)(2,1)S(1)} all-to-all(bf16[16,16,2048]{2,1,0:T(8,128)(2,1)S(1)} %bitcast.71), channel_id=1, replica_groups=mesh['grp'=2,'ep'=16] {'ep'}, dimensions={0} | all-to-all | bytes 2097152 | tf_op jit(solution)/shard_map/all_to_all | solution.py:132
  139.3 1.0 copy-done.5
  140.3 1.8 fusion.34
  142.1 6.6 %convolution_convert_fusion = bf16[256,2048]{1,0:T(8,128)(2,1)} fusion(bf16[704,2048]{1,0:T(8,128)(2,1)S(1)} %copy-done, bf16[256,2048]{1,0:T(8,128)(2,1)} %bitcast.83, bf16[2048,704]{0,1:T(8,128)(2,1)} %param.36, f32[256,704]{0,1:T(8,128)} %fusion.34), kind=kOutput, calls=%fused_computation.5 | convolution fusion | flops 1478000640 | bytes 8585216 | tf_op jit(solution)/shard_map/dot_general | solution.py:137
  148.7 5.1 %all-to-all-start.2 = ((bf16[16,16,2048]{2,1,0:T(8,128)(2,1)}), bf16[16,16,2048]{2,1,0:T(8,128)(2,1)}, u32[]{:S(2)}, u32[]{:S(2)}) async-start(bf16[16,16,2048]{2,1,0:T(8,128)(2,1)} %bitcast.81), calls=%async_computation.2 | async-start | bytes 2097152 | tf_op jit(solution)/shard_map/all_to_all | solution.py:139
  153.8 5.8 %mul.188 = f32[16,64,16,64]{3,2,1,0:T(8,128)} broadcast(f32[16,64,16]{2,1,0:T(8,128)} %bitcast.70), dimensions={0,1,2} | broadcast | bytes 4259840 | tf_op jit(solution)/shard_map/mul | solution.py:38
  159.7 7.6 %mul.216 = f32[16,64,1024]{2,1,0:T(8,128)} reshape(f32[16,64,16,64]{3,2,1,0:T(8,128)} %mul.188) | data formatting | bytes 8388608 | tf_op jit(solution)/shard_map/mul | solution.py:38
  167.3 4.5 %mul.192 = f32[16,64,16,64]{3,2,1,0:T(8,128)} broadcast(f32[16,64,16]{2,1,0:T(8,128)S(1)} %copy.52), dimensions={0,1,2} | broadcast | bytes 4259840 | tf_op jit(solution)/shard_map/mul | solution.py:39
  171.8 7.6 %mul.222 = f32[16,64,1024]{2,1,0:T(8,128)} reshape(f32[16,64,16,64]{3,2,1,0:T(8,128)} %mul.192) | data formatting | bytes 8388608 | tf_op jit(solution)/shard_map/mul | solution.py:39
  179.5 0.0 copy-start.1
  179.5 8.9 %multiply_add_fusion.1 = f32[16,64,1024]{2,1,0:T(8,128)} fusion(f32[16,64,1024]{2,1,0:T(8,128)} %mul.222, f32[16,64,1024]{2,1,0:T(8,128)} %mul.216, f32[16,64,1024]{2,1,0:T(8,128)} %param.20, f32[16,1024]{1,0:T(8,128)S(1)} %copy-done.10, f32[16,1024]{1,0:T(8,128)S(1)} %copy-done.13, f32[16,1024]{1,0:T(8,128)S(1)} %copy-done.8), kind=kLoop, calls=%fused_computation.4 | loop fusion | flops 5242880 | bytes 16973824 | tf_op jit(solution)/shard_map/add | solution.py:37
  188.4 1.4 convert_reduce_fusion
  189.8 1.0 fusion.2
  (41 shorter events, 0.1 us)
Async XLA Ops:
  7.2 134.9 %copy-start = (bf16[704,2048]{1,0:T(8,128)(2,1)S(1)}, bf16[704,2048]{1,0:T(8,128)(2,1)}, u32[]{:S(2)}) copy-start(bf16[704,2048]{1,0:T(8,128)(2,1)} %param.37) | copy-start | bytes 8650756
  7.2 54.2 %copy-start.16 = (f32[16,2]{0,1:T(2,128)S(1)}, f32[16,2]{0,1:T(2,128)}, u32[]{:S(2)}) copy-start(f32[16,2]{0,1:T(2,128)} %param.34) | copy-start | bytes 388
  7.2 44.2 %all-gather.2.cloned.1.call-start = ((), (), s32[]{:S(2)}) async-start(), calls=%async_computation.3 | async-start | bytes 1114112 | tf_op jit(solution)/shard_map/all_gather | solution.py:90
  12.7 56.2 %copy-start.7 = (f32[16,1024]{1,0:T(8,128)}, f32[16,1024]{1,0:T(8,128)S(1)}, u32[]{:S(2)}) copy-start(f32[16,1024]{1,0:T(8,128)S(1)} %fusion.23) | copy-start | bytes 196612
  57.5 12.0 %all-to-all-start = ((bf16[16,2,1536]{2,1,0:T(2,128)(2,1)}), bf16[16,2,1536]{2,1,0:T(2,128)(2,1)S(1)}, u32[]{:S(2)}, u32[]{:S(2)}) async-start(bf16[16,2,1536]{2,1,0:T(2,128)(2,1)} %reshape.183), calls=%async_computation | async-start | bytes 196608 | tf_op jit(solution)/shard_map/all_to_all | solution.py:97
  61.6 13.4 %copy-start.4 = (bf16[16,2048]{1,0:T(8,128)(2,1)S(1)}, bf16[16,2048]{1,0:T(8,128)(2,1)}, u32[]{:S(2)}) copy-start(bf16[16,2048]{1,0:T(8,128)(2,1)} %fusion.17) | copy-start | bytes 196612
  75.0 6.8 %copy-start.9 = (f32[16,1024]{1,0:T(8,128)}, f32[16,1024]{1,0:T(8,128)S(1)}, u32[]{:S(2)}) copy-start(f32[16,1024]{1,0:T(8,128)S(1)} %reshape.177) | copy-start | bytes 196612
  82.9 5.8 %copy-start.2 = (f32[16,64,16,64]{3,2,1,0:T(8,128)S(1)}, f32[16,64,16,64]{3,2,1,0:T(8,128)}, u32[]{:S(2)}) copy-start(f32[16,64,16,64]{3,2,1,0:T(8,128)} %reshape.167) | copy-start | bytes 12582916
  82.9 5.8 %copy-start.11 = (f32[16,16,64]{2,1,0:T(8,128)S(1)}, f32[16,16,64]{2,1,0:T(8,128)}, u32[]{:S(2)}) copy-start(f32[16,16,64]{2,1,0:T(8,128)} %copy.51) | copy-start | bytes 196612
  83.0 5.8 %copy-start.12 = (f32[16,16,64]{2,1,0:T(8,128)S(1)}, f32[16,16,64]{2,1,0:T(8,128)}, u32[]{:S(2)}) copy-start(f32[16,16,64]{2,1,0:T(8,128)} %copy.53) | copy-start | bytes 196612
  88.8 5.2 %copy-start.3 = (f32[16,16,64]{1,2,0:T(8,128)}, f32[16,16,64]{1,2,0:T(8,128)S(1)}, u32[]{:S(2)}) copy-start(f32[16,16,64]{1,2,0:T(8,128)S(1)} %multiply_reduce_fusion) | copy-start | bytes 196612
  88.8 5.2 %copy-start.6 = (bf16[16,16,64,1]{2,0,1,3:T(8,128)(2,1)S(1)}, bf16[16,16,64,1]{2,0,1,3:T(8,128)(2,1)}, u32[]{:S(2)}) copy-start(bf16[16,16,64,1]{2,0,1,3:T(8,128)(2,1)} %get-tuple-element.8) | copy-start | bytes 98308
  103.6 4.8 %copy-start.14 = (bf16[16,64]{1,0:T(8,128)(2,1)S(1)}, bf16[16,64]{1,0:T(8,128)(2,1)}, u32[]{:S(2)}) copy-start(bf16[16,64]{1,0:T(8,128)(2,1)} %get-tuple-element.2) | copy-start | bytes 6148
  105.2 3.2 %copy-start.15 = (f32[2048]{0:T(1024)S(1)}, f32[2048]{0:T(1024)}, u32[]{:S(2)}) copy-start(f32[2048]{0:T(1024)} %param.32) | copy-start | bytes 24580
  105.2 35.0 %copy-start.17 = (bf16[2048,704]{0,1:T(8,128)(2,1)S(1)}, bf16[2048,704]{0,1:T(8,128)(2,1)}, u32[]{:S(2)}) copy-start(bf16[2048,704]{0,1:T(8,128)(2,1)} %param.35) | copy-start | bytes 8650756
  139.3 1.0 copy-start.5
  148.7 39.6 %all-to-all-start.2 = ((bf16[16,16,2048]{2,1,0:T(8,128)(2,1)}), bf16[16,16,2048]{2,1,0:T(8,128)(2,1)}, u32[]{:S(2)}, u32[]{:S(2)}) async-start(bf16[16,16,2048]{2,1,0:T(8,128)(2,1)} %bitcast.81), calls=%async_computation.2 | async-start | bytes 2097152 | tf_op jit(solution)/shard_map/all_to_all | solution.py:139
  171.8 7.7 %copy-start.8 = (f32[16,1024]{1,0:T(8,128)S(1)}, f32[16,1024]{1,0:T(8,128)}, u32[]{:S(2)}) copy-start(f32[16,1024]{1,0:T(8,128)} %copy-done.7) | copy-start | bytes 196612
  171.8 7.7 %copy-start.10 = (f32[16,1024]{1,0:T(8,128)S(1)}, f32[16,1024]{1,0:T(8,128)}, u32[]{:S(2)}) copy-start(f32[16,1024]{1,0:T(8,128)} %copy-done.9) | copy-start | bytes 196612
  171.8 7.7 %copy-start.13 = (f32[16,1024]{1,0:T(8,128)S(1)}, f32[16,1024]{1,0:T(8,128)}, u32[]{:S(2)}) copy-start(f32[16,1024]{1,0:T(8,128)} %get-tuple-element.14) | copy-start | bytes 196612
  179.5 11.3 %copy-start.1 = (bf16[704,2048]{1,0:T(8,128)(2,1)S(1)}, bf16[704,2048]{1,0:T(8,128)(2,1)}, u32[]{:S(2)}) copy-start(bf16[704,2048]{1,0:T(8,128)(2,1)} %param.37) | copy-start | bytes 8650756
Sparse Core Ops, SparseCore 0:
  10.7 40.5 all-gather.1
where the time goes:
time: 199 us; the launch traced here: 198 us
  local copies, waits for them, and re-layouts  47.2 us (24%)
  waiting for transfers between devices  38.7 us (19%)
  blocking collectives  30.5 us (15%)
  matrix products  30.2 us (15%)
  other arithmetic  28 us (14%)
  between operations  14.4 us (7%)
  starting transfers between devices  8.8 us (4%)
    all_gather x1, waiting for transfers between devices, shards(): shard_rows = lax.all_gather(normed, 'ep', axis=0, tiled=True)  38.6 us
    all_to_all x1, blocking collectives, shards(): lax.all_to_all(send_buffer, 'ep', split_axis=0, concat_axis=0, tiled=True)  30.5 us
    add x2, other arithmetic, update_state(): blocks * decay_rate.reshape(seq_count, 1, head_count, head_size)  14 us
    mul x2, local copies, waits for them, and re-layouts, update_state(): recalled[..., None] * removed[:, None]  13.5 us
    mul x2, local copies, waits for them, and re-layouts, update_state(): jnp.swapaxes(value_heads, 1, 2)[..., None] * key_heads[:, None]  12.2 us
    dot_general x1, matrix products, update_state(): jnp.einsum('svhk,shk->shv', updated, recept_heads, precision=lax.Precisio...  8.51 us
    reshape x1, local copies, waits for them, and re-layouts, update_state(): blocks = state_in.reshape(seq_count, head_size, head_count, head_size)  7.28 us
    dot_general x1, matrix products, shards(): jnp.dot(hidden, w_down, preferred_element_type=jnp.float32)  6.64 us
  transfers between devices with their start and end apart: 3, of which 1 were waited for; matrix products, arithmetic and copies ran while one was open for 23% of the time, Pallas kernels for 0%

commit v1 on v0

v1 whole, which is shorter than its diff:
```python
import functools

import jax
import jax.numpy as jnp
from jax import lax
from jax.experimental import pallas as pl
from jax.experimental.pallas import tpu as pltpu
from jax.sharding import PartitionSpec as P

EXP_SPLIT = 4

norm_eps = 1e-06
group_eps = 0.00064
f32 = jnp.float32
bf16 = jnp.bfloat16
NT = (((1,), (1,)), ((), ()))
VM = pl.BlockSpec(memory_space=pltpu.VMEM)
ANY = pl.BlockSpec(memory_space=pl.ANY)


def scaled_rows(values, scale_gain):
    floats = values.astype(f32)
    return (
        floats
        * lax.rsqrt(jnp.mean(floats * floats, axis=-1, keepdims=True) + norm_eps)
        * scale_gain
    )


def decay_of(normed, w_decay_down, w_decay_up, decay_base):
    decay_low = jnp.dot(normed, w_decay_down, preferred_element_type=f32).astype(bf16)
    decay_act = jnp.tanh(decay_low.astype(f32)).astype(bf16)
    decay_pre = decay_base + jnp.dot(decay_act, w_decay_up, preferred_element_type=f32)
    return jnp.exp(-jnp.exp(-jax.nn.softplus(-decay_pre) - 0.5))


def removal_of(normed, w_remove_down, w_remove_up):
    remove_low = jnp.dot(normed, w_remove_down, preferred_element_type=f32).astype(bf16)
    return jax.nn.sigmoid(jnp.dot(remove_low, w_remove_up, preferred_element_type=f32))


def swap(piece, bits):
    size = lax.axis_size("ep")
    return lax.ppermute(piece, "ep", [(i, i ^ bits) for i in range(size)])


def gather_pieces(own):
    size = lax.axis_size("ep")
    pieces = {0: own}
    for d in range(size // 4 - 1, 0, -1):
        pieces[4 * d] = swap(own, 4 * d)
    for d in list(pieces):
        pieces[d + 2] = swap(pieces[d], 2)
    for d in list(pieces):
        pieces[d + 1] = swap(pieces[d], 1)
    return [pieces[d] for d in range(size)]


def norm_kernel(x_ref, gain_ref, out_ref):
    out_ref[...] = scaled_rows(x_ref[...], gain_ref[...]).astype(bf16)


def norm_rows(values, gain):
    return pl.pallas_call(
        norm_kernel,
        out_shape=jax.ShapeDtypeStruct(values.shape, bf16),
        in_specs=[VM, VM],
        out_specs=VM,
        name="norm_rows",
    )(values, gain.reshape(1, -1))


def project_kernel(place_ref, *refs):
    out_ref = refs[-1]
    count = out_ref.shape[0]
    pieces, weights = refs[:count], refs[count : count + 3]
    rows = pieces[0].shape[0]
    width = weights[0].shape[0]
    tokens = jnp.concatenate([piece[...] for piece in pieces], axis=0)
    parts = [
        lax.dot_general(tokens, w[...], NT, preferred_element_type=f32).astype(bf16)
        for w in weights
    ]
    place = place_ref[0]
    for d in range(count):
        target = place ^ d
        for m in range(3):
            out_ref[target, :, m * width : (m + 1) * width] = parts[m][d * rows : (d + 1) * rows]


def project(pieces, weights):
    count = len(pieces)
    rows = pieces[0].shape[0]
    width = weights[0].shape[1]
    return pl.pallas_call(
        project_kernel,
        out_shape=jax.ShapeDtypeStruct((count, rows, 3 * width), bf16),
        in_specs=[pl.BlockSpec(memory_space=pltpu.SMEM)] + [VM] * (count + 3),
        out_specs=VM,
        name="project",
    )(lax.axis_index("ep").astype(jnp.int32).reshape(1), *pieces, *[w.T for w in weights])


def mixer_kernel(
    state_ref, joined_ref, decay_ref, removal_ref, gain_ref, hidden_ref, ffn_gain_ref, w_out_ref,
    state_out_ref, residual_ref, expert_ref,
    vec_ref, readout_ref, w_out_buf, sem, *, head,
):
    step = pl.program_id(0)
    steps = pl.num_programs(0)
    batch, values, inner = state_ref.shape
    chunk = min(256, inner)
    count = joined_ref.shape[0]
    width = inner // count
    copy = pltpu.make_async_copy(w_out_ref, w_out_buf, sem)

    def ones(dtype, scale=1.0):
        a = lax.broadcasted_iota(jnp.int32, (chunk, chunk), 0) // head
        b = lax.broadcasted_iota(jnp.int32, (chunk, chunk), 1) // head
        return jnp.where(a == b, scale, 0.0).astype(dtype)

    def head_sums(x, block, precision=None):
        return jnp.concatenate(
            [
                jnp.dot(
                    x[:, c : c + chunk], block, preferred_element_type=f32, precision=precision
                )
                for c in range(0, inner, chunk)
            ],
            axis=1,
        )

    @pl.when(step == 0)
    def _():
        copy.start()
        for m in range(3):
            for j in range(count):
                vec_ref[m, :, j * width : (j + 1) * width] = joined_ref[
                    j, :, m * width : (m + 1) * width
                ].astype(f32)
        keys = vec_ref[1]
        unit = keys * lax.rsqrt(
            head_sums(keys * keys, ones(f32), lax.Precision.HIGHEST) + norm_eps
        )
        vec_ref[3] = unit
        vec_ref[4] = unit * removal_ref[...]

    block = ones(bf16)
    lane = lax.broadcasted_iota(jnp.int32, (values, inner), 1) % head
    row = lax.broadcasted_iota(jnp.int32, (values, inner), 0)
    diagonal = lane == row
    for b in range(batch):
        s = step * batch + b
        receptance = vec_ref[0, pl.ds(s, 1), :]
        keys = vec_ref[1, pl.ds(s, 1), :]
        new_values = vec_ref[2, pl.ds(s, 1), :]
        unit = vec_ref[3, pl.ds(s, 1), :]
        removed = vec_ref[4, pl.ds(s, 1), :]
        decay = decay_ref[pl.ds(s, 1), :]
        state = state_ref[b]
        recalled = head_sums((state * unit).astype(bf16), block)
        spread = head_sums(jnp.where(diagonal, new_values, 0.0).astype(bf16), block)
        updated = state * decay - recalled * removed + spread * keys
        state_out_ref[b] = updated
        read = head_sums((updated * receptance).astype(bf16), block)
        readout_ref[pl.ds(s, 1), :] = jnp.sum(
            jnp.where(diagonal, read, 0.0), axis=0, keepdims=True
        )

    @pl.when(step == steps - 1)
    def _():
        readout = readout_ref[...]
        mean_block = ones(f32, 1.0 / head)
        center = readout - head_sums(readout, mean_block, lax.Precision.HIGHEST)
        variance = head_sums(center * center, mean_block, lax.Precision.HIGHEST)
        grouped = (center * lax.rsqrt(variance + group_eps) * gain_ref[...]).astype(bf16)
        copy.wait()
        residual = hidden_ref[...].astype(f32) + jnp.dot(
            grouped, w_out_buf[...], preferred_element_type=f32
        )
        residual_ref[...] = residual
        expert_ref[...] = scaled_rows(residual, ffn_gain_ref[...]).astype(bf16)


def mixer(state_in, joined, decay, removal, group_gain, hidden_in, ffn_gain, w_out):
    seqs, head, inner = state_in.shape
    width = hidden_in.shape[1]
    batch = 4 if seqs % 4 == 0 else 1

    def whole(shape):
        return pl.BlockSpec(shape, lambda i: (0,) * len(shape))

    by_seq = pl.BlockSpec((batch, head, inner), lambda i: (i, 0, 0))
    return pl.pallas_call(
        functools.partial(mixer_kernel, head=head),
        grid=(seqs // batch,),
        out_shape=(
            jax.ShapeDtypeStruct(state_in.shape, f32),
            jax.ShapeDtypeStruct((seqs, width), f32),
            jax.ShapeDtypeStruct((seqs, width), bf16),
        ),
        in_specs=[
            by_seq,
            whole(joined.shape),
            whole((seqs, inner)),
            whole((seqs, inner)),
            whole((1, inner)),
            whole((seqs, width)),
            whole((1, width)),
            ANY,
        ],
        out_specs=(by_seq, whole((seqs, width)), whole((seqs, width))),
        scratch_shapes=[
            pltpu.VMEM((5, seqs, inner), f32),
            pltpu.VMEM((seqs, inner), f32),
            pltpu.VMEM(w_out.shape, bf16),
            pltpu.SemaphoreType.DMA(()),
        ],
        name="mixer",
    )(
        state_in, joined, decay, removal, group_gain.reshape(1, -1), hidden_in,
        ffn_gain.reshape(1, -1), w_out,
    )


def expert_kernel(*refs, count):
    pieces = refs[:count]
    gate_ref, up_ref, down_ref = refs[count : count + 3]
    outs = refs[count + 3 : -5]
    gate_buf, up_buf, down_buf, hidden_ref, sems = refs[-5:]
    rows = pieces[0].shape[0]
    units = gate_buf.shape[0]
    cuts = 2
    part = units // cuts
    copies = []
    for c in range(cuts):
        span = pl.ds(c * part, part)
        for m, (source, target) in enumerate(((gate_ref, gate_buf), (up_ref, up_buf))):
            copies.append(
                pltpu.make_async_copy(source.at[span], target.at[span], sems.at[2 * c + m])
            )
    last = pltpu.make_async_copy(down_ref, down_buf, sems.at[2 * cuts])
    for copy in copies:
        copy.start()
    last.start()
    tokens = jnp.concatenate([piece[...] for piece in pieces], axis=0)
    for c in range(cuts):
        span = pl.ds(c * part, part)
        copies[2 * c].wait()
        gate = lax.dot_general(tokens, gate_buf[span], NT, preferred_element_type=f32)
        copies[2 * c + 1].wait()
        up = lax.dot_general(tokens, up_buf[span], NT, preferred_element_type=f32)
        hidden_ref[:, c * part : (c + 1) * part] = (jax.nn.silu(gate) * up).astype(bf16)
    last.wait()
    result = jnp.dot(hidden_ref[...], down_buf[...], preferred_element_type=f32).astype(bf16)
    for d in range(count):
        outs[2 * (d // 4) + d % 2][d % 4 // 2] = result[d * rows : (d + 1) * rows]


def run_experts(pieces, w_gate, w_up, w_down):
    count = len(pieces)
    rows, width = pieces[0].shape
    units = w_down.shape[0]
    return pl.pallas_call(
        functools.partial(expert_kernel, count=count),
        out_shape=[jax.ShapeDtypeStruct((2, rows, width), bf16)] * (count // 2),
        in_specs=[VM] * count + [ANY] * 3,
        out_specs=[VM] * (count // 2),
        scratch_shapes=[pltpu.VMEM((units, width), bf16)] * 3
        + [pltpu.VMEM((count * rows, units), bf16), pltpu.SemaphoreType.DMA((5,))],
        name="experts",
    )(*pieces, w_gate.T, w_up.T, w_down)


def add(a, b):
    return (a.astype(f32) + b.astype(f32)).astype(bf16)


def shards(
    hidden_in,
    state_in,
    norm_gain,
    w_recept,
    w_key,
    w_value,
    decay_base,
    w_decay_down,
    w_decay_up,
    w_remove_down,
    w_remove_up,
    group_gain,
    w_out,
    ffn_gain,
    routes,
    route_gate,
    w_gate,
    w_up,
    w_down,
):
    place = lax.axis_index("ep")
    groups = lax.axis_size("ep") // EXP_SPLIT
    normed = norm_rows(hidden_in, norm_gain)
    pieces = gather_pieces(normed)
    spread = project(pieces, (w_recept, w_key, w_value))
    joined = lax.all_to_all(spread, "ep", split_axis=0, concat_axis=0, tiled=True)
    decay_rate = decay_of(normed, w_decay_down, w_decay_up, decay_base)
    removal = removal_of(normed, w_remove_down, w_remove_up)
    state_out, residual, expert_in = mixer(
        state_in, joined, decay_rate, removal, group_gain, hidden_in, ffn_gain, w_out
    )
    outs = run_experts(gather_pieces(expert_in), w_gate, w_up, w_down)
    mixed = residual
    for d in range(groups - 1, -1, -1):
        by_side = add(outs[2 * d], swap(outs[2 * d + 1], 1))
        part = add(by_side[0], swap(by_side[1], 2))
        if d:
            part = swap(part, EXP_SPLIT * d)
        weight = jnp.sum(
            jnp.where(routes == (place // EXP_SPLIT) ^ d, route_gate, 0.0), axis=1, keepdims=True
        )
        mixed = mixed + weight * part.astype(f32)
    return (mixed.astype(bf16), state_out)


def solution(mesh):
    placed = (
        P(("grp", "ep"), None),
        P(("grp", "ep"), None, None),
        P(),
        P(None, "ep"),
        P(None, "ep"),
        P(None, "ep"),
        P(),
        P(),
        P(),
        P(),
        P(),
        P(),
        P(),
        P(),
        P(("grp", "ep"), None),
        P(("grp", "ep"), None),
        P(None, "ep"),
        P(None, "ep"),
        P("ep", None),
    )
    return jax.shard_map(
        shards,
        mesh=mesh,
        in_specs=placed,
        out_specs=(P(("grp", "ep"), None), P(("grp", "ep"), None, None)),
        check_vma=False,
    )
```

time: 199 us -> 92.8 us (0.47)
  local copies, waits for them, and re-layouts: 47.2 us -> 1.83 us
  blocking collectives: 30.5 us -> 0 us
  starting transfers between devices: 8.8 us -> 37.2 us
  matrix products: 30.2 us -> 4.05 us
  other arithmetic: 28 us -> 4.58 us
  Pallas kernels: 0 us -> 23 us
  waiting for transfers between devices: 38.7 us -> 20.6 us
  between operations: 14.4 us -> 1.08 us
    all_gather x1 -> x0, waiting for transfers between devices: 38.6 us -> none  [shards(): shard_rows = lax.all_gather(normed, 'ep', axis=0, tiled=True)]
    ppermute x0 -> x41, starting transfers between devices: none -> 31.7 us  [swap(): return lax.ppermute(piece, 'ep', [(i, i ^ bits) for i in range(size)])]
    all_to_all x1 -> x0, blocking collectives: 30.5 us -> none  [shards(): lax.all_to_all(send_buffer, 'ep', split_axis=0, concat_axis=0, tiled=True)]
    mul x9 -> x0, local copies, waits for them, and re-layouts: 28.3 us -> none  [the longest x2 13.5 us: update_state(): recalled[..., None] * removed[:, None]]
    dot_general x11 -> x2, matrix products: 30.2 us -> 4.05 us  [the longest x1 2.1 us: removal_of(): jnp.dot(remove_low, w_remove_up, preferred_element_type=f32)]
    pallas_call x0 -> x4, Pallas kernels: none -> 23 us  [the longest x1 10.5 us: mixer(): pl.pallas_call(functools.partial(mixer_kernel, head=head), grid=(seqs //...]
    ppermute x0 -> x41, waiting for transfers between devices: none -> 14.8 us  [swap(): return lax.ppermute(piece, 'ep', [(i, i ^ bits) for i in range(size)])]
    add x2 -> x0, other arithmetic: 14 us -> none  [update_state(): blocks * decay_rate.reshape(seq_count, 1, head_count, head_size)]
  transfers between devices with their start and end apart: 3 -> 42, of which waited for: 1 -> 16; matrix products, arithmetic and copies ran while one was open for 23% -> 9% of each run, Pallas kernels for 0% -> 0%
where the time goes in v1:
time: 92.8 us; the launch traced here: 92.3 us
  starting transfers between devices  37.2 us (40%)
  Pallas kernels  23 us (25%)
  waiting for transfers between devices  20.6 us (22%)
  other arithmetic  4.58 us (5%)
  matrix products  4.05 us (4%)
  local copies, waits for them, and re-layouts  1.83 us (2%)
  between operations  1.08 us (1%)
    ppermute x41, starting transfers between devices, swap(): return lax.ppermute(piece, 'ep', [(i, i ^ bits) for i in range(size)])  31.7 us
    ppermute x41, waiting for transfers between devices, swap(): return lax.ppermute(piece, 'ep', [(i, i ^ bits) for i in range(size)])  14.8 us
    pallas_call x1, Pallas kernels, mixer(): pl.pallas_call(functools.partial(mixer_kernel, head=head), grid=(seqs //...  10.5 us
    pallas_call x1, Pallas kernels, run_experts(): pl.pallas_call(functools.partial(expert_kernel, count=count), out_shape=[...  7.59 us
    all_to_all x1, waiting for transfers between devices, shards(): lax.all_to_all(spread, 'ep', split_axis=0, concat_axis=0, tiled=True)  5.8 us
    all_to_all x1, starting transfers between devices, shards(): lax.all_to_all(spread, 'ep', split_axis=0, concat_axis=0, tiled=True)  5.56 us
    convert_element_type x7, other arithmetic, add(): return (a.astype(f32) + b.astype(f32)).astype(bf16)  3.81 us
    pallas_call x1, Pallas kernels, project(): pl.pallas_call(project_kernel, out_shape=jax.ShapeDtypeStruct((count, row...  3.22 us
  transfers between devices with their start and end apart: 42, of which 16 were waited for; matrix products, arithmetic and copies ran while one was open for 9% of the time, Pallas kernels for 0%

profile of v1, /device:TPU:0, one launch (start us, length us, event | category | flops | bytes accessed | tf_op | source)
XLA Modules:
  0.0 92.3 jit_solution(10342455530512958413)
XLA Ops:
  0.6 1.6 %norm_rows.1.refs_0_ = bf16[16,2048]{1,0:T(8,128)(2,1)} custom-call(bf16[16,2048]{1,0:T(8,128)(2,1)} %hidden_ref.1, f32[1,2048]{1,0:T(1,128)} %bitcast.49), custom_call_target="tpu_custom_call" | custom-call | tf_op jit(solution)/shard_map/norm_rows/pallas_call | solution.py:64
  2.3 4.1 %collective-permute-start.7 = (bf16[16,2048]{1,0:T(8,128)(2,1)}, bf16[16,2048]{1,0:T(8,128)(2,1)S(1)}, u32[]{:S(2)}, u32[]{:S(2)}) collective-permute-start(bf16[16,2048]{1,0:T(8,128)(2,1)} %norm_rows.1.refs_0_), channel_id=1, source_target_pairs={{0,8},{1,9},{2,10},{3,11},{4,12},{5,13},{6,14},{7,15},{8,0},{9,1},... | collective-permute-start | bytes 196616 | tf_op jit(solution)/shard_map/ppermute | solution.py:44
  6.4 1.3 %collective-permute-start.11 = (bf16[16,2048]{1,0:T(8,128)(2,1)}, bf16[16,2048]{1,0:T(8,128)(2,1)S(1)}, u32[]{:S(2)}, u32[]{:S(2)}) collective-permute-start(bf16[16,2048]{1,0:T(8,128)(2,1)} %norm_rows.1.refs_0_), channel_id=1, source_target_pairs={{0,12},{1,13},{2,14},{3,15},{4,8},{5,9},{6,10},{7,11},{8,4},{9,5},... | collective-permute-start | bytes 196616 | tf_op jit(solution)/shard_map/ppermute | solution.py:44
  7.7 0.2 collective-permute-start.3
  7.9 1.5 %collective-permute-start.1 = (bf16[16,2048]{1,0:T(8,128)(2,1)}, bf16[16,2048]{1,0:T(8,128)(2,1)S(1)}, u32[]{:S(2)}, u32[]{:S(2)}) collective-permute-start(bf16[16,2048]{1,0:T(8,128)(2,1)} %norm_rows.1.refs_0_), channel_id=1, source_target_pairs={{0,2},{1,3},{2,0},{3,1},{4,6},{5,7},{6,4},{7,5},{8,10},{9,11},{10,... | collective-permute-start | bytes 196616 | tf_op jit(solution)/shard_map/ppermute | solution.py:44
  9.5 0.8 collective-permute-done.7.refs_8_
  10.3 2.7 %collective-permute-start.9 = (bf16[16,2048]{1,0:T(8,128)(2,1)S(1)}, bf16[16,2048]{1,0:T(8,128)(2,1)S(1)}, u32[]{:S(2)}, u32[]{:S(2)}) collective-permute-start(bf16[16,2048]{1,0:T(8,128)(2,1)S(1)} %collective-permute-done.7.refs_8_), channel_id=1, source_target_pairs={{0,2},{1,3},{2,0},{3,1},{4,6},{5,7},{6,4},{7,5},{8,10},{9,11},{10,... | collective-permute-start | bytes 196616 | tf_op jit(solution)/shard_map/ppermute | solution.py:44
  12.9 1.3 %collective-permute-start.13 = (bf16[16,2048]{1,0:T(8,128)(2,1)S(1)}, bf16[16,2048]{1,0:T(8,128)(2,1)S(1)}, u32[]{:S(2)}, u32[]{:S(2)}) collective-permute-start(bf16[16,2048]{1,0:T(8,128)(2,1)S(1)} %collective-permute-done.11.refs_12_), channel_id=1, source_target_pairs={{0,2},{1,3},{2,0},{3,1},{4,6},{5,7},{6,4},{7,5},{8,10},{9,11},{10,... | collective-permute-start | bytes 196616 | tf_op jit(solution)/shard_map/ppermute | solution.py:44
  14.3 0.7 collective-permute-start.5
  15.0 0.5 collective-permute-start.4
  15.5 0.1 collective-permute-start.8
  15.6 1.6 %collective-permute-done.13.refs_14_ = bf16[16,2048]{1,0:T(8,128)(2,1)S(1)} collective-permute-done((bf16[16,2048]{1,0:T(8,128)(2,1)S(1)}, bf16[16,2048]{1,0:T(8,128)(2,1)S(1)}, u32[]{:S(2)}, u32[]{:S(2)}) %collective-permute-start.13) | collective-permute-done | bytes 65568 | tf_op jit(solution)/shard_map/ppermute | solution.py:44
  17.2 1.3 %collective-permute-done.5.refs_6_ = bf16[16,2048]{1,0:T(8,128)(2,1)S(1)} collective-permute-done((bf16[16,2048]{1,0:T(8,128)(2,1)S(1)}, bf16[16,2048]{1,0:T(8,128)(2,1)S(1)}, u32[]{:S(2)}, u32[]{:S(2)}) %collective-permute-start.5) | collective-permute-done | bytes 65568 | tf_op jit(solution)/shard_map/ppermute | solution.py:44
  18.5 0.5 collective-permute-start.14
  19.1 0.1 collective-permute-start.6
  19.1 1.9 %fusion.15.decay_ref = f32[16,1024]{1,0:T(8,128)} fusion(bf16[128,1024]{1,0:T(8,128)(2,1)} %param.27, bf16[16,2048]{1,0:T(8,128)(2,1)} %norm_rows.1.refs_0_, bf16[2048,128]{1,0:T(8,128)(2,1)S(1)} %copy-done, f32[1024]{0:T(1024)} %param.25), kind=kOutput, calls=%fused_computation.29 | convolution fusion | flops 12769280 | bytes 921600 | tf_op jit(solution)/shard_map/dot_general | solution.py:33
  21.3 0.4 copy-done.28
  21.8 3.2 %project.1 = bf16[16,16,192]{2,1,0:T(8,128)(2,1)} custom-call(s32[1]{0:T(128)} %bitcast.place_ref, bf16[16,2048]{1,0:T(8,128)(2,1)} %norm_rows.1.refs_0_, bf16[16,2048]{1,0:T(8,128)(2,1)} %copy-done.22, bf16[16,2048]{1,0:T(8,128)(2,1)} %copy-done.21, bf16[16,2048]{1,0:T(8,128)(2,1)} %copy-done.29, bf16[16,2048]{1,0:T(8,128)(2,1)} %copy-done.20, ...), custom_call_target="tpu_custom_call" | custom-call | tf_op jit(solution)/shard_map/project/pallas_call | solution.py:95
  25.0 5.6 %all-to-all-start = ((bf16[16,16,192]{2,1,0:T(8,128)(2,1)}), bf16[16,16,192]{2,1,0:T(8,128)(2,1)S(1)}, u32[]{:S(2)}, u32[]{:S(2)}) async-start(bf16[16,16,192]{2,1,0:T(8,128)(2,1)} %project.1), calls=%async_computation | async-start | bytes 262144 | tf_op jit(solution)/shard_map/all_to_all | solution.py:305
  30.6 2.1 %fusion.2.removal_ref = f32[16,1024]{1,0:T(8,128)} fusion(bf16[128,1024]{1,0:T(8,128)(2,1)} %param.29, bf16[16,2048]{1,0:T(8,128)(2,1)} %norm_rows.1.refs_0_, bf16[2048,128]{1,0:T(8,128)(2,1)} %param.28), kind=kOutput, calls=%fused_computation.3 | convolution fusion | flops 12634112 | bytes 917504 | tf_op jit(solution)/shard_map/dot_general | solution.py:39
  32.7 5.8 %all-to-all-done.joined_ref = bf16[16,16,192]{2,1,0:T(8,128)(2,1)S(1)} async-done(((bf16[16,16,192]{2,1,0:T(8,128)(2,1)}), bf16[16,16,192]{2,1,0:T(8,128)(2,1)S(1)}, u32[]{:S(2)}, u32[]{:S(2)}) %all-to-all-start) | async-done | bytes 98336 | tf_op jit(solution)/shard_map/all_to_all | solution.py:305
  38.5 0.6 copy-done.1
  39.1 10.5 %mixer.1 = (f32[16,64,1024]{2,1,0:T(8,128)}, f32[16,2048]{1,0:T(8,128)}, bf16[16,2048]{1,0:T(8,128)(2,1)}) custom-call(f32[16,64,1024]{2,1,0:T(8,128)} %state_ref.1, bf16[16,16,192]{2,1,0:T(8,128)(2,1)} %copy-done.1, f32[16,1024]{1,0:T(8,128)} %fusion.15.decay_ref, f32[16,1024]{1,0:T(8,128)} %fusion.2.removal_ref, f32[1,1024]{1,0:T(1,128)} %bitcast.50, ...), custom_call_target="tpu_custom_call" | custom-call | tf_op jit(solution)/shard_map/mixer/pallas_call | solution.py:194
  49.6 0.1 collective-permute-start.18
  49.7 1.2 %collective-permute-start.22 = (bf16[16,2048]{1,0:T(8,128)(2,1)}, bf16[16,2048]{1,0:T(8,128)(2,1)S(1)}, u32[]{:S(2)}, u32[]{:S(2)}) collective-permute-start(bf16[16,2048]{1,0:T(8,128)(2,1)} %get-tuple-element.14.refs_0_), channel_id=1, source_target_pairs={{0,8},{1,9},{2,10},{3,11},{4,12},{5,13},{6,14},{7,15},{8,0},{9,1},... | collective-permute-start | bytes 196616 | tf_op jit(solution)/shard_map/ppermute | solution.py:44
  51.0 3.1 %collective-permute-start.26 = (bf16[16,2048]{1,0:T(8,128)(2,1)}, bf16[16,2048]{1,0:T(8,128)(2,1)S(1)}, u32[]{:S(2)}, u32[]{:S(2)}) collective-permute-start(bf16[16,2048]{1,0:T(8,128)(2,1)} %get-tuple-element.14.refs_0_), channel_id=1, source_target_pairs={{0,12},{1,13},{2,14},{3,15},{4,8},{5,9},{6,10},{7,11},{8,4},{9,5},... | collective-permute-start | bytes 196616 | tf_op jit(solution)/shard_map/ppermute | solution.py:44
  54.1 0.5 collective-permute-done.18.refs_4_
  54.6 1.6 %collective-permute-start.20 = (bf16[16,2048]{1,0:T(8,128)(2,1)S(1)}, bf16[16,2048]{1,0:T(8,128)(2,1)S(1)}, u32[]{:S(2)}, u32[]{:S(2)}) collective-permute-start(bf16[16,2048]{1,0:T(8,128)(2,1)S(1)} %collective-permute-done.18.refs_4_), channel_id=1, source_target_pairs={{0,2},{1,3},{2,0},{3,1},{4,6},{5,7},{6,4},{7,5},{8,10},{9,11},{10,... | collective-permute-start | bytes 196616 | tf_op jit(solution)/shard_map/ppermute | solution.py:44
  56.2 1.9 %collective-permute-done.22.refs_8_ = bf16[16,2048]{1,0:T(8,128)(2,1)S(1)} collective-permute-done((bf16[16,2048]{1,0:T(8,128)(2,1)}, bf16[16,2048]{1,0:T(8,128)(2,1)S(1)}, u32[]{:S(2)}, u32[]{:S(2)}) %collective-permute-start.22) | collective-permute-done | bytes 65568 | tf_op jit(solution)/shard_map/ppermute | solution.py:44
  58.1 0.7 collective-permute-start.24
  58.8 1.3 %collective-permute-start.28 = (bf16[16,2048]{1,0:T(8,128)(2,1)S(1)}, bf16[16,2048]{1,0:T(8,128)(2,1)S(1)}, u32[]{:S(2)}, u32[]{:S(2)}) collective-permute-start(bf16[16,2048]{1,0:T(8,128)(2,1)S(1)} %collective-permute-done.26.refs_12_), channel_id=1, source_target_pairs={{0,2},{1,3},{2,0},{3,1},{4,6},{5,7},{6,4},{7,5},{8,10},{9,11},{10,... | collective-permute-start | bytes 196616 | tf_op jit(solution)/shard_map/ppermute | solution.py:44
  60.2 0.5 collective-permute-start.23
  60.7 0.1 collective-permute-start.27
  60.8 1.6 %collective-permute-done.24.refs_10_ = bf16[16,2048]{1,0:T(8,128)(2,1)S(1)} collective-permute-done((bf16[16,2048]{1,0:T(8,128)(2,1)S(1)}, bf16[16,2048]{1,0:T(8,128)(2,1)S(1)}, u32[]{:S(2)}, u32[]{:S(2)}) %collective-permute-start.24) | collective-permute-done | bytes 65568 | tf_op jit(solution)/shard_map/ppermute | solution.py:44
  62.4 0.7 collective-permute-done.28.refs_14_
  63.1 0.5 collective-permute-start.25
  63.6 0.1 collective-permute-start.29
  63.7 0.6 collective-permute-done.21.refs_7_
  64.4 0.2 collective-permute-done.25.refs_11_
  64.5 0.4 collective-permute-done.29.refs_15_
  65.0 0.1 copy-done.16
  65.1 0.4 copy-done.17
  65.5 7.6 %experts.1 = (bf16[2,16,2048]{2,1,0:T(8,128)(2,1)}, bf16[2,16,2048]{2,1,0:T(8,128)(2,1)}, bf16[2,16,2048]{2,1,0:T(8,128)(2,1)}, bf16[2,16,2048]{2,1,0:T(8,128)(2...) custom-call(bf16[16,2048]{1,0:T(8,128)(2,1)} %get-tuple-element.14.r, ...), custom_call_target="tpu_custom_call" | custom-call | tf_op jit(solution)/shard_map/experts/pallas_call | solution.py:264
  73.1 0.2 collective-permute-start.39
  73.3 0.4 collective-permute-start.30
  73.7 0.2 collective-permute-start.33
  73.8 0.4 collective-permute-start.36
  74.2 0.5 collective-permute-done.39
  74.7 0.9 %add_convert_fusion = bf16[2,16,2048]{2,1,0:T(8,128)(2,1)S(1)} fusion(bf16[2,16,2048]{2,1,0:T(8,128)(2,1)S(1)} %collective-permute-done.39, bf16[2,16,2048]{2,1,0:T(8,128)(2,1)} %get-tuple-element.21), kind=kLoop, calls=%fused_computation.11 | loop fusion | flops 262144 | bytes 393216 | tf_op jit(solution)/shard_map/convert_element_type | solution.py:276
  75.7 1.4 %collective-permute-start.40 = (bf16[16,2048]{1,0:T(8,128)(2,1)S(1)}, bf16[16,2048]{1,0:T(8,128)(2,1)S(1)}, u32[]{:S(2)}, u32[]{:S(2)}) collective-permute-start(bf16[16,2048]{1,0:T(8,128)(2,1)S(1)} %slice_bitcast_fusion), channel_id=1, source_target_pairs={{0,2},{1,3},{2,0},{3,1},{4,6},{5,7},{6,4},{7,5},{8,10},{9,11},{10,... | collective-permute-start | bytes 196616 | tf_op jit(solution)/shard_map/ppermute | solution.py:44
  77.1 0.9 %add_convert_fusion.3 = bf16[2,16,2048]{2,1,0:T(8,128)(2,1)S(1)} fusion(bf16[2,16,2048]{2,1,0:T(8,128)(2,1)S(1)} %collective-permute-done.30, bf16[2,16,2048]{2,1,0:T(8,128)(2,1)} %get-tuple-element.15), kind=kLoop, calls=%fused_computation.14 | loop fusion | flops 262144 | bytes 393216 | tf_op jit(solution)/shard_map/convert_element_type | solution.py:276
  78.0 0.8 collective-permute-start.31
  78.8 0.9 %add_convert_fusion.2 = bf16[2,16,2048]{2,1,0:T(8,128)(2,1)S(1)} fusion(bf16[2,16,2048]{2,1,0:T(8,128)(2,1)S(1)} %collective-permute-done.33, bf16[2,16,2048]{2,1,0:T(8,128)(2,1)} %get-tuple-element.17), kind=kLoop, calls=%fused_computation.13 | loop fusion | flops 262144 | bytes 393216 | tf_op jit(solution)/shard_map/convert_element_type | solution.py:276
  79.7 1.4 %collective-permute-start.34 = (bf16[16,2048]{1,0:T(8,128)(2,1)S(1)}, bf16[16,2048]{1,0:T(8,128)(2,1)S(1)}, u32[]{:S(2)}, u32[]{:S(2)}) collective-permute-start(bf16[16,2048]{1,0:T(8,128)(2,1)S(1)} %slice_bitcast_fusion.4), channel_id=1, source_target_pairs={{0,2},{1,3},{2,0},{3,1},{4,6},{5,7},{6,4},{7,5},{8,10},{9,11},{10,... | collective-permute-start | bytes 196616 | tf_op jit(solution)/shard_map/ppermute | solution.py:44
  81.1 0.9 %add_convert_fusion.1 = bf16[2,16,2048]{2,1,0:T(8,128)(2,1)S(1)} fusion(bf16[2,16,2048]{2,1,0:T(8,128)(2,1)S(1)} %collective-permute-done.36, bf16[2,16,2048]{2,1,0:T(8,128)(2,1)} %get-tuple-element.19), kind=kLoop, calls=%fused_computation.12 | loop fusion | flops 262144 | bytes 393216 | tf_op jit(solution)/shard_map/convert_element_type | solution.py:276
  82.1 0.8 collective-permute-start.37
  82.9 1.8 %collective-permute-start.32 = (bf16[16,2048]{1,0:T(8,128)(2,1)S(1)}, bf16[16,2048]{1,0:T(8,128)(2,1)S(1)}, u32[]{:S(2)}, u32[]{:S(2)}) collective-permute-start(bf16[16,2048]{1,0:T(8,128)(2,1)S(1)} %fusion.10), channel_id=1, source_target_pairs={{0,12},{1,13},{2,14},{3,15},{4,8},{5,9},{6,10},{7,11},{8,4},{9,5},... | collective-permute-start | bytes 196616 | tf_op jit(solution)/shard_map/ppermute | solution.py:44
  84.7 1.1 %collective-permute-start.35 = (bf16[16,2048]{1,0:T(8,128)(2,1)S(1)}, bf16[16,2048]{1,0:T(8,128)(2,1)S(1)}, u32[]{:S(2)}, u32[]{:S(2)}) collective-permute-start(bf16[16,2048]{1,0:T(8,128)(2,1)S(1)} %fusion.9), channel_id=1, source_target_pairs={{0,8},{1,9},{2,10},{3,11},{4,12},{5,13},{6,14},{7,15},{8,0},{9,1},... | collective-permute-start | bytes 196616 | tf_op jit(solution)/shard_map/ppermute | solution.py:44
  85.8 0.6 collective-permute-done.37
  86.4 1.1 %collective-permute-start.38 = (bf16[16,2048]{1,0:T(8,128)(2,1)S(1)}, bf16[16,2048]{1,0:T(8,128)(2,1)S(1)}, u32[]{:S(2)}, u32[]{:S(2)}) collective-permute-start(bf16[16,2048]{1,0:T(8,128)(2,1)S(1)} %fusion.8), channel_id=1, source_target_pairs={{0,4},{1,5},{2,6},{3,7},{4,0},{5,1},{6,2},{7,3},{8,12},{9,13},{10,... | collective-permute-start | bytes 196616 | tf_op jit(solution)/shard_map/ppermute | solution.py:44
  87.6 2.1 %collective-permute-done.32 = bf16[16,2048]{1,0:T(8,128)(2,1)S(1)} collective-permute-done((bf16[16,2048]{1,0:T(8,128)(2,1)S(1)}, bf16[16,2048]{1,0:T(8,128)(2,1)S(1)}, u32[]{:S(2)}, u32[]{:S(2)}) %collective-permute-start.32) | collective-permute-done | bytes 65568 | tf_op jit(solution)/shard_map/ppermute | solution.py:44
  89.7 1.7 %collective-permute-done.35 = bf16[16,2048]{1,0:T(8,128)(2,1)S(1)} collective-permute-done((bf16[16,2048]{1,0:T(8,128)(2,1)S(1)}, bf16[16,2048]{1,0:T(8,128)(2,1)S(1)}, u32[]{:S(2)}, u32[]{:S(2)}) %collective-permute-start.35) | collective-permute-done | bytes 65568 | tf_op jit(solution)/shard_map/ppermute | solution.py:44
  91.4 0.2 collective-permute-done.38
  91.6 0.7 add_convert_fusion.4
  (109 shorter events, 0.4 us)
Async XLA Ops:
  0.6 18.5 %copy-start = (bf16[2048,128]{1,0:T(8,128)(2,1)S(1)}, bf16[2048,128]{1,0:T(8,128)(2,1)}, u32[]{:S(2)}) copy-start(bf16[2048,128]{1,0:T(8,128)(2,1)} %param.26) | copy-start | bytes 1572868
  2.3 8.0 %collective-permute-start.7 = (bf16[16,2048]{1,0:T(8,128)(2,1)}, bf16[16,2048]{1,0:T(8,128)(2,1)S(1)}, u32[]{:S(2)}, u32[]{:S(2)}) collective-permute-start(bf16[16,2048]{1,0:T(8,128)(2,1)} %norm_rows.1.refs_0_), channel_id=1, source_target_pairs={{0,8},{1,9},{2,10},{3,11},{4,12},{5,13},{6,14},{7,15},{8,0},{9,1},... | collective-permute-start | bytes 196616 | tf_op jit(solution)/shard_map/ppermute | solution.py:44
  6.4 6.6 %collective-permute-start.11 = (bf16[16,2048]{1,0:T(8,128)(2,1)}, bf16[16,2048]{1,0:T(8,128)(2,1)S(1)}, u32[]{:S(2)}, u32[]{:S(2)}) collective-permute-start(bf16[16,2048]{1,0:T(8,128)(2,1)} %norm_rows.1.refs_0_), channel_id=1, source_target_pairs={{0,12},{1,13},{2,14},{3,15},{4,8},{5,9},{6,10},{7,11},{8,4},{9,5},... | collective-permute-start | bytes 196616 | tf_op jit(solution)/shard_map/ppermute | solution.py:44
  7.7 6.6 %collective-permute-start.3 = (bf16[16,2048]{1,0:T(8,128)(2,1)}, bf16[16,2048]{1,0:T(8,128)(2,1)S(1)}, u32[]{:S(2)}, u32[]{:S(2)}) collective-permute-start(bf16[16,2048]{1,0:T(8,128)(2,1)} %norm_rows.1.refs_0_), channel_id=1, source_target_pairs={{0,4},{1,5},{2,6},{3,7},{4,0},{5,1},{6,2},{7,3},{8,12},{9,13},{10,... | collective-permute-start | bytes 196616 | tf_op jit(solution)/shard_map/ppermute | solution.py:44
  7.9 7.0 %collective-permute-start.1 = (bf16[16,2048]{1,0:T(8,128)(2,1)}, bf16[16,2048]{1,0:T(8,128)(2,1)S(1)}, u32[]{:S(2)}, u32[]{:S(2)}) collective-permute-start(bf16[16,2048]{1,0:T(8,128)(2,1)} %norm_rows.1.refs_0_), channel_id=1, source_target_pairs={{0,2},{1,3},{2,0},{3,1},{4,6},{5,7},{6,4},{7,5},{8,10},{9,11},{10,... | collective-permute-start | bytes 196616 | tf_op jit(solution)/shard_map/ppermute | solution.py:44
  9.5 5.5 %collective-permute-start = (bf16[16,2048]{1,0:T(8,128)(2,1)}, bf16[16,2048]{1,0:T(8,128)(2,1)S(1)}, u32[]{:S(2)}, u32[]{:S(2)}) collective-permute-start(bf16[16,2048]{1,0:T(8,128)(2,1)} %norm_rows.1.refs_0_), channel_id=1, source_target_pairs={{0,1},{1,0},{2,3},{3,2},{4,5},{5,4},{6,7},{7,6},{8,9},{9,8},{10,11... | collective-permute-start | bytes 196616 | tf_op jit(solution)/shard_map/ppermute | solution.py:44
  10.3 10.9 %copy-start.18 = (bf16[16,2048]{1,0:T(8,128)(2,1)}, bf16[16,2048]{1,0:T(8,128)(2,1)S(1)}, u32[]{:S(2)}) copy-start(bf16[16,2048]{1,0:T(8,128)(2,1)S(1)} %collective-permute-done.7.refs_8_) | copy-start | bytes 196612
  10.3 5.2 %collective-permute-start.9 = (bf16[16,2048]{1,0:T(8,128)(2,1)S(1)}, bf16[16,2048]{1,0:T(8,128)(2,1)S(1)}, u32[]{:S(2)}, u32[]{:S(2)}) collective-permute-start(bf16[16,2048]{1,0:T(8,128)(2,1)S(1)} %collective-permute-done.7.refs_8_), channel_id=1, source_target_pairs={{0,2},{1,3},{2,0},{3,1},{4,6},{5,7},{6,4},{7,5},{8,10},{9,11},{10,... | collective-permute-start | bytes 196616 | tf_op jit(solution)/shard_map/ppermute | solution.py:44
  12.9 8.3 %copy-start.19 = (bf16[16,2048]{1,0:T(8,128)(2,1)}, bf16[16,2048]{1,0:T(8,128)(2,1)S(1)}, u32[]{:S(2)}) copy-start(bf16[16,2048]{1,0:T(8,128)(2,1)S(1)} %collective-permute-done.11.refs_12_) | copy-start | bytes 196612
  12.9 4.3 %collective-permute-start.13 = (bf16[16,2048]{1,0:T(8,128)(2,1)S(1)}, bf16[16,2048]{1,0:T(8,128)(2,1)S(1)}, u32[]{:S(2)}, u32[]{:S(2)}) collective-permute-start(bf16[16,2048]{1,0:T(8,128)(2,1)S(1)} %collective-permute-done.11.refs_12_), channel_id=1, source_target_pairs={{0,2},{1,3},{2,0},{3,1},{4,6},{5,7},{6,4},{7,5},{8,10},{9,11},{10,... | collective-permute-start | bytes 196616 | tf_op jit(solution)/shard_map/ppermute | solution.py:44
  14.3 6.9 %copy-start.20 = (bf16[16,2048]{1,0:T(8,128)(2,1)}, bf16[16,2048]{1,0:T(8,128)(2,1)S(1)}, u32[]{:S(2)}) copy-start(bf16[16,2048]{1,0:T(8,128)(2,1)S(1)} %collective-permute-done.3.refs_4_) | copy-start | bytes 196612
  14.3 4.3 %collective-permute-start.5 = (bf16[16,2048]{1,0:T(8,128)(2,1)S(1)}, bf16[16,2048]{1,0:T(8,128)(2,1)S(1)}, u32[]{:S(2)}, u32[]{:S(2)}) collective-permute-start(bf16[16,2048]{1,0:T(8,128)(2,1)S(1)} %collective-permute-done.3.refs_4_), channel_id=1, source_target_pairs={{0,2},{1,3},{2,0},{3,1},{4,6},{5,7},{6,4},{7,5},{8,10},{9,11},{10,... | collective-permute-start | bytes 196616 | tf_op jit(solution)/shard_map/ppermute | solution.py:44
  15.0 6.2 %copy-start.21 = (bf16[16,2048]{1,0:T(8,128)(2,1)}, bf16[16,2048]{1,0:T(8,128)(2,1)S(1)}, u32[]{:S(2)}) copy-start(bf16[16,2048]{1,0:T(8,128)(2,1)S(1)} %collective-permute-done.1.refs_2_) | copy-start | bytes 196612
  15.0 3.6 %collective-permute-start.12 = (bf16[16,2048]{1,0:T(8,128)(2,1)S(1)}, bf16[16,2048]{1,0:T(8,128)(2,1)S(1)}, u32[]{:S(2)}, u32[]{:S(2)}) collective-permute-start(bf16[16,2048]{1,0:T(8,128)(2,1)S(1)} %collective-permute-done.11.refs_12_), channel_id=1, source_target_pairs={{0,1},{1,0},{2,3},{3,2},{4,5},{5,4},{6,7},{7,6},{8,9},{9,8},{10,11... | collective-permute-start | bytes 196616 | tf_op jit(solution)/shard_map/ppermute | solution.py:44
  15.0 6.2 %copy-start.22 = (bf16[16,2048]{1,0:T(8,128)(2,1)}, bf16[16,2048]{1,0:T(8,128)(2,1)S(1)}, u32[]{:S(2)}) copy-start(bf16[16,2048]{1,0:T(8,128)(2,1)S(1)} %collective-permute-done.refs_1_) | copy-start | bytes 196612
  15.0 4.1 %collective-permute-start.4 = (bf16[16,2048]{1,0:T(8,128)(2,1)S(1)}, bf16[16,2048]{1,0:T(8,128)(2,1)S(1)}, u32[]{:S(2)}, u32[]{:S(2)}) collective-permute-start(bf16[16,2048]{1,0:T(8,128)(2,1)S(1)} %collective-permute-done.3.refs_4_), channel_id=1, source_target_pairs={{0,1},{1,0},{2,3},{3,2},{4,5},{5,4},{6,7},{7,6},{8,9},{9,8},{10,11... | collective-permute-start | bytes 196616 | tf_op jit(solution)/shard_map/ppermute | solution.py:44
  15.5 5.7 %copy-start.23 = (bf16[16,2048]{1,0:T(8,128)(2,1)}, bf16[16,2048]{1,0:T(8,128)(2,1)S(1)}, u32[]{:S(2)}) copy-start(bf16[16,2048]{1,0:T(8,128)(2,1)S(1)} %collective-permute-done.9.refs_10_) | copy-start | bytes 196612
  15.5 5.6 %collective-permute-start.8 = (bf16[16,2048]{1,0:T(8,128)(2,1)S(1)}, bf16[16,2048]{1,0:T(8,128)(2,1)S(1)}, u32[]{:S(2)}, u32[]{:S(2)}) collective-permute-start(bf16[16,2048]{1,0:T(8,128)(2,1)S(1)} %collective-permute-done.7.refs_8_), channel_id=1, source_target_pairs={{0,1},{1,0},{2,3},{3,2},{4,5},{5,4},{6,7},{7,6},{8,9},{9,8},{10,11... | collective-permute-start | bytes 196616 | tf_op jit(solution)/shard_map/ppermute | solution.py:44
  17.2 4.0 %copy-start.24 = (bf16[16,2048]{1,0:T(8,128)(2,1)}, bf16[16,2048]{1,0:T(8,128)(2,1)S(1)}, u32[]{:S(2)}) copy-start(bf16[16,2048]{1,0:T(8,128)(2,1)S(1)} %collective-permute-done.13.refs_14_) | copy-start | bytes 196612
  17.2 3.9 %collective-permute-start.2 = (bf16[16,2048]{1,0:T(8,128)(2,1)S(1)}, bf16[16,2048]{1,0:T(8,128)(2,1)S(1)}, u32[]{:S(2)}, u32[]{:S(2)}) collective-permute-start(bf16[16,2048]{1,0:T(8,128)(2,1)S(1)} %collective-permute-done.1.refs_2_), channel_id=1, source_target_pairs={{0,1},{1,0},{2,3},{3,2},{4,5},{5,4},{6,7},{7,6},{8,9},{9,8},{10,11... | collective-permute-start | bytes 196616 | tf_op jit(solution)/shard_map/ppermute | solution.py:44
  18.5 2.7 %copy-start.25 = (bf16[16,2048]{1,0:T(8,128)(2,1)}, bf16[16,2048]{1,0:T(8,128)(2,1)S(1)}, u32[]{:S(2)}) copy-start(bf16[16,2048]{1,0:T(8,128)(2,1)S(1)} %collective-permute-done.5.refs_6_) | copy-start | bytes 196612
  18.5 2.6 %collective-permute-start.10 = (bf16[16,2048]{1,0:T(8,128)(2,1)S(1)}, bf16[16,2048]{1,0:T(8,128)(2,1)S(1)}, u32[]{:S(2)}, u32[]{:S(2)}) collective-permute-start(bf16[16,2048]{1,0:T(8,128)(2,1)S(1)} %collective-permute-done.9.refs_10_), channel_id=1, source_target_pairs={{0,1},{1,0},{2,3},{3,2},{4,5},{5,4},{6,7},{7,6},{8,9},{9,8},{10,11... | collective-permute-start | bytes 196616 | tf_op jit(solution)/shard_map/ppermute | solution.py:44
  18.5 2.7 %copy-start.26 = (bf16[16,2048]{1,0:T(8,128)(2,1)}, bf16[16,2048]{1,0:T(8,128)(2,1)S(1)}, u32[]{:S(2)}) copy-start(bf16[16,2048]{1,0:T(8,128)(2,1)S(1)} %collective-permute-done.12.refs_13_) | copy-start | bytes 196612
  18.5 2.6 %collective-permute-start.14 = (bf16[16,2048]{1,0:T(8,128)(2,1)S(1)}, bf16[16,2048]{1,0:T(8,128)(2,1)S(1)}, u32[]{:S(2)}, u32[]{:S(2)}) collective-permute-start(bf16[16,2048]{1,0:T(8,128)(2,1)S(1)} %collective-permute-done.13.refs_14_), channel_id=1, source_target_pairs={{0,1},{1,0},{2,3},{3,2},{4,5},{5,4},{6,7},{7,6},{8,9},{9,8},{10,11... | collective-permute-start | bytes 196616 | tf_op jit(solution)/shard_map/ppermute | solution.py:44
  19.1 2.2 %copy-start.27 = (bf16[16,2048]{1,0:T(8,128)(2,1)}, bf16[16,2048]{1,0:T(8,128)(2,1)S(1)}, u32[]{:S(2)}) copy-start(bf16[16,2048]{1,0:T(8,128)(2,1)S(1)} %collective-permute-done.4.refs_5_) | copy-start | bytes 196612
  19.1 2.1 %collective-permute-start.6 = (bf16[16,2048]{1,0:T(8,128)(2,1)S(1)}, bf16[16,2048]{1,0:T(8,128)(2,1)S(1)}, u32[]{:S(2)}, u32[]{:S(2)}) collective-permute-start(bf16[16,2048]{1,0:T(8,128)(2,1)S(1)} %collective-permute-done.5.refs_6_), channel_id=1, source_target_pairs={{0,1},{1,0},{2,3},{3,2},{4,5},{5,4},{6,7},{7,6},{8,9},{9,8},{10,11... | collective-permute-start | bytes 196616 | tf_op jit(solution)/shard_map/ppermute | solution.py:44
  25.0 13.5 %all-to-all-start = ((bf16[16,16,192]{2,1,0:T(8,128)(2,1)}), bf16[16,16,192]{2,1,0:T(8,128)(2,1)S(1)}, u32[]{:S(2)}, u32[]{:S(2)}) async-start(bf16[16,16,192]{2,1,0:T(8,128)(2,1)} %project.1), calls=%async_computation | async-start | bytes 262144 | tf_op jit(solution)/shard_map/all_to_all | solution.py:305
  49.6 4.9 %collective-permute-start.18 = (bf16[16,2048]{1,0:T(8,128)(2,1)}, bf16[16,2048]{1,0:T(8,128)(2,1)S(1)}, u32[]{:S(2)}, u32[]{:S(2)}) collective-permute-start(bf16[16,2048]{1,0:T(8,128)(2,1)} %get-tuple-element.14.refs_0_), channel_id=1, source_target_pairs={{0,4},{1,5},{2,6},{3,7},{4,0},{5,1},{6,2},{7,3},{8,12},{9,13},{10,... | collective-permute-start | bytes 196616 | tf_op jit(solution)/shard_map/ppermute | solution.py:44
  49.7 8.4 %collective-permute-start.22 = (bf16[16,2048]{1,0:T(8,128)(2,1)}, bf16[16,2048]{1,0:T(8,128)(2,1)S(1)}, u32[]{:S(2)}, u32[]{:S(2)}) collective-permute-start(bf16[16,2048]{1,0:T(8,128)(2,1)} %get-tuple-element.14.refs_0_), channel_id=1, source_target_pairs={{0,8},{1,9},{2,10},{3,11},{4,12},{5,13},{6,14},{7,15},{8,0},{9,1},... | collective-permute-start | bytes 196616 | tf_op jit(solution)/shard_map/ppermute | solution.py:44
  51.0 7.9 %collective-permute-start.26 = (bf16[16,2048]{1,0:T(8,128)(2,1)}, bf16[16,2048]{1,0:T(8,128)(2,1)S(1)}, u32[]{:S(2)}, u32[]{:S(2)}) collective-permute-start(bf16[16,2048]{1,0:T(8,128)(2,1)} %get-tuple-element.14.refs_0_), channel_id=1, source_target_pairs={{0,12},{1,13},{2,14},{3,15},{4,8},{5,9},{6,10},{7,11},{8,4},{9,5},... | collective-permute-start | bytes 196616 | tf_op jit(solution)/shard_map/ppermute | solution.py:44
  54.1 6.0 %collective-permute-start.16 = (bf16[16,2048]{1,0:T(8,128)(2,1)}, bf16[16,2048]{1,0:T(8,128)(2,1)S(1)}, u32[]{:S(2)}, u32[]{:S(2)}) collective-permute-start(bf16[16,2048]{1,0:T(8,128)(2,1)} %get-tuple-element.14.refs_0_), channel_id=1, source_target_pairs={{0,2},{1,3},{2,0},{3,1},{4,6},{5,7},{6,4},{7,5},{8,10},{9,11},{10,... | collective-permute-start | bytes 196616 | tf_op jit(solution)/shard_map/ppermute | solution.py:44
  54.1 6.0 %collective-permute-start.15 = (bf16[16,2048]{1,0:T(8,128)(2,1)}, bf16[16,2048]{1,0:T(8,128)(2,1)S(1)}, u32[]{:S(2)}, u32[]{:S(2)}) collective-permute-start(bf16[16,2048]{1,0:T(8,128)(2,1)} %get-tuple-element.14.refs_0_), channel_id=1, source_target_pairs={{0,1},{1,0},{2,3},{3,2},{4,5},{5,4},{6,7},{7,6},{8,9},{9,8},{10,11... | collective-permute-start | bytes 196616 | tf_op jit(solution)/shard_map/ppermute | solution.py:44
  54.6 10.3 %copy-start.3 = (bf16[16,2048]{1,0:T(8,128)(2,1)}, bf16[16,2048]{1,0:T(8,128)(2,1)S(1)}, u32[]{:S(2)}) copy-start(bf16[16,2048]{1,0:T(8,128)(2,1)S(1)} %collective-permute-done.18.refs_4_) | copy-start | bytes 196612
  54.6 6.1 %collective-permute-start.20 = (bf16[16,2048]{1,0:T(8,128)(2,1)S(1)}, bf16[16,2048]{1,0:T(8,128)(2,1)S(1)}, u32[]{:S(2)}, u32[]{:S(2)}) collective-permute-start(bf16[16,2048]{1,0:T(8,128)(2,1)S(1)} %collective-permute-done.18.refs_4_), channel_id=1, source_target_pairs={{0,2},{1,3},{2,0},{3,1},{4,6},{5,7},{6,4},{7,5},{8,10},{9,11},{10,... | collective-permute-start | bytes 196616 | tf_op jit(solution)/shard_map/ppermute | solution.py:44
  58.1 6.8 %copy-start.4 = (bf16[16,2048]{1,0:T(8,128)(2,1)}, bf16[16,2048]{1,0:T(8,128)(2,1)S(1)}, u32[]{:S(2)}) copy-start(bf16[16,2048]{1,0:T(8,128)(2,1)S(1)} %collective-permute-done.22.refs_8_) | copy-start | bytes 196612
  58.1 4.3 %collective-permute-start.24 = (bf16[16,2048]{1,0:T(8,128)(2,1)S(1)}, bf16[16,2048]{1,0:T(8,128)(2,1)S(1)}, u32[]{:S(2)}, u32[]{:S(2)}) collective-permute-start(bf16[16,2048]{1,0:T(8,128)(2,1)S(1)} %collective-permute-done.22.refs_8_), channel_id=1, source_target_pairs={{0,2},{1,3},{2,0},{3,1},{4,6},{5,7},{6,4},{7,5},{8,10},{9,11},{10,... | collective-permute-start | bytes 196616 | tf_op jit(solution)/shard_map/ppermute | solution.py:44
  58.8 6.1 %copy-start.5 = (bf16[16,2048]{1,0:T(8,128)(2,1)}, bf16[16,2048]{1,0:T(8,128)(2,1)S(1)}, u32[]{:S(2)}) copy-start(bf16[16,2048]{1,0:T(8,128)(2,1)S(1)} %collective-permute-done.26.refs_12_) | copy-start | bytes 196612
  58.8 4.3 %collective-permute-start.28 = (bf16[16,2048]{1,0:T(8,128)(2,1)S(1)}, bf16[16,2048]{1,0:T(8,128)(2,1)S(1)}, u32[]{:S(2)}, u32[]{:S(2)}) collective-permute-start(bf16[16,2048]{1,0:T(8,128)(2,1)S(1)} %collective-permute-done.26.refs_12_), channel_id=1, source_target_pairs={{0,2},{1,3},{2,0},{3,1},{4,6},{5,7},{6,4},{7,5},{8,10},{9,11},{10,... | collective-permute-start | bytes 196616 | tf_op jit(solution)/shard_map/ppermute | solution.py:44
  60.1 4.7 %copy-start.6 = (bf16[16,2048]{1,0:T(8,128)(2,1)}, bf16[16,2048]{1,0:T(8,128)(2,1)S(1)}, u32[]{:S(2)}) copy-start(bf16[16,2048]{1,0:T(8,128)(2,1)S(1)} %collective-permute-done.16.refs_2_) | copy-start | bytes 196612
  60.1 3.0 %collective-permute-start.19 = (bf16[16,2048]{1,0:T(8,128)(2,1)S(1)}, bf16[16,2048]{1,0:T(8,128)(2,1)S(1)}, u32[]{:S(2)}, u32[]{:S(2)}) collective-permute-start(bf16[16,2048]{1,0:T(8,128)(2,1)S(1)} %collective-permute-done.18.refs_4_), channel_id=1, source_target_pairs={{0,1},{1,0},{2,3},{3,2},{4,5},{5,4},{6,7},{7,6},{8,9},{9,8},{10,11... | collective-permute-start | bytes 196616 | tf_op jit(solution)/shard_map/ppermute | solution.py:44
  60.2 4.7 %copy-start.7 = (bf16[16,2048]{1,0:T(8,128)(2,1)}, bf16[16,2048]{1,0:T(8,128)(2,1)S(1)}, u32[]{:S(2)}) copy-start(bf16[16,2048]{1,0:T(8,128)(2,1)S(1)} %collective-permute-done.15.refs_1_) | copy-start | bytes 196612
  60.2 3.4 %collective-permute-start.23 = (bf16[16,2048]{1,0:T(8,128)(2,1)S(1)}, bf16[16,2048]{1,0:T(8,128)(2,1)S(1)}, u32[]{:S(2)}, u32[]{:S(2)}) collective-permute-start(bf16[16,2048]{1,0:T(8,128)(2,1)S(1)} %collective-permute-done.22.refs_8_), channel_id=1, source_target_pairs={{0,1},{1,0},{2,3},{3,2},{4,5},{5,4},{6,7},{7,6},{8,9},{9,8},{10,11... | collective-permute-start | bytes 196616 | tf_op jit(solution)/shard_map/ppermute | solution.py:44
  60.7 4.2 %copy-start.8 = (bf16[16,2048]{1,0:T(8,128)(2,1)}, bf16[16,2048]{1,0:T(8,128)(2,1)S(1)}, u32[]{:S(2)}) copy-start(bf16[16,2048]{1,0:T(8,128)(2,1)S(1)} %collective-permute-done.20.refs_6_) | copy-start | bytes 196612
  60.7 3.0 %collective-permute-start.27 = (bf16[16,2048]{1,0:T(8,128)(2,1)S(1)}, bf16[16,2048]{1,0:T(8,128)(2,1)S(1)}, u32[]{:S(2)}, u32[]{:S(2)}) collective-permute-start(bf16[16,2048]{1,0:T(8,128)(2,1)S(1)} %collective-permute-done.26.refs_12_), channel_id=1, source_target_pairs={{0,1},{1,0},{2,3},{3,2},{4,5},{5,4},{6,7},{7,6},{8,9},{9,8},{10,11... | collective-permute-start | bytes 196616 | tf_op jit(solution)/shard_map/ppermute | solution.py:44
  62.4 2.5 %copy-start.9 = (bf16[16,2048]{1,0:T(8,128)(2,1)}, bf16[16,2048]{1,0:T(8,128)(2,1)S(1)}, u32[]{:S(2)}) copy-start(bf16[16,2048]{1,0:T(8,128)(2,1)S(1)} %collective-permute-done.24.refs_10_) | copy-start | bytes 196612
  62.4 1.3 %collective-permute-start.17 = (bf16[16,2048]{1,0:T(8,128)(2,1)S(1)}, bf16[16,2048]{1,0:T(8,128)(2,1)S(1)}, u32[]{:S(2)}, u32[]{:S(2)}) collective-permute-start(bf16[16,2048]{1,0:T(8,128)(2,1)S(1)} %collective-permute-done.16.refs_2_), channel_id=1, source_target_pairs={{0,1},{1,0},{2,3},{3,2},{4,5},{5,4},{6,7},{7,6},{8,9},{9,8},{10,11... | collective-permute-start | bytes 196616 | tf_op jit(solution)/shard_map/ppermute | solution.py:44
  63.1 1.8 %copy-start.10 = (bf16[16,2048]{1,0:T(8,128)(2,1)}, bf16[16,2048]{1,0:T(8,128)(2,1)S(1)}, u32[]{:S(2)}) copy-start(bf16[16,2048]{1,0:T(8,128)(2,1)S(1)} %collective-permute-done.28.refs_14_) | copy-start | bytes 196612
  63.1 1.3 %collective-permute-start.21 = (bf16[16,2048]{1,0:T(8,128)(2,1)S(1)}, bf16[16,2048]{1,0:T(8,128)(2,1)S(1)}, u32[]{:S(2)}, u32[]{:S(2)}) collective-permute-start(bf16[16,2048]{1,0:T(8,128)(2,1)S(1)} %collective-permute-done.20.refs_6_), channel_id=1, source_target_pairs={{0,1},{1,0},{2,3},{3,2},{4,5},{5,4},{6,7},{7,6},{8,9},{9,8},{10,11... | collective-permute-start | bytes 196616 | tf_op jit(solution)/shard_map/ppermute | solution.py:44
  63.1 1.4 %collective-permute-start.25 = (bf16[16,2048]{1,0:T(8,128)(2,1)S(1)}, bf16[16,2048]{1,0:T(8,128)(2,1)S(1)}, u32[]{:S(2)}, u32[]{:S(2)}) collective-permute-start(bf16[16,2048]{1,0:T(8,128)(2,1)S(1)} %collective-permute-done.24.refs_10_), channel_id=1, source_target_pairs={{0,1},{1,0},{2,3},{3,2},{4,5},{5,4},{6,7},{7,6},{8,9},{9,8},{10,11... | collective-permute-start | bytes 196616 | tf_op jit(solution)/shard_map/ppermute | solution.py:44
  63.6 1.3 %collective-permute-start.29 = (bf16[16,2048]{1,0:T(8,128)(2,1)S(1)}, bf16[16,2048]{1,0:T(8,128)(2,1)S(1)}, u32[]{:S(2)}, u32[]{:S(2)}) collective-permute-start(bf16[16,2048]{1,0:T(8,128)(2,1)S(1)} %collective-permute-done.28.refs_14_), channel_id=1, source_target_pairs={{0,1},{1,0},{2,3},{3,2},{4,5},{5,4},{6,7},{7,6},{8,9},{9,8},{10,11... | collective-permute-start | bytes 196616 | tf_op jit(solution)/shard_map/ppermute | solution.py:44
  65.5 22.0 %copy-start.33 = (f32[16,2]{0,1:T(2,128)S(1)}, f32[16,2]{0,1:T(2,128)}, u32[]{:S(2)}) copy-start(f32[16,2]{0,1:T(2,128)} %param.34) | copy-start | bytes 388
  65.5 22.0 %copy-start.34 = (s32[16,2]{0,1:T(2,128)S(1)}, s32[16,2]{0,1:T(2,128)}, u32[]{:S(2)}) copy-start(s32[16,2]{0,1:T(2,128)} %param.33) | copy-start | bytes 388
  65.5 26.1 %copy-start.2 = (f32[16,2048]{1,0:T(8,128)S(1)}, f32[16,2048]{1,0:T(8,128)}, u32[]{:S(2)}) copy-start(f32[16,2048]{1,0:T(8,128)} %get-tuple-element.13) | copy-start | bytes 393220
  73.1 1.6 %collective-permute-start.39 = (bf16[2,16,2048]{2,1,0:T(8,128)(2,1)}, bf16[2,16,2048]{2,1,0:T(8,128)(2,1)S(1)}, u32[]{:S(2)}, u32[]{:S(2)}) collective-permute-start(bf16[2,16,2048]{2,1,0:T(8,128)(2,1)} %get-tuple-element.22), channel_id=1, source_target_pairs={{0,1},{1,0},{2,3},{3,2},{4,5},{5,4},{6,7},{7,6},{8,9},{9,8},{10,11... | collective-permute-start | bytes 393224 | tf_op jit(solution)/shard_map/ppermute | solution.py:44
  73.3 3.7 %collective-permute-start.30 = (bf16[2,16,2048]{2,1,0:T(8,128)(2,1)}, bf16[2,16,2048]{2,1,0:T(8,128)(2,1)S(1)}, u32[]{:S(2)}, u32[]{:S(2)}) collective-permute-start(bf16[2,16,2048]{2,1,0:T(8,128)(2,1)} %get-tuple-element.16), channel_id=1, source_target_pairs={{0,1},{1,0},{2,3},{3,2},{4,5},{5,4},{6,7},{7,6},{8,9},{9,8},{10,11... | collective-permute-start | bytes 393224 | tf_op jit(solution)/shard_map/ppermute | solution.py:44
  73.7 5.1 %collective-permute-start.33 = (bf16[2,16,2048]{2,1,0:T(8,128)(2,1)}, bf16[2,16,2048]{2,1,0:T(8,128)(2,1)S(1)}, u32[]{:S(2)}, u32[]{:S(2)}) collective-permute-start(bf16[2,16,2048]{2,1,0:T(8,128)(2,1)} %get-tuple-element.18), channel_id=1, source_target_pairs={{0,1},{1,0},{2,3},{3,2},{4,5},{5,4},{6,7},{7,6},{8,9},{9,8},{10,11... | collective-permute-start | bytes 393224 | tf_op jit(solution)/shard_map/ppermute | solution.py:44
  73.8 7.3 %collective-permute-start.36 = (bf16[2,16,2048]{2,1,0:T(8,128)(2,1)}, bf16[2,16,2048]{2,1,0:T(8,128)(2,1)S(1)}, u32[]{:S(2)}, u32[]{:S(2)}) collective-permute-start(bf16[2,16,2048]{2,1,0:T(8,128)(2,1)} %get-tuple-element.20), channel_id=1, source_target_pairs={{0,1},{1,0},{2,3},{3,2},{4,5},{5,4},{6,7},{7,6},{8,9},{9,8},{10,11... | collective-permute-start | bytes 393224 | tf_op jit(solution)/shard_map/ppermute | solution.py:44
  75.7 11.9 %collective-permute-start.40 = (bf16[16,2048]{1,0:T(8,128)(2,1)S(1)}, bf16[16,2048]{1,0:T(8,128)(2,1)S(1)}, u32[]{:S(2)}, u32[]{:S(2)}) collective-permute-start(bf16[16,2048]{1,0:T(8,128)(2,1)S(1)} %slice_bitcast_fusion), channel_id=1, source_target_pairs={{0,2},{1,3},{2,0},{3,1},{4,6},{5,7},{6,4},{7,5},{8,10},{9,11},{10,... | collective-permute-start | bytes 196616 | tf_op jit(solution)/shard_map/ppermute | solution.py:44
  78.0 4.9 %collective-permute-start.31 = (bf16[16,2048]{1,0:T(8,128)(2,1)S(1)}, bf16[16,2048]{1,0:T(8,128)(2,1)S(1)}, u32[]{:S(2)}, u32[]{:S(2)}) collective-permute-start(bf16[16,2048]{1,0:T(8,128)(2,1)S(1)} %slice_bitcast_fusion.6), channel_id=1, source_target_pairs={{0,2},{1,3},{2,0},{3,1},{4,6},{5,7},{6,4},{7,5},{8,10},{9,11},{10,... | collective-permute-start | bytes 196616 | tf_op jit(solution)/shard_map/ppermute | solution.py:44
  79.7 5.0 %collective-permute-start.34 = (bf16[16,2048]{1,0:T(8,128)(2,1)S(1)}, bf16[16,2048]{1,0:T(8,128)(2,1)S(1)}, u32[]{:S(2)}, u32[]{:S(2)}) collective-permute-start(bf16[16,2048]{1,0:T(8,128)(2,1)S(1)} %slice_bitcast_fusion.4), channel_id=1, source_target_pairs={{0,2},{1,3},{2,0},{3,1},{4,6},{5,7},{6,4},{7,5},{8,10},{9,11},{10,... | collective-permute-start | bytes 196616 | tf_op jit(solution)/shard_map/ppermute | solution.py:44
  82.1 4.3 %collective-permute-start.37 = (bf16[16,2048]{1,0:T(8,128)(2,1)S(1)}, bf16[16,2048]{1,0:T(8,128)(2,1)S(1)}, u32[]{:S(2)}, u32[]{:S(2)}) collective-permute-start(bf16[16,2048]{1,0:T(8,128)(2,1)S(1)} %slice_bitcast_fusion.2), channel_id=1, source_target_pairs={{0,2},{1,3},{2,0},{3,1},{4,6},{5,7},{6,4},{7,5},{8,10},{9,11},{10,... | collective-permute-start | bytes 196616 | tf_op jit(solution)/shard_map/ppermute | solution.py:44
  82.9 6.8 %collective-permute-start.32 = (bf16[16,2048]{1,0:T(8,128)(2,1)S(1)}, bf16[16,2048]{1,0:T(8,128)(2,1)S(1)}, u32[]{:S(2)}, u32[]{:S(2)}) collective-permute-start(bf16[16,2048]{1,0:T(8,128)(2,1)S(1)} %fusion.10), channel_id=1, source_target_pairs={{0,12},{1,13},{2,14},{3,15},{4,8},{5,9},{6,10},{7,11},{8,4},{9,5},... | collective-permute-start | bytes 196616 | tf_op jit(solution)/shard_map/ppermute | solution.py:44
  84.7 6.7 %collective-permute-start.35 = (bf16[16,2048]{1,0:T(8,128)(2,1)S(1)}, bf16[16,2048]{1,0:T(8,128)(2,1)S(1)}, u32[]{:S(2)}, u32[]{:S(2)}) collective-permute-start(bf16[16,2048]{1,0:T(8,128)(2,1)S(1)} %fusion.9), channel_id=1, source_target_pairs={{0,8},{1,9},{2,10},{3,11},{4,12},{5,13},{6,14},{7,15},{8,0},{9,1},... | collective-permute-start | bytes 196616 | tf_op jit(solution)/shard_map/ppermute | solution.py:44
  86.4 5.1 %collective-permute-start.38 = (bf16[16,2048]{1,0:T(8,128)(2,1)S(1)}, bf16[16,2048]{1,0:T(8,128)(2,1)S(1)}, u32[]{:S(2)}, u32[]{:S(2)}) collective-permute-start(bf16[16,2048]{1,0:T(8,128)(2,1)S(1)} %fusion.8), channel_id=1, source_target_pairs={{0,4},{1,5},{2,6},{3,7},{4,0},{5,1},{6,2},{7,3},{8,12},{9,13},{10,... | collective-permute-start | bytes 196616 | tf_op jit(solution)/shard_map/ppermute | solution.py:44
  (13 other events, 11.4 us)

commit v2 on v1

--- a/solution.py
+++ b/solution.py
@@ -76,7 +76,10 @@
     pieces, weights = refs[:count], refs[count : count + 3]
     rows = pieces[0].shape[0]
     width = weights[0].shape[0]
-    tokens = jnp.concatenate([piece[...] for piece in pieces], axis=0)
+    gain = refs[count + 3][...]
+    tokens = jnp.concatenate(
+        [scaled_rows(piece[...], gain).astype(bf16) for piece in pieces], axis=0
+    )
     parts = [
         lax.dot_general(tokens, w[...], NT, preferred_element_type=f32).astype(bf16)
         for w in weights
@@ -88,17 +91,18 @@
             out_ref[target, :, m * width : (m + 1) * width] = parts[m][d * rows : (d + 1) * rows]
 
 
-def project(pieces, weights):
+def project(pieces, weights, gain):
     count = len(pieces)
     rows = pieces[0].shape[0]
     width = weights[0].shape[1]
     return pl.pallas_call(
         project_kernel,
         out_shape=jax.ShapeDtypeStruct((count, rows, 3 * width), bf16),
-        in_specs=[pl.BlockSpec(memory_space=pltpu.SMEM)] + [VM] * (count + 3),
+        in_specs=[pl.BlockSpec(memory_space=pltpu.SMEM)] + [VM] * (count + 4),
         out_specs=VM,
+        compiler_params=pltpu.CompilerParams(vmem_limit_bytes=16 * 2**20),
         name="project",
-    )(lax.axis_index("ep").astype(jnp.int32).reshape(1), *pieces, *[w.T for w in weights])
+    )(lax.axis_index("ep").astype(jnp.int32).reshape(1), *pieces, *[w.T for w in weights], gain.reshape(1, -1))
 
 
 def mixer_kernel(
@@ -145,26 +149,35 @@
         vec_ref[3] = unit
         vec_ref[4] = unit * removal_ref[...]
 
-    block = ones(bf16)
     lane = lax.broadcasted_iota(jnp.int32, (values, inner), 1) % head
     row = lax.broadcasted_iota(jnp.int32, (values, inner), 0)
     diagonal = lane == row
+
+    def vector(m, b):
+        return vec_ref[m, pl.ds(step * batch + b, 1), :]
+
+    def block_sums(tables):
+        cut = [t[:, c : c + chunk] for t in tables for c in range(0, inner, chunk)]
+        sums = jnp.dot(jnp.concatenate(cut, axis=0), ones(bf16), preferred_element_type=f32)
+        pieces = [sums[k * values : (k + 1) * values] for k in range(len(cut))]
+        per = inner // chunk
+        return [
+            jnp.concatenate(pieces[k * per : (k + 1) * per], axis=1) for k in range(len(tables))
+        ]
+
+    recalled = block_sums([(state_ref[b] * vector(3, b)).astype(bf16) for b in range(batch)])
+    spread = block_sums(
+        [jnp.where(diagonal, vector(2, b), 0.0).astype(bf16) for b in range(batch)]
+    )
     for b in range(batch):
-        s = step * batch + b
-        receptance = vec_ref[0, pl.ds(s, 1), :]
-        keys = vec_ref[1, pl.ds(s, 1), :]
-        new_values = vec_ref[2, pl.ds(s, 1), :]
-        unit = vec_ref[3, pl.ds(s, 1), :]
-        removed = vec_ref[4, pl.ds(s, 1), :]
-        decay = decay_ref[pl.ds(s, 1), :]
-        state = state_ref[b]
-        recalled = head_sums((state * unit).astype(bf16), block)
-        spread = head_sums(jnp.where(diagonal, new_values, 0.0).astype(bf16), block)
-        updated = state * decay - recalled * removed + spread * keys
-        state_out_ref[b] = updated
-        read = head_sums((updated * receptance).astype(bf16), block)
-        readout_ref[pl.ds(s, 1), :] = jnp.sum(
-            jnp.where(diagonal, read, 0.0), axis=0, keepdims=True
+        decay = decay_ref[pl.ds(step * batch + b, 1), :]
+        state_out_ref[b] = (
+            state_ref[b] * decay - recalled[b] * vector(4, b) + spread[b] * vector(1, b)
+        )
+    read = block_sums([(state_out_ref[b] * vector(0, b)).astype(bf16) for b in range(batch)])
+    for b in range(batch):
+        readout_ref[pl.ds(step * batch + b, 1), :] = jnp.sum(
+            jnp.where(diagonal, read[b], 0.0), axis=0, keepdims=True
         )
 
     @pl.when(step == steps - 1)
@@ -216,6 +229,7 @@
             pltpu.VMEM(w_out.shape, bf16),
             pltpu.SemaphoreType.DMA(()),
         ],
+        compiler_params=pltpu.CompilerParams(vmem_limit_bytes=32 * 2**20),
         name="mixer",
     )(
         state_in, joined, decay, removal, group_gain.reshape(1, -1), hidden_in,
@@ -268,6 +282,7 @@
         out_specs=[VM] * (count // 2),
         scratch_shapes=[pltpu.VMEM((units, width), bf16)] * 3
         + [pltpu.VMEM((count * rows, units), bf16), pltpu.SemaphoreType.DMA((5,))],
+        compiler_params=pltpu.CompilerParams(vmem_limit_bytes=24 * 2**20),
         name="experts",
     )(*pieces, w_gate.T, w_up.T, w_down)
 
@@ -300,8 +315,8 @@
     place = lax.axis_index("ep")
     groups = lax.axis_size("ep") // EXP_SPLIT
     normed = norm_rows(hidden_in, norm_gain)
-    pieces = gather_pieces(normed)
-    spread = project(pieces, (w_recept, w_key, w_value))
+    pieces = gather_pieces(hidden_in)
+    spread = project(pieces, (w_recept, w_key, w_value), norm_gain)
     joined = lax.all_to_all(spread, "ep", split_axis=0, concat_axis=0, tiled=True)
     decay_rate = decay_of(normed, w_decay_down, w_decay_up, decay_base)
     removal = removal_of(normed, w_remove_down, w_remove_up)

time: 92.8 us -> 87.5 us (0.943)
  Pallas kernels: 23 us -> 15.7 us
  local copies, waits for them, and re-layouts: 1.83 us -> 8.82 us
  other arithmetic: 4.58 us -> 0.96 us
  waiting for transfers between devices: 20.6 us -> 19.3 us
  matrix products: 4.05 us -> 2.78 us
  starting transfers between devices: 37.2 us -> 38.4 us
    unnamed x70 -> x32, local copies, waits for them, and re-layouts: 1.8 us -> 8.8 us
    pallas_call x1, Pallas kernels: 10.5 us -> 6.87 us  [mixer(): pl.pallas_call(functools.partial(mixer_kernel, head=head), grid=(seqs //...]
    convert_element_type x7, other arithmetic: 3.81 us -> 0.19 us  [add(): return (a.astype(f32) + b.astype(f32)).astype(bf16)]
    pallas_call x1, Pallas kernels: 7.59 us -> 5.34 us  [run_experts(): pl.pallas_call(functools.partial(expert_kernel, count=count), out_shape=[...]
    ppermute x41, waiting for transfers between devices: 14.8 us -> 12.9 us  [swap(): return lax.ppermute(piece, 'ep', [(i, i ^ bits) for i in range(size)])]
    pallas_call x1, Pallas kernels: 3.22 us -> 1.93 us  [project(): pl.pallas_call(project_kernel, out_shape=jax.ShapeDtypeStruct((count, row...]
    ppermute x41, starting transfers between devices: 31.7 us -> 32.8 us  [swap(): return lax.ppermute(piece, 'ep', [(i, i ^ bits) for i in range(size)])]
  transfers between devices with their start and end apart: 42 -> 42, of which waited for: 16 -> 15; matrix products, arithmetic and copies ran while one was open for 9% -> 3% of each run, Pallas kernels for 0% -> 2%
where the time goes in v2:
time: 87.5 us; the launch traced here: 86.9 us
  starting transfers between devices  38.4 us (44%)
  waiting for transfers between devices  19.3 us (22%)
  Pallas kernels  15.7 us (18%)
  local copies, waits for them, and re-layouts  8.82 us (10%)
  matrix products  2.78 us (3%)
  other arithmetic  0.96 us (1%)
  between operations  0.91 us (1%)
    ppermute x41, starting transfers between devices, swap(): return lax.ppermute(piece, 'ep', [(i, i ^ bits) for i in range(size)])  32.8 us
    ppermute x41, waiting for transfers between devices, swap(): return lax.ppermute(piece, 'ep', [(i, i ^ bits) for i in range(size)])  12.9 us
    unnamed x32, local copies, waits for them, and re-layouts  8.8 us
    pallas_call x1, Pallas kernels, mixer(): pl.pallas_call(functools.partial(mixer_kernel, head=head), grid=(seqs //...  6.87 us
    all_to_all x1, waiting for transfers between devices, shards(): lax.all_to_all(spread, 'ep', split_axis=0, concat_axis=0, tiled=True)  6.43 us
    all_to_all x1, starting transfers between devices, shards(): lax.all_to_all(spread, 'ep', split_axis=0, concat_axis=0, tiled=True)  5.59 us
    pallas_call x1, Pallas kernels, run_experts(): pl.pallas_call(functools.partial(expert_kernel, count=count), out_shape=[...  5.34 us
    pallas_call x1, Pallas kernels, project(): pl.pallas_call(project_kernel, out_shape=jax.ShapeDtypeStruct((count, row...  1.93 us
  transfers between devices with their start and end apart: 42, of which 15 were waited for; matrix products, arithmetic and copies ran while one was open for 3% of the time, Pallas kernels for 2%

profile of v2, /device:TPU:0, one launch (start us, length us, event | category | flops | bytes accessed | tf_op | source)
XLA Modules:
  0.0 86.9 jit_solution(15741312356155441720)
XLA Ops:
  0.6 0.0 copy-start
  0.7 4.1 %collective-permute-start.7 = (bf16[16,2048]{1,0:T(8,128)(2,1)}, bf16[16,2048]{1,0:T(8,128)(2,1)S(1)}, u32[]{:S(2)}, u32[]{:S(2)}) collective-permute-start(bf16[16,2048]{1,0:T(8,128)(2,1)} %hidden_ref.1), channel_id=1, source_target_pairs={{0,8},{1,9},{2,10},{3,11},{4,12},{5,13},{6,14},{7,15},{8,0},{9,1},... | collective-permute-start | bytes 196616 | tf_op jit(solution)/shard_map/ppermute | solution.py:44
  4.8 1.3 %collective-permute-start.11 = (bf16[16,2048]{1,0:T(8,128)(2,1)}, bf16[16,2048]{1,0:T(8,128)(2,1)S(1)}, u32[]{:S(2)}, u32[]{:S(2)}) collective-permute-start(bf16[16,2048]{1,0:T(8,128)(2,1)} %hidden_ref.1), channel_id=1, source_target_pairs={{0,12},{1,13},{2,14},{3,15},{4,8},{5,9},{6,10},{7,11},{8,4},{9,5},... | collective-permute-start | bytes 196616 | tf_op jit(solution)/shard_map/ppermute | solution.py:44
  6.2 0.2 collective-permute-start.3
  6.4 1.5 %collective-permute-start.1 = (bf16[16,2048]{1,0:T(8,128)(2,1)}, bf16[16,2048]{1,0:T(8,128)(2,1)S(1)}, u32[]{:S(2)}, u32[]{:S(2)}) collective-permute-start(bf16[16,2048]{1,0:T(8,128)(2,1)} %hidden_ref.1), channel_id=1, source_target_pairs={{0,2},{1,3},{2,0},{3,1},{4,6},{5,7},{6,4},{7,5},{8,10},{9,11},{10,... | collective-permute-start | bytes 196616 | tf_op jit(solution)/shard_map/ppermute | solution.py:44
  7.9 0.8 collective-permute-done.7.refs_8_
  8.7 2.6 %collective-permute-start.9 = (bf16[16,2048]{1,0:T(8,128)(2,1)S(1)}, bf16[16,2048]{1,0:T(8,128)(2,1)S(1)}, u32[]{:S(2)}, u32[]{:S(2)}) collective-permute-start(bf16[16,2048]{1,0:T(8,128)(2,1)S(1)} %collective-permute-done.7.refs_8_), channel_id=1, source_target_pairs={{0,2},{1,3},{2,0},{3,1},{4,6},{5,7},{6,4},{7,5},{8,10},{9,11},{10,... | collective-permute-start | bytes 196616 | tf_op jit(solution)/shard_map/ppermute | solution.py:44
  11.4 1.3 %collective-permute-start.13 = (bf16[16,2048]{1,0:T(8,128)(2,1)S(1)}, bf16[16,2048]{1,0:T(8,128)(2,1)S(1)}, u32[]{:S(2)}, u32[]{:S(2)}) collective-permute-start(bf16[16,2048]{1,0:T(8,128)(2,1)S(1)} %collective-permute-done.11.refs_12_), channel_id=1, source_target_pairs={{0,2},{1,3},{2,0},{3,1},{4,6},{5,7},{6,4},{7,5},{8,10},{9,11},{10,... | collective-permute-start | bytes 196616 | tf_op jit(solution)/shard_map/ppermute | solution.py:44
  12.7 0.7 collective-permute-start.5
  13.4 0.5 collective-permute-start.4
  13.9 1.6 %norm_rows.1 = bf16[16,2048]{1,0:T(8,128)(2,1)} custom-call(bf16[16,2048]{1,0:T(8,128)(2,1)} %hidden_ref.1, f32[1,2048]{1,0:T(1,128)} %bitcast.48), custom_call_target="tpu_custom_call" | custom-call | tf_op jit(solution)/shard_map/norm_rows/pallas_call | solution.py:64
  15.5 0.1 collective-permute-start.8
  15.6 0.1 collective-permute-done.13.refs_14_
  15.7 0.4 collective-permute-start.2
  16.0 0.9 %collective-permute-done.5.refs_6_ = bf16[16,2048]{1,0:T(8,128)(2,1)S(1)} collective-permute-done((bf16[16,2048]{1,0:T(8,128)(2,1)S(1)}, bf16[16,2048]{1,0:T(8,128)(2,1)S(1)}, u32[]{:S(2)}, u32[]{:S(2)}) %collective-permute-start.5) | collective-permute-done | bytes 65568 | tf_op jit(solution)/shard_map/ppermute | solution.py:44
  17.0 0.5 collective-permute-start.14
  17.5 0.1 collective-permute-start.6
  17.6 1.3 %fusion.15.decay_ref = f32[16,1024]{1,0:T(8,128)S(1)} fusion(bf16[128,1024]{1,0:T(8,128)(2,1)} %param.27, bf16[16,2048]{1,0:T(8,128)(2,1)} %norm_rows.1, bf16[2048,128]{1,0:T(8,128)(2,1)S(1)} %copy-done, f32[1024]{0:T(1024)} %param.25), kind=kOutput, calls=%fused_computation.29 | convolution fusion | flops 12769280 | bytes 921600 | tf_op jit(solution)/shard_map/dot_general | solution.py:33
  19.0 0.8 copy-done.6
  19.8 0.9 %copy-done.8 = bf16[2048,64]{0,1:T(8,128)(2,1)S(1)} copy-done((bf16[2048,64]{0,1:T(8,128)(2,1)S(1)}, bf16[2048,64]{0,1:T(8,128)(2,1)}, u32[]{:S(2)}) %copy-start.8) | copy-done | bytes 262168
  20.8 0.9 %copy-done.9 = bf16[2048,64]{0,1:T(8,128)(2,1)S(1)} copy-done((bf16[2048,64]{0,1:T(8,128)(2,1)S(1)}, bf16[2048,64]{0,1:T(8,128)(2,1)}, u32[]{:S(2)}) %copy-start.9) | copy-done | bytes 262168
  21.7 0.9 %copy-done.10 = bf16[2048,64]{0,1:T(8,128)(2,1)S(1)} copy-done((bf16[2048,64]{0,1:T(8,128)(2,1)S(1)}, bf16[2048,64]{0,1:T(8,128)(2,1)}, u32[]{:S(2)}) %copy-start.10) | copy-done | bytes 262168
  22.7 0.7 copy-done.11
  23.4 1.9 %project.1 = bf16[16,16,192]{2,1,0:T(8,128)(2,1)} custom-call(s32[1]{0:T(128)} %bitcast.place_ref, bf16[16,2048]{1,0:T(8,128)(2,1)S(1)} %copy-done.6, bf16[16,2048]{1,0:T(8,128)(2,1)S(1)} %collective-permute-done.refs_1_, bf16[16,2048]{1,0:T(8,128)(2,1)S(1)} %collective-permute-done.1.refs_2_, bf16[16,2048]{1,0:T(8,128)(2,1)S(1)} %collective-permute-done.2.refs_3_, ...), custom_call_target="tpu_custom_call" | custom-call | tf_op jit(solution)/shard_map/project/pallas_call | solution.py:98
  25.3 5.6 %all-to-all-start = ((bf16[16,16,192]{2,1,0:T(8,128)(2,1)}), bf16[16,16,192]{2,1,0:T(8,128)(2,1)S(1)}, u32[]{:S(2)}, u32[]{:S(2)}) async-start(bf16[16,16,192]{2,1,0:T(8,128)(2,1)} %project.1), calls=%async_computation | async-start | bytes 262144 | tf_op jit(solution)/shard_map/all_to_all | solution.py:320
  30.9 1.5 %fusion.2.removal_ref = f32[16,1024]{1,0:T(8,128)S(1)} fusion(bf16[128,1024]{1,0:T(8,128)(2,1)} %param.29, bf16[16,2048]{1,0:T(8,128)(2,1)} %norm_rows.1, bf16[2048,128]{1,0:T(8,128)(2,1)} %param.28), kind=kOutput, calls=%fused_computation.3 | convolution fusion | flops 12634112 | bytes 917504 | tf_op jit(solution)/shard_map/dot_general | solution.py:39
  32.4 6.4 %all-to-all-done.joined_ref = bf16[16,16,192]{2,1,0:T(8,128)(2,1)S(1)} async-done(((bf16[16,16,192]{2,1,0:T(8,128)(2,1)}), bf16[16,16,192]{2,1,0:T(8,128)(2,1)S(1)}, u32[]{:S(2)}, u32[]{:S(2)}) %all-to-all-start) | async-done | bytes 98336 | tf_op jit(solution)/shard_map/all_to_all | solution.py:320
  38.8 2.2 %copy-done.1 = f32[16,64,1024]{2,1,0:T(8,128)S(1)} copy-done((f32[16,64,1024]{2,1,0:T(8,128)S(1)}, f32[16,64,1024]{2,1,0:T(8,128)}, u32[]{:S(2)}) %copy-start.1) | copy-done | bytes 4194328
  41.0 2.2 %copy-done.2 = bf16[1024,2048]{1,0:T(8,128)(2,1)S(1)} copy-done((bf16[1024,2048]{1,0:T(8,128)(2,1)S(1)}, bf16[1024,2048]{1,0:T(8,128)(2,1)}, u32[]{:S(2)}) %copy-start.2) | copy-done | bytes 4194328
  43.2 6.9 %mixer.1 = (f32[16,64,1024]{2,1,0:T(8,128)}, f32[16,2048]{1,0:T(8,128)S(1)}, bf16[16,2048]{1,0:T(8,128)(2,1)S(1)}) custom-call(f32[16,64,1024]{2,1,0:T(8,128)S(1)} %copy-done.1, bf16[16,16,192]{2,1,0:T(8,128)(2,1)S(1)} %all-to-all-done.joined_ref, f32[16,1024]{1,0:T(8,128)S(1)} %fusion.15.decay_ref, f32[16,1024]{1,0:T(8,128)S(1)} %fusion.2.removal_ref, ...), custom_call_target="tpu_custom_call" | custom-call | tf_op jit(solution)/shard_map/mixer/pallas_call | solution.py:207
  50.1 0.1 collective-permute-start.18
  50.1 1.2 %collective-permute-start.22 = (bf16[16,2048]{1,0:T(8,128)(2,1)S(1)}, bf16[16,2048]{1,0:T(8,128)(2,1)S(1)}, u32[]{:S(2)}, u32[]{:S(2)}) collective-permute-start(bf16[16,2048]{1,0:T(8,128)(2,1)S(1)} %get-tuple-element.14.refs_0_), channel_id=1, source_target_pairs={{0,8},{1,9},{2,10},{3,11},{4,12},{5,13},{6,14},{7,15},{8,0},{9,1},... | collective-permute-start | bytes 196616 | tf_op jit(solution)/shard_map/ppermute | solution.py:44
  51.4 3.1 %collective-permute-start.26 = (bf16[16,2048]{1,0:T(8,128)(2,1)S(1)}, bf16[16,2048]{1,0:T(8,128)(2,1)S(1)}, u32[]{:S(2)}, u32[]{:S(2)}) collective-permute-start(bf16[16,2048]{1,0:T(8,128)(2,1)S(1)} %get-tuple-element.14.refs_0_), channel_id=1, source_target_pairs={{0,12},{1,13},{2,14},{3,15},{4,8},{5,9},{6,10},{7,11},{8,4},{9,5},... | collective-permute-start | bytes 196616 | tf_op jit(solution)/shard_map/ppermute | solution.py:44
  54.5 0.3 collective-permute-done.18.refs_4_
  54.8 1.8 %collective-permute-start.20 = (bf16[16,2048]{1,0:T(8,128)(2,1)S(1)}, bf16[16,2048]{1,0:T(8,128)(2,1)S(1)}, u32[]{:S(2)}, u32[]{:S(2)}) collective-permute-start(bf16[16,2048]{1,0:T(8,128)(2,1)S(1)} %collective-permute-done.18.refs_4_), channel_id=1, source_target_pairs={{0,2},{1,3},{2,0},{3,1},{4,6},{5,7},{6,4},{7,5},{8,10},{9,11},{10,... | collective-permute-start | bytes 196616 | tf_op jit(solution)/shard_map/ppermute | solution.py:44
  56.5 1.8 %collective-permute-done.22.refs_8_ = bf16[16,2048]{1,0:T(8,128)(2,1)S(1)} collective-permute-done((bf16[16,2048]{1,0:T(8,128)(2,1)S(1)}, bf16[16,2048]{1,0:T(8,128)(2,1)S(1)}, u32[]{:S(2)}, u32[]{:S(2)}) %collective-permute-start.22) | collective-permute-done | bytes 65568 | tf_op jit(solution)/shard_map/ppermute | solution.py:44
  58.3 0.7 collective-permute-start.24
  59.0 1.3 %collective-permute-start.28 = (bf16[16,2048]{1,0:T(8,128)(2,1)S(1)}, bf16[16,2048]{1,0:T(8,128)(2,1)S(1)}, u32[]{:S(2)}, u32[]{:S(2)}) collective-permute-start(bf16[16,2048]{1,0:T(8,128)(2,1)S(1)} %collective-permute-done.26.refs_12_), channel_id=1, source_target_pairs={{0,2},{1,3},{2,0},{3,1},{4,6},{5,7},{6,4},{7,5},{8,10},{9,11},{10,... | collective-permute-start | bytes 196616 | tf_op jit(solution)/shard_map/ppermute | solution.py:44
  60.4 0.5 collective-permute-start.23
  60.9 0.1 collective-permute-start.27
  60.9 1.6 %collective-permute-done.24.refs_10_ = bf16[16,2048]{1,0:T(8,128)(2,1)S(1)} collective-permute-done((bf16[16,2048]{1,0:T(8,128)(2,1)S(1)}, bf16[16,2048]{1,0:T(8,128)(2,1)S(1)}, u32[]{:S(2)}, u32[]{:S(2)}) %collective-permute-start.24) | collective-permute-done | bytes 65568 | tf_op jit(solution)/shard_map/ppermute | solution.py:44
  62.6 0.7 collective-permute-done.28.refs_14_
  63.3 0.5 collective-permute-start.25
  63.8 0.1 collective-permute-start.29
  63.9 0.7 collective-permute-done.21.refs_7_
  64.6 0.2 collective-permute-done.25.refs_11_
  64.7 0.4 collective-permute-done.29.refs_15_
  65.1 5.3 %experts.1 = (bf16[2,16,2048]{2,1,0:T(8,128)(2,1)S(1)}, bf16[2,16,2048]{2,1,0:T(8,128)(2,1)S(1)}, bf16[2,16,2048]{2,1,0:T(8,128)(2,1)S(1)}, bf16[2,16,2048]{2,1,...) custom-call(bf16[16,2048]{1,0:T(8,128)(2,1)S(1)} %get-tuple-element., ...), custom_call_target="tpu_custom_call" | custom-call | tf_op jit(solution)/shard_map/experts/pallas_call | solution.py:278
  70.5 0.2 collective-permute-start.39
  70.7 0.4 collective-permute-start.30
  71.0 0.2 collective-permute-start.33
  71.2 0.4 collective-permute-start.36
  71.5 0.3 collective-permute-done.39
  71.9 1.4 %collective-permute-start.40 = (bf16[16,2048]{1,0:T(8,128)(2,1)S(1)}, bf16[16,2048]{1,0:T(8,128)(2,1)S(1)}, u32[]{:S(2)}, u32[]{:S(2)}) collective-permute-start(bf16[16,2048]{1,0:T(8,128)(2,1)S(1)} %slice_bitcast_fusion), channel_id=1, source_target_pairs={{0,2},{1,3},{2,0},{3,1},{4,6},{5,7},{6,4},{7,5},{8,10},{9,11},{10,... | collective-permute-start | bytes 196616 | tf_op jit(solution)/shard_map/ppermute | solution.py:44
  73.3 0.8 collective-permute-start.31
  74.2 1.4 %collective-permute-start.34 = (bf16[16,2048]{1,0:T(8,128)(2,1)S(1)}, bf16[16,2048]{1,0:T(8,128)(2,1)S(1)}, u32[]{:S(2)}, u32[]{:S(2)}) collective-permute-start(bf16[16,2048]{1,0:T(8,128)(2,1)S(1)} %slice_bitcast_fusion.4), channel_id=1, source_target_pairs={{0,2},{1,3},{2,0},{3,1},{4,6},{5,7},{6,4},{7,5},{8,10},{9,11},{10,... | collective-permute-start | bytes 196616 | tf_op jit(solution)/shard_map/ppermute | solution.py:44
  75.6 0.8 collective-permute-start.37
  76.4 2.0 %collective-permute-done.31 = bf16[16,2048]{1,0:T(8,128)(2,1)S(1)} collective-permute-done((bf16[16,2048]{1,0:T(8,128)(2,1)S(1)}, bf16[16,2048]{1,0:T(8,128)(2,1)S(1)}, u32[]{:S(2)}, u32[]{:S(2)}) %collective-permute-start.31) | collective-permute-done | bytes 65568 | tf_op jit(solution)/shard_map/ppermute | solution.py:44
  78.4 1.8 %collective-permute-start.32 = (bf16[16,2048]{1,0:T(8,128)(2,1)S(1)}, bf16[16,2048]{1,0:T(8,128)(2,1)S(1)}, u32[]{:S(2)}, u32[]{:S(2)}) collective-permute-start(bf16[16,2048]{1,0:T(8,128)(2,1)S(1)} %fusion.10), channel_id=1, source_target_pairs={{0,12},{1,13},{2,14},{3,15},{4,8},{5,9},{6,10},{7,11},{8,4},{9,5},... | collective-permute-start | bytes 196616 | tf_op jit(solution)/shard_map/ppermute | solution.py:44
  80.2 0.5 collective-permute-start.35
  80.7 2.3 %collective-permute-start.38 = (bf16[16,2048]{1,0:T(8,128)(2,1)S(1)}, bf16[16,2048]{1,0:T(8,128)(2,1)S(1)}, u32[]{:S(2)}, u32[]{:S(2)}) collective-permute-start(bf16[16,2048]{1,0:T(8,128)(2,1)S(1)} %fusion.8), channel_id=1, source_target_pairs={{0,4},{1,5},{2,6},{3,7},{4,0},{5,1},{6,2},{7,3},{8,12},{9,13},{10,... | collective-permute-start | bytes 196616 | tf_op jit(solution)/shard_map/ppermute | solution.py:44
  83.1 1.7 %collective-permute-done.32 = bf16[16,2048]{1,0:T(8,128)(2,1)S(1)} collective-permute-done((bf16[16,2048]{1,0:T(8,128)(2,1)S(1)}, bf16[16,2048]{1,0:T(8,128)(2,1)S(1)}, u32[]{:S(2)}, u32[]{:S(2)}) %collective-permute-start.32) | collective-permute-done | bytes 65568 | tf_op jit(solution)/shard_map/ppermute | solution.py:44
  84.8 1.4 %collective-permute-done.35 = bf16[16,2048]{1,0:T(8,128)(2,1)S(1)} collective-permute-done((bf16[16,2048]{1,0:T(8,128)(2,1)S(1)}, bf16[16,2048]{1,0:T(8,128)(2,1)S(1)}, u32[]{:S(2)}, u32[]{:S(2)}) %collective-permute-start.35) | collective-permute-done | bytes 65568 | tf_op jit(solution)/shard_map/ppermute | solution.py:44
  86.2 0.7 add_convert_fusion.4
  (71 shorter events, 0.4 us)
Async XLA Ops:
  0.6 16.9 %copy-start = (bf16[2048,128]{1,0:T(8,128)(2,1)S(1)}, bf16[2048,128]{1,0:T(8,128)(2,1)}, u32[]{:S(2)}) copy-start(bf16[2048,128]{1,0:T(8,128)(2,1)} %param.26) | copy-start | bytes 1572868
  0.6 38.1 %copy-start.7 = (bf16[16,2048]{1,0:T(8,128)(2,1)S(1)}, bf16[16,2048]{1,0:T(8,128)(2,1)}, u32[]{:S(2)}) copy-start(bf16[16,2048]{1,0:T(8,128)(2,1)} %hidden_ref.1) | copy-start | bytes 196612
  0.7 38.1 %copy-start.13 = (f32[1024]{0:T(1024)S(1)}, f32[1024]{0:T(1024)}, u32[]{:S(2)}) copy-start(f32[1024]{0:T(1024)} %param.30) | copy-start | bytes 12292
  0.7 38.1 %copy-start.12 = (f32[2048]{0:T(1024)S(1)}, f32[2048]{0:T(1024)}, u32[]{:S(2)}) copy-start(f32[2048]{0:T(1024)} %param.32) | copy-start | bytes 24580
  0.7 8.1 %collective-permute-start.7 = (bf16[16,2048]{1,0:T(8,128)(2,1)}, bf16[16,2048]{1,0:T(8,128)(2,1)S(1)}, u32[]{:S(2)}, u32[]{:S(2)}) collective-permute-start(bf16[16,2048]{1,0:T(8,128)(2,1)} %hidden_ref.1), channel_id=1, source_target_pairs={{0,8},{1,9},{2,10},{3,11},{4,12},{5,13},{6,14},{7,15},{8,0},{9,1},... | collective-permute-start | bytes 196616 | tf_op jit(solution)/shard_map/ppermute | solution.py:44
  4.8 6.6 %collective-permute-start.11 = (bf16[16,2048]{1,0:T(8,128)(2,1)}, bf16[16,2048]{1,0:T(8,128)(2,1)S(1)}, u32[]{:S(2)}, u32[]{:S(2)}) collective-permute-start(bf16[16,2048]{1,0:T(8,128)(2,1)} %hidden_ref.1), channel_id=1, source_target_pairs={{0,12},{1,13},{2,14},{3,15},{4,8},{5,9},{6,10},{7,11},{8,4},{9,5},... | collective-permute-start | bytes 196616 | tf_op jit(solution)/shard_map/ppermute | solution.py:44
  6.2 6.6 %collective-permute-start.3 = (bf16[16,2048]{1,0:T(8,128)(2,1)}, bf16[16,2048]{1,0:T(8,128)(2,1)S(1)}, u32[]{:S(2)}, u32[]{:S(2)}) collective-permute-start(bf16[16,2048]{1,0:T(8,128)(2,1)} %hidden_ref.1), channel_id=1, source_target_pairs={{0,4},{1,5},{2,6},{3,7},{4,0},{5,1},{6,2},{7,3},{8,12},{9,13},{10,... | collective-permute-start | bytes 196616 | tf_op jit(solution)/shard_map/ppermute | solution.py:44
  6.4 7.0 %collective-permute-start.1 = (bf16[16,2048]{1,0:T(8,128)(2,1)}, bf16[16,2048]{1,0:T(8,128)(2,1)S(1)}, u32[]{:S(2)}, u32[]{:S(2)}) collective-permute-start(bf16[16,2048]{1,0:T(8,128)(2,1)} %hidden_ref.1), channel_id=1, source_target_pairs={{0,2},{1,3},{2,0},{3,1},{4,6},{5,7},{6,4},{7,5},{8,10},{9,11},{10,... | collective-permute-start | bytes 196616 | tf_op jit(solution)/shard_map/ppermute | solution.py:44
  7.9 5.5 %collective-permute-start = (bf16[16,2048]{1,0:T(8,128)(2,1)}, bf16[16,2048]{1,0:T(8,128)(2,1)S(1)}, u32[]{:S(2)}, u32[]{:S(2)}) collective-permute-start(bf16[16,2048]{1,0:T(8,128)(2,1)} %hidden_ref.1), channel_id=1, source_target_pairs={{0,1},{1,0},{2,3},{3,2},{4,5},{5,4},{6,7},{7,6},{8,9},{9,8},{10,11... | collective-permute-start | bytes 196616 | tf_op jit(solution)/shard_map/ppermute | solution.py:44
  8.7 6.8 %collective-permute-start.9 = (bf16[16,2048]{1,0:T(8,128)(2,1)S(1)}, bf16[16,2048]{1,0:T(8,128)(2,1)S(1)}, u32[]{:S(2)}, u32[]{:S(2)}) collective-permute-start(bf16[16,2048]{1,0:T(8,128)(2,1)S(1)} %collective-permute-done.7.refs_8_), channel_id=1, source_target_pairs={{0,2},{1,3},{2,0},{3,1},{4,6},{5,7},{6,4},{7,5},{8,10},{9,11},{10,... | collective-permute-start | bytes 196616 | tf_op jit(solution)/shard_map/ppermute | solution.py:44
  11.4 4.3 %collective-permute-start.13 = (bf16[16,2048]{1,0:T(8,128)(2,1)S(1)}, bf16[16,2048]{1,0:T(8,128)(2,1)S(1)}, u32[]{:S(2)}, u32[]{:S(2)}) collective-permute-start(bf16[16,2048]{1,0:T(8,128)(2,1)S(1)} %collective-permute-done.11.refs_12_), channel_id=1, source_target_pairs={{0,2},{1,3},{2,0},{3,1},{4,6},{5,7},{6,4},{7,5},{8,10},{9,11},{10,... | collective-permute-start | bytes 196616 | tf_op jit(solution)/shard_map/ppermute | solution.py:44
  12.7 4.3 %collective-permute-start.5 = (bf16[16,2048]{1,0:T(8,128)(2,1)S(1)}, bf16[16,2048]{1,0:T(8,128)(2,1)S(1)}, u32[]{:S(2)}, u32[]{:S(2)}) collective-permute-start(bf16[16,2048]{1,0:T(8,128)(2,1)S(1)} %collective-permute-done.3.refs_4_), channel_id=1, source_target_pairs={{0,2},{1,3},{2,0},{3,1},{4,6},{5,7},{6,4},{7,5},{8,10},{9,11},{10,... | collective-permute-start | bytes 196616 | tf_op jit(solution)/shard_map/ppermute | solution.py:44
  13.4 3.6 %collective-permute-start.12 = (bf16[16,2048]{1,0:T(8,128)(2,1)S(1)}, bf16[16,2048]{1,0:T(8,128)(2,1)S(1)}, u32[]{:S(2)}, u32[]{:S(2)}) collective-permute-start(bf16[16,2048]{1,0:T(8,128)(2,1)S(1)} %collective-permute-done.11.refs_12_), channel_id=1, source_target_pairs={{0,1},{1,0},{2,3},{3,2},{4,5},{5,4},{6,7},{7,6},{8,9},{9,8},{10,11... | collective-permute-start | bytes 196616 | tf_op jit(solution)/shard_map/ppermute | solution.py:44
  13.4 4.1 %collective-permute-start.4 = (bf16[16,2048]{1,0:T(8,128)(2,1)S(1)}, bf16[16,2048]{1,0:T(8,128)(2,1)S(1)}, u32[]{:S(2)}, u32[]{:S(2)}) collective-permute-start(bf16[16,2048]{1,0:T(8,128)(2,1)S(1)} %collective-permute-done.3.refs_4_), channel_id=1, source_target_pairs={{0,1},{1,0},{2,3},{3,2},{4,5},{5,4},{6,7},{7,6},{8,9},{9,8},{10,11... | collective-permute-start | bytes 196616 | tf_op jit(solution)/shard_map/ppermute | solution.py:44
  15.5 3.4 %collective-permute-start.8 = (bf16[16,2048]{1,0:T(8,128)(2,1)S(1)}, bf16[16,2048]{1,0:T(8,128)(2,1)S(1)}, u32[]{:S(2)}, u32[]{:S(2)}) collective-permute-start(bf16[16,2048]{1,0:T(8,128)(2,1)S(1)} %collective-permute-done.7.refs_8_), channel_id=1, source_target_pairs={{0,1},{1,0},{2,3},{3,2},{4,5},{5,4},{6,7},{7,6},{8,9},{9,8},{10,11... | collective-permute-start | bytes 196616 | tf_op jit(solution)/shard_map/ppermute | solution.py:44
  15.7 3.3 %collective-permute-start.2 = (bf16[16,2048]{1,0:T(8,128)(2,1)S(1)}, bf16[16,2048]{1,0:T(8,128)(2,1)S(1)}, u32[]{:S(2)}, u32[]{:S(2)}) collective-permute-start(bf16[16,2048]{1,0:T(8,128)(2,1)S(1)} %collective-permute-done.1.refs_2_), channel_id=1, source_target_pairs={{0,1},{1,0},{2,3},{3,2},{4,5},{5,4},{6,7},{7,6},{8,9},{9,8},{10,11... | collective-permute-start | bytes 196616 | tf_op jit(solution)/shard_map/ppermute | solution.py:44
  17.0 2.0 %collective-permute-start.10 = (bf16[16,2048]{1,0:T(8,128)(2,1)S(1)}, bf16[16,2048]{1,0:T(8,128)(2,1)S(1)}, u32[]{:S(2)}, u32[]{:S(2)}) collective-permute-start(bf16[16,2048]{1,0:T(8,128)(2,1)S(1)} %collective-permute-done.9.refs_10_), channel_id=1, source_target_pairs={{0,1},{1,0},{2,3},{3,2},{4,5},{5,4},{6,7},{7,6},{8,9},{9,8},{10,11... | collective-permute-start | bytes 196616 | tf_op jit(solution)/shard_map/ppermute | solution.py:44
  17.0 2.0 %collective-permute-start.14 = (bf16[16,2048]{1,0:T(8,128)(2,1)S(1)}, bf16[16,2048]{1,0:T(8,128)(2,1)S(1)}, u32[]{:S(2)}, u32[]{:S(2)}) collective-permute-start(bf16[16,2048]{1,0:T(8,128)(2,1)S(1)} %collective-permute-done.13.refs_14_), channel_id=1, source_target_pairs={{0,1},{1,0},{2,3},{3,2},{4,5},{5,4},{6,7},{7,6},{8,9},{9,8},{10,11... | collective-permute-start | bytes 196616 | tf_op jit(solution)/shard_map/ppermute | solution.py:44
  17.5 1.5 %collective-permute-start.6 = (bf16[16,2048]{1,0:T(8,128)(2,1)S(1)}, bf16[16,2048]{1,0:T(8,128)(2,1)S(1)}, u32[]{:S(2)}, u32[]{:S(2)}) collective-permute-start(bf16[16,2048]{1,0:T(8,128)(2,1)S(1)} %collective-permute-done.5.refs_6_), channel_id=1, source_target_pairs={{0,1},{1,0},{2,3},{3,2},{4,5},{5,4},{6,7},{7,6},{8,9},{9,8},{10,11... | collective-permute-start | bytes 196616 | tf_op jit(solution)/shard_map/ppermute | solution.py:44
  19.0 0.8 copy-start.6
  19.8 0.9 %copy-start.8 = (bf16[2048,64]{0,1:T(8,128)(2,1)S(1)}, bf16[2048,64]{0,1:T(8,128)(2,1)}, u32[]{:S(2)}) copy-start(bf16[2048,64]{0,1:T(8,128)(2,1)} %param.22) | copy-start | bytes 786436
  20.8 0.9 %copy-start.9 = (bf16[2048,64]{0,1:T(8,128)(2,1)S(1)}, bf16[2048,64]{0,1:T(8,128)(2,1)}, u32[]{:S(2)}) copy-start(bf16[2048,64]{0,1:T(8,128)(2,1)} %param.23) | copy-start | bytes 786436
  21.7 0.9 %copy-start.10 = (bf16[2048,64]{0,1:T(8,128)(2,1)S(1)}, bf16[2048,64]{0,1:T(8,128)(2,1)}, u32[]{:S(2)}) copy-start(bf16[2048,64]{0,1:T(8,128)(2,1)} %param.24) | copy-start | bytes 786436
  22.7 0.7 copy-start.11
  25.3 13.5 %all-to-all-start = ((bf16[16,16,192]{2,1,0:T(8,128)(2,1)}), bf16[16,16,192]{2,1,0:T(8,128)(2,1)S(1)}, u32[]{:S(2)}, u32[]{:S(2)}) async-start(bf16[16,16,192]{2,1,0:T(8,128)(2,1)} %project.1), calls=%async_computation | async-start | bytes 262144 | tf_op jit(solution)/shard_map/all_to_all | solution.py:320
  38.8 2.2 %copy-start.1 = (f32[16,64,1024]{2,1,0:T(8,128)S(1)}, f32[16,64,1024]{2,1,0:T(8,128)}, u32[]{:S(2)}) copy-start(f32[16,64,1024]{2,1,0:T(8,128)} %state_ref.1) | copy-start | bytes 12582916
  41.0 2.2 %copy-start.2 = (bf16[1024,2048]{1,0:T(8,128)(2,1)S(1)}, bf16[1024,2048]{1,0:T(8,128)(2,1)}, u32[]{:S(2)}) copy-start(bf16[1024,2048]{1,0:T(8,128)(2,1)} %w_out_ref.1) | copy-start | bytes 12582916
  43.2 21.9 %copy-start.3 = (bf16[2048,704]{0,1:T(8,128)(2,1)S(1)}, bf16[2048,704]{0,1:T(8,128)(2,1)}, u32[]{:S(2)}) copy-start(bf16[2048,704]{0,1:T(8,128)(2,1)} %param.35) | copy-start | bytes 8650756
  43.2 21.9 %copy-start.4 = (bf16[2048,704]{0,1:T(8,128)(2,1)S(1)}, bf16[2048,704]{0,1:T(8,128)(2,1)}, u32[]{:S(2)}) copy-start(bf16[2048,704]{0,1:T(8,128)(2,1)} %param.36) | copy-start | bytes 8650756
  43.2 21.9 %copy-start.5 = (bf16[704,2048]{1,0:T(8,128)(2,1)S(1)}, bf16[704,2048]{1,0:T(8,128)(2,1)}, u32[]{:S(2)}) copy-start(bf16[704,2048]{1,0:T(8,128)(2,1)} %refs_18_.1) | copy-start | bytes 8650756
  50.1 4.7 %collective-permute-start.18 = (bf16[16,2048]{1,0:T(8,128)(2,1)S(1)}, bf16[16,2048]{1,0:T(8,128)(2,1)S(1)}, u32[]{:S(2)}, u32[]{:S(2)}) collective-permute-start(bf16[16,2048]{1,0:T(8,128)(2,1)S(1)} %get-tuple-element.14.refs_0_), channel_id=1, source_target_pairs={{0,4},{1,5},{2,6},{3,7},{4,0},{5,1},{6,2},{7,3},{8,12},{9,13},{10,... | collective-permute-start | bytes 196616 | tf_op jit(solution)/shard_map/ppermute | solution.py:44
  50.1 8.2 %collective-permute-start.22 = (bf16[16,2048]{1,0:T(8,128)(2,1)S(1)}, bf16[16,2048]{1,0:T(8,128)(2,1)S(1)}, u32[]{:S(2)}, u32[]{:S(2)}) collective-permute-start(bf16[16,2048]{1,0:T(8,128)(2,1)S(1)} %get-tuple-element.14.refs_0_), channel_id=1, source_target_pairs={{0,8},{1,9},{2,10},{3,11},{4,12},{5,13},{6,14},{7,15},{8,0},{9,1},... | collective-permute-start | bytes 196616 | tf_op jit(solution)/shard_map/ppermute | solution.py:44
  51.4 7.7 %collective-permute-start.26 = (bf16[16,2048]{1,0:T(8,128)(2,1)S(1)}, bf16[16,2048]{1,0:T(8,128)(2,1)S(1)}, u32[]{:S(2)}, u32[]{:S(2)}) collective-permute-start(bf16[16,2048]{1,0:T(8,128)(2,1)S(1)} %get-tuple-element.14.refs_0_), channel_id=1, source_target_pairs={{0,12},{1,13},{2,14},{3,15},{4,8},{5,9},{6,10},{7,11},{8,4},{9,5},... | collective-permute-start | bytes 196616 | tf_op jit(solution)/shard_map/ppermute | solution.py:44
  54.5 5.8 %collective-permute-start.16 = (bf16[16,2048]{1,0:T(8,128)(2,1)S(1)}, bf16[16,2048]{1,0:T(8,128)(2,1)S(1)}, u32[]{:S(2)}, u32[]{:S(2)}) collective-permute-start(bf16[16,2048]{1,0:T(8,128)(2,1)S(1)} %get-tuple-element.14.refs_0_), channel_id=1, source_target_pairs={{0,2},{1,3},{2,0},{3,1},{4,6},{5,7},{6,4},{7,5},{8,10},{9,11},{10,... | collective-permute-start | bytes 196616 | tf_op jit(solution)/shard_map/ppermute | solution.py:44
  54.5 5.8 %collective-permute-start.15 = (bf16[16,2048]{1,0:T(8,128)(2,1)S(1)}, bf16[16,2048]{1,0:T(8,128)(2,1)S(1)}, u32[]{:S(2)}, u32[]{:S(2)}) collective-permute-start(bf16[16,2048]{1,0:T(8,128)(2,1)S(1)} %get-tuple-element.14.refs_0_), channel_id=1, source_target_pairs={{0,1},{1,0},{2,3},{3,2},{4,5},{5,4},{6,7},{7,6},{8,9},{9,8},{10,11... | collective-permute-start | bytes 196616 | tf_op jit(solution)/shard_map/ppermute | solution.py:44
  54.8 6.1 %collective-permute-start.20 = (bf16[16,2048]{1,0:T(8,128)(2,1)S(1)}, bf16[16,2048]{1,0:T(8,128)(2,1)S(1)}, u32[]{:S(2)}, u32[]{:S(2)}) collective-permute-start(bf16[16,2048]{1,0:T(8,128)(2,1)S(1)} %collective-permute-done.18.refs_4_), channel_id=1, source_target_pairs={{0,2},{1,3},{2,0},{3,1},{4,6},{5,7},{6,4},{7,5},{8,10},{9,11},{10,... | collective-permute-start | bytes 196616 | tf_op jit(solution)/shard_map/ppermute | solution.py:44
  58.3 4.3 %collective-permute-start.24 = (bf16[16,2048]{1,0:T(8,128)(2,1)S(1)}, bf16[16,2048]{1,0:T(8,128)(2,1)S(1)}, u32[]{:S(2)}, u32[]{:S(2)}) collective-permute-start(bf16[16,2048]{1,0:T(8,128)(2,1)S(1)} %collective-permute-done.22.refs_8_), channel_id=1, source_target_pairs={{0,2},{1,3},{2,0},{3,1},{4,6},{5,7},{6,4},{7,5},{8,10},{9,11},{10,... | collective-permute-start | bytes 196616 | tf_op jit(solution)/shard_map/ppermute | solution.py:44
  59.0 4.3 %collective-permute-start.28 = (bf16[16,2048]{1,0:T(8,128)(2,1)S(1)}, bf16[16,2048]{1,0:T(8,128)(2,1)S(1)}, u32[]{:S(2)}, u32[]{:S(2)}) collective-permute-start(bf16[16,2048]{1,0:T(8,128)(2,1)S(1)} %collective-permute-done.26.refs_12_), channel_id=1, source_target_pairs={{0,2},{1,3},{2,0},{3,1},{4,6},{5,7},{6,4},{7,5},{8,10},{9,11},{10,... | collective-permute-start | bytes 196616 | tf_op jit(solution)/shard_map/ppermute | solution.py:44
  60.3 3.0 %collective-permute-start.19 = (bf16[16,2048]{1,0:T(8,128)(2,1)S(1)}, bf16[16,2048]{1,0:T(8,128)(2,1)S(1)}, u32[]{:S(2)}, u32[]{:S(2)}) collective-permute-start(bf16[16,2048]{1,0:T(8,128)(2,1)S(1)} %collective-permute-done.18.refs_4_), channel_id=1, source_target_pairs={{0,1},{1,0},{2,3},{3,2},{4,5},{5,4},{6,7},{7,6},{8,9},{9,8},{10,11... | collective-permute-start | bytes 196616 | tf_op jit(solution)/shard_map/ppermute | solution.py:44
  60.4 3.5 %collective-permute-start.23 = (bf16[16,2048]{1,0:T(8,128)(2,1)S(1)}, bf16[16,2048]{1,0:T(8,128)(2,1)S(1)}, u32[]{:S(2)}, u32[]{:S(2)}) collective-permute-start(bf16[16,2048]{1,0:T(8,128)(2,1)S(1)} %collective-permute-done.22.refs_8_), channel_id=1, source_target_pairs={{0,1},{1,0},{2,3},{3,2},{4,5},{5,4},{6,7},{7,6},{8,9},{9,8},{10,11... | collective-permute-start | bytes 196616 | tf_op jit(solution)/shard_map/ppermute | solution.py:44
  60.9 3.0 %collective-permute-start.27 = (bf16[16,2048]{1,0:T(8,128)(2,1)S(1)}, bf16[16,2048]{1,0:T(8,128)(2,1)S(1)}, u32[]{:S(2)}, u32[]{:S(2)}) collective-permute-start(bf16[16,2048]{1,0:T(8,128)(2,1)S(1)} %collective-permute-done.26.refs_12_), channel_id=1, source_target_pairs={{0,1},{1,0},{2,3},{3,2},{4,5},{5,4},{6,7},{7,6},{8,9},{9,8},{10,11... | collective-permute-start | bytes 196616 | tf_op jit(solution)/shard_map/ppermute | solution.py:44
  62.6 1.3 %collective-permute-start.17 = (bf16[16,2048]{1,0:T(8,128)(2,1)S(1)}, bf16[16,2048]{1,0:T(8,128)(2,1)S(1)}, u32[]{:S(2)}, u32[]{:S(2)}) collective-permute-start(bf16[16,2048]{1,0:T(8,128)(2,1)S(1)} %collective-permute-done.16.refs_2_), channel_id=1, source_target_pairs={{0,1},{1,0},{2,3},{3,2},{4,5},{5,4},{6,7},{7,6},{8,9},{9,8},{10,11... | collective-permute-start | bytes 196616 | tf_op jit(solution)/shard_map/ppermute | solution.py:44
  63.3 1.3 %collective-permute-start.21 = (bf16[16,2048]{1,0:T(8,128)(2,1)S(1)}, bf16[16,2048]{1,0:T(8,128)(2,1)S(1)}, u32[]{:S(2)}, u32[]{:S(2)}) collective-permute-start(bf16[16,2048]{1,0:T(8,128)(2,1)S(1)} %collective-permute-done.20.refs_6_), channel_id=1, source_target_pairs={{0,1},{1,0},{2,3},{3,2},{4,5},{5,4},{6,7},{7,6},{8,9},{9,8},{10,11... | collective-permute-start | bytes 196616 | tf_op jit(solution)/shard_map/ppermute | solution.py:44
  63.3 1.4 %collective-permute-start.25 = (bf16[16,2048]{1,0:T(8,128)(2,1)S(1)}, bf16[16,2048]{1,0:T(8,128)(2,1)S(1)}, u32[]{:S(2)}, u32[]{:S(2)}) collective-permute-start(bf16[16,2048]{1,0:T(8,128)(2,1)S(1)} %collective-permute-done.24.refs_10_), channel_id=1, source_target_pairs={{0,1},{1,0},{2,3},{3,2},{4,5},{5,4},{6,7},{7,6},{8,9},{9,8},{10,11... | collective-permute-start | bytes 196616 | tf_op jit(solution)/shard_map/ppermute | solution.py:44
  63.8 1.3 %collective-permute-start.29 = (bf16[16,2048]{1,0:T(8,128)(2,1)S(1)}, bf16[16,2048]{1,0:T(8,128)(2,1)S(1)}, u32[]{:S(2)}, u32[]{:S(2)}) collective-permute-start(bf16[16,2048]{1,0:T(8,128)(2,1)S(1)} %collective-permute-done.28.refs_14_), channel_id=1, source_target_pairs={{0,1},{1,0},{2,3},{3,2},{4,5},{5,4},{6,7},{7,6},{8,9},{9,8},{10,11... | collective-permute-start | bytes 196616 | tf_op jit(solution)/shard_map/ppermute | solution.py:44
  65.1 18.0 %copy-start.14 = (f32[16,2]{0,1:T(2,128)S(1)}, f32[16,2]{0,1:T(2,128)}, u32[]{:S(2)}) copy-start(f32[16,2]{0,1:T(2,128)} %param.34) | copy-start | bytes 388
  65.1 18.0 %copy-start.15 = (s32[16,2]{0,1:T(2,128)S(1)}, s32[16,2]{0,1:T(2,128)}, u32[]{:S(2)}) copy-start(s32[16,2]{0,1:T(2,128)} %param.33) | copy-start | bytes 388
  70.5 1.4 %collective-permute-start.39 = (bf16[2,16,2048]{2,1,0:T(8,128)(2,1)S(1)}, bf16[2,16,2048]{2,1,0:T(8,128)(2,1)S(1)}, u32[]{:S(2)}, u32[]{:S(2)}) collective-permute-start(bf16[2,16,2048]{2,1,0:T(8,128)(2,1)S(1)} %get-tuple-element.22), channel_id=1, source_target_pairs={{0,1},{1,0},{2,3},{3,2},{4,5},{5,4},{6,7},{7,6},{8,9},{9,8},{10,11... | collective-permute-start | bytes 393224 | tf_op jit(solution)/shard_map/ppermute | solution.py:44
  70.7 2.6 %collective-permute-start.30 = (bf16[2,16,2048]{2,1,0:T(8,128)(2,1)S(1)}, bf16[2,16,2048]{2,1,0:T(8,128)(2,1)S(1)}, u32[]{:S(2)}, u32[]{:S(2)}) collective-permute-start(bf16[2,16,2048]{2,1,0:T(8,128)(2,1)S(1)} %get-tuple-element.16), channel_id=1, source_target_pairs={{0,1},{1,0},{2,3},{3,2},{4,5},{5,4},{6,7},{7,6},{8,9},{9,8},{10,11... | collective-permute-start | bytes 393224 | tf_op jit(solution)/shard_map/ppermute | solution.py:44
  71.0 3.1 %collective-permute-start.33 = (bf16[2,16,2048]{2,1,0:T(8,128)(2,1)S(1)}, bf16[2,16,2048]{2,1,0:T(8,128)(2,1)S(1)}, u32[]{:S(2)}, u32[]{:S(2)}) collective-permute-start(bf16[2,16,2048]{2,1,0:T(8,128)(2,1)S(1)} %get-tuple-element.18), channel_id=1, source_target_pairs={{0,1},{1,0},{2,3},{3,2},{4,5},{5,4},{6,7},{7,6},{8,9},{9,8},{10,11... | collective-permute-start | bytes 393224 | tf_op jit(solution)/shard_map/ppermute | solution.py:44
  71.2 4.4 %collective-permute-start.36 = (bf16[2,16,2048]{2,1,0:T(8,128)(2,1)S(1)}, bf16[2,16,2048]{2,1,0:T(8,128)(2,1)S(1)}, u32[]{:S(2)}, u32[]{:S(2)}) collective-permute-start(bf16[2,16,2048]{2,1,0:T(8,128)(2,1)S(1)} %get-tuple-element.20), channel_id=1, source_target_pairs={{0,1},{1,0},{2,3},{3,2},{4,5},{5,4},{6,7},{7,6},{8,9},{9,8},{10,11... | collective-permute-start | bytes 393224 | tf_op jit(solution)/shard_map/ppermute | solution.py:44
  71.9 11.2 %collective-permute-start.40 = (bf16[16,2048]{1,0:T(8,128)(2,1)S(1)}, bf16[16,2048]{1,0:T(8,128)(2,1)S(1)}, u32[]{:S(2)}, u32[]{:S(2)}) collective-permute-start(bf16[16,2048]{1,0:T(8,128)(2,1)S(1)} %slice_bitcast_fusion), channel_id=1, source_target_pairs={{0,2},{1,3},{2,0},{3,1},{4,6},{5,7},{6,4},{7,5},{8,10},{9,11},{10,... | collective-permute-start | bytes 196616 | tf_op jit(solution)/shard_map/ppermute | solution.py:44
  73.3 5.0 %collective-permute-start.31 = (bf16[16,2048]{1,0:T(8,128)(2,1)S(1)}, bf16[16,2048]{1,0:T(8,128)(2,1)S(1)}, u32[]{:S(2)}, u32[]{:S(2)}) collective-permute-start(bf16[16,2048]{1,0:T(8,128)(2,1)S(1)} %slice_bitcast_fusion.6), channel_id=1, source_target_pairs={{0,2},{1,3},{2,0},{3,1},{4,6},{5,7},{6,4},{7,5},{8,10},{9,11},{10,... | collective-permute-start | bytes 196616 | tf_op jit(solution)/shard_map/ppermute | solution.py:44
  74.2 6.0 %collective-permute-start.34 = (bf16[16,2048]{1,0:T(8,128)(2,1)S(1)}, bf16[16,2048]{1,0:T(8,128)(2,1)S(1)}, u32[]{:S(2)}, u32[]{:S(2)}) collective-permute-start(bf16[16,2048]{1,0:T(8,128)(2,1)S(1)} %slice_bitcast_fusion.4), channel_id=1, source_target_pairs={{0,2},{1,3},{2,0},{3,1},{4,6},{5,7},{6,4},{7,5},{8,10},{9,11},{10,... | collective-permute-start | bytes 196616 | tf_op jit(solution)/shard_map/ppermute | solution.py:44
  75.6 5.1 %collective-permute-start.37 = (bf16[16,2048]{1,0:T(8,128)(2,1)S(1)}, bf16[16,2048]{1,0:T(8,128)(2,1)S(1)}, u32[]{:S(2)}, u32[]{:S(2)}) collective-permute-start(bf16[16,2048]{1,0:T(8,128)(2,1)S(1)} %slice_bitcast_fusion.2), channel_id=1, source_target_pairs={{0,2},{1,3},{2,0},{3,1},{4,6},{5,7},{6,4},{7,5},{8,10},{9,11},{10,... | collective-permute-start | bytes 196616 | tf_op jit(solution)/shard_map/ppermute | solution.py:44
  78.4 6.4 %collective-permute-start.32 = (bf16[16,2048]{1,0:T(8,128)(2,1)S(1)}, bf16[16,2048]{1,0:T(8,128)(2,1)S(1)}, u32[]{:S(2)}, u32[]{:S(2)}) collective-permute-start(bf16[16,2048]{1,0:T(8,128)(2,1)S(1)} %fusion.10), channel_id=1, source_target_pairs={{0,12},{1,13},{2,14},{3,15},{4,8},{5,9},{6,10},{7,11},{8,4},{9,5},... | collective-permute-start | bytes 196616 | tf_op jit(solution)/shard_map/ppermute | solution.py:44
  80.2 6.0 %collective-permute-start.35 = (bf16[16,2048]{1,0:T(8,128)(2,1)S(1)}, bf16[16,2048]{1,0:T(8,128)(2,1)S(1)}, u32[]{:S(2)}, u32[]{:S(2)}) collective-permute-start(bf16[16,2048]{1,0:T(8,128)(2,1)S(1)} %fusion.9), channel_id=1, source_target_pairs={{0,8},{1,9},{2,10},{3,11},{4,12},{5,13},{6,14},{7,15},{8,0},{9,1},... | collective-permute-start | bytes 196616 | tf_op jit(solution)/shard_map/ppermute | solution.py:44
  80.7 5.4 %collective-permute-start.38 = (bf16[16,2048]{1,0:T(8,128)(2,1)S(1)}, bf16[16,2048]{1,0:T(8,128)(2,1)S(1)}, u32[]{:S(2)}, u32[]{:S(2)}) collective-permute-start(bf16[16,2048]{1,0:T(8,128)(2,1)S(1)} %fusion.8), channel_id=1, source_target_pairs={{0,4},{1,5},{2,6},{3,7},{4,0},{5,1},{6,2},{7,3},{8,12},{9,13},{10,... | collective-permute-start | bytes 196616 | tf_op jit(solution)/shard_map/ppermute | solution.py:44

commit v3 on v2

--- a/solution.py
+++ b/solution.py
@@ -37,6 +37,10 @@
 def removal_of(normed, w_remove_down, w_remove_up):
     remove_low = jnp.dot(normed, w_remove_down, preferred_element_type=f32).astype(bf16)
     return jax.nn.sigmoid(jnp.dot(remove_low, w_remove_up, preferred_element_type=f32))
+
+
+def in_hbm(array):
+    return pltpu.with_memory_space_constraint(array, pltpu.HBM)
 
 
 def swap(piece, bits):
@@ -102,7 +106,7 @@
         out_specs=VM,
         compiler_params=pltpu.CompilerParams(vmem_limit_bytes=16 * 2**20),
         name="project",
-    )(lax.axis_index("ep").astype(jnp.int32).reshape(1), *pieces, *[w.T for w in weights], gain.reshape(1, -1))
+    )(lax.axis_index("ep").astype(jnp.int32).reshape(1), in_hbm(pieces[0]), *pieces[1:], *[in_hbm(w.T) for w in weights], in_hbm(gain.reshape(1, -1)))
 
 
 def mixer_kernel(
@@ -232,8 +236,8 @@
         compiler_params=pltpu.CompilerParams(vmem_limit_bytes=32 * 2**20),
         name="mixer",
     )(
-        state_in, joined, decay, removal, group_gain.reshape(1, -1), hidden_in,
-        ffn_gain.reshape(1, -1), w_out,
+        in_hbm(state_in), joined, decay, removal, group_gain.reshape(1, -1), hidden_in,
+        ffn_gain.reshape(1, -1), in_hbm(w_out),
     )
 
 

time: 87.5 us -> 82.6 us (0.944)
  local copies, waits for them, and re-layouts: 8.82 us -> 0.08 us
  Pallas kernels: 15.7 us -> 19.8 us
    unnamed x32 -> x18, local copies, waits for them, and re-layouts: 8.8 us -> 0.06 us
    pallas_call x1, Pallas kernels: 6.87 us -> 9.87 us  [mixer(): pl.pallas_call(functools.partial(mixer_kernel, head=head), grid=(seqs //...]
    pallas_call x1, Pallas kernels: 1.93 us -> 3.05 us  [project(): pl.pallas_call(project_kernel, out_shape=jax.ShapeDtypeStruct((count, row...]
  transfers between devices with their start and end apart: 42 -> 42, of which waited for: 15 -> 15; matrix products, arithmetic and copies ran while one was open for 3% -> 4% of each run, Pallas kernels for 2% -> 2%
where the time goes in v3:
time: 82.6 us; the launch traced here: 82.3 us
  starting transfers between devices  38.4 us (46%)
  Pallas kernels  19.8 us (24%)
  waiting for transfers between devices  19.3 us (23%)
  matrix products  2.78 us (3%)
  other arithmetic  0.96 us (1%)
  between operations  0.91 us (1%)
    ppermute x41, starting transfers between devices, swap(): return lax.ppermute(piece, 'ep', [(i, i ^ bits) for i in range(size)])  32.8 us
    ppermute x41, waiting for transfers between devices, swap(): return lax.ppermute(piece, 'ep', [(i, i ^ bits) for i in range(size)])  12.9 us
    pallas_call x1, Pallas kernels, mixer(): pl.pallas_call(functools.partial(mixer_kernel, head=head), grid=(seqs //...  9.87 us
    all_to_all x1, waiting for transfers between devices, shards(): lax.all_to_all(spread, 'ep', split_axis=0, concat_axis=0, tiled=True)  6.43 us
    all_to_all x1, starting transfers between devices, shards(): lax.all_to_all(spread, 'ep', split_axis=0, concat_axis=0, tiled=True)  5.59 us
    pallas_call x1, Pallas kernels, run_experts(): pl.pallas_call(functools.partial(expert_kernel, count=count), out_shape=[...  5.34 us
    pallas_call x1, Pallas kernels, project(): pl.pallas_call(project_kernel, out_shape=jax.ShapeDtypeStruct((count, row...  3.05 us
  transfers between devices with their start and end apart: 42, of which 15 were waited for; matrix products, arithmetic and copies ran while one was open for 4% of the time, Pallas kernels for 2%

profile of v3, /device:TPU:0, one launch (start us, length us, event | category | flops | bytes accessed | tf_op | source)
XLA Modules:
  0.0 82.3 jit_solution(8619538443088738561)
XLA Ops:
  0.6 0.0 copy-start
  0.6 0.0 copy-start.4
  0.7 4.1 %collective-permute-start.7 = (bf16[16,2048]{1,0:T(8,128)(2,1)}, bf16[16,2048]{1,0:T(8,128)(2,1)S(1)}, u32[]{:S(2)}, u32[]{:S(2)}) collective-permute-start(bf16[16,2048]{1,0:T(8,128)(2,1)} %hidden_ref.1), channel_id=1, source_target_pairs={{0,8},{1,9},{2,10},{3,11},{4,12},{5,13},{6,14},{7,15},{8,0},{9,1},... | collective-permute-start | bytes 196616 | tf_op jit(solution)/shard_map/ppermute | solution.py:48
  4.8 1.3 %collective-permute-start.11 = (bf16[16,2048]{1,0:T(8,128)(2,1)}, bf16[16,2048]{1,0:T(8,128)(2,1)S(1)}, u32[]{:S(2)}, u32[]{:S(2)}) collective-permute-start(bf16[16,2048]{1,0:T(8,128)(2,1)} %hidden_ref.1), channel_id=1, source_target_pairs={{0,12},{1,13},{2,14},{3,15},{4,8},{5,9},{6,10},{7,11},{8,4},{9,5},... | collective-permute-start | bytes 196616 | tf_op jit(solution)/shard_map/ppermute | solution.py:48
  6.2 0.2 collective-permute-start.3
  6.4 1.5 %collective-permute-start.1 = (bf16[16,2048]{1,0:T(8,128)(2,1)}, bf16[16,2048]{1,0:T(8,128)(2,1)S(1)}, u32[]{:S(2)}, u32[]{:S(2)}) collective-permute-start(bf16[16,2048]{1,0:T(8,128)(2,1)} %hidden_ref.1), channel_id=1, source_target_pairs={{0,2},{1,3},{2,0},{3,1},{4,6},{5,7},{6,4},{7,5},{8,10},{9,11},{10,... | collective-permute-start | bytes 196616 | tf_op jit(solution)/shard_map/ppermute | solution.py:48
  7.9 0.8 collective-permute-done.7.refs_8_
  8.7 2.6 %collective-permute-start.9 = (bf16[16,2048]{1,0:T(8,128)(2,1)S(1)}, bf16[16,2048]{1,0:T(8,128)(2,1)S(1)}, u32[]{:S(2)}, u32[]{:S(2)}) collective-permute-start(bf16[16,2048]{1,0:T(8,128)(2,1)S(1)} %collective-permute-done.7.refs_8_), channel_id=1, source_target_pairs={{0,2},{1,3},{2,0},{3,1},{4,6},{5,7},{6,4},{7,5},{8,10},{9,11},{10,... | collective-permute-start | bytes 196616 | tf_op jit(solution)/shard_map/ppermute | solution.py:48
  11.4 1.3 %collective-permute-start.13 = (bf16[16,2048]{1,0:T(8,128)(2,1)S(1)}, bf16[16,2048]{1,0:T(8,128)(2,1)S(1)}, u32[]{:S(2)}, u32[]{:S(2)}) collective-permute-start(bf16[16,2048]{1,0:T(8,128)(2,1)S(1)} %collective-permute-done.11.refs_12_), channel_id=1, source_target_pairs={{0,2},{1,3},{2,0},{3,1},{4,6},{5,7},{6,4},{7,5},{8,10},{9,11},{10,... | collective-permute-start | bytes 196616 | tf_op jit(solution)/shard_map/ppermute | solution.py:48
  12.7 0.0 collective-permute-done.3.refs_4_
  12.7 0.7 collective-permute-start.5
  13.4 0.5 collective-permute-start.4
  13.9 1.6 %norm_rows.1 = bf16[16,2048]{1,0:T(8,128)(2,1)} custom-call(bf16[16,2048]{1,0:T(8,128)(2,1)} %hidden_ref.1, f32[1,2048]{1,0:T(1,128)} %bitcast.50), custom_call_target="tpu_custom_call" | custom-call | tf_op jit(solution)/shard_map/norm_rows/pallas_call | solution.py:68
  15.5 0.1 collective-permute-start.8
  15.6 0.1 collective-permute-done.13.refs_14_
  15.7 0.4 collective-permute-start.2
  16.0 0.9 %collective-permute-done.5.refs_6_ = bf16[16,2048]{1,0:T(8,128)(2,1)S(1)} collective-permute-done((bf16[16,2048]{1,0:T(8,128)(2,1)S(1)}, bf16[16,2048]{1,0:T(8,128)(2,1)S(1)}, u32[]{:S(2)}, u32[]{:S(2)}) %collective-permute-start.5) | collective-permute-done | bytes 65568 | tf_op jit(solution)/shard_map/ppermute | solution.py:48
  17.0 0.5 collective-permute-start.14
  17.5 0.1 collective-permute-start.6
  17.6 1.3 %fusion.15.decay_ref = f32[16,1024]{1,0:T(8,128)S(1)} fusion(bf16[128,1024]{1,0:T(8,128)(2,1)} %param.27, bf16[16,2048]{1,0:T(8,128)(2,1)} %norm_rows.1, bf16[2048,128]{1,0:T(8,128)(2,1)S(1)} %copy-done, f32[1024]{0:T(1024)} %param.25), kind=kOutput, calls=%fused_computation.29 | convolution fusion | flops 12769280 | bytes 921600 | tf_op jit(solution)/shard_map/dot_general | solution.py:33
  19.0 3.0 %project.1 = bf16[16,16,192]{2,1,0:T(8,128)(2,1)} custom-call(s32[1]{0:T(128)} %bitcast.place_ref, bf16[16,2048]{1,0:T(8,128)(2,1)} %hidden_ref.1, bf16[16,2048]{1,0:T(8,128)(2,1)S(1)} %collective-permute-done.refs_1_, bf16[16,2048]{1,0:T(8,128)(2,1)S(1)} %collective-permute-done.1.refs_2_, bf16[16,2048]{1,0:T(8,128)(2,1)S(1)} %collective-permute-done.2.refs_3_, ...), custom_call_target="tpu_custom_call" | custom-call | tf_op jit(solution)/shard_map/project/pallas_call | solution.py:102
  22.0 5.6 %all-to-all-start = ((bf16[16,16,192]{2,1,0:T(8,128)(2,1)}), bf16[16,16,192]{2,1,0:T(8,128)(2,1)S(1)}, u32[]{:S(2)}, u32[]{:S(2)}) async-start(bf16[16,16,192]{2,1,0:T(8,128)(2,1)} %project.1), calls=%async_computation | async-start | bytes 262144 | tf_op jit(solution)/shard_map/all_to_all | solution.py:324
  27.6 1.5 %fusion.2.removal_ref = f32[16,1024]{1,0:T(8,128)S(1)} fusion(bf16[128,1024]{1,0:T(8,128)(2,1)} %param.29, bf16[16,2048]{1,0:T(8,128)(2,1)} %norm_rows.1, bf16[2048,128]{1,0:T(8,128)(2,1)} %param.28), kind=kOutput, calls=%fused_computation.3 | convolution fusion | flops 12634112 | bytes 917504 | tf_op jit(solution)/shard_map/dot_general | solution.py:39
  29.1 6.4 %all-to-all-done.joined_ref = bf16[16,16,192]{2,1,0:T(8,128)(2,1)S(1)} async-done(((bf16[16,16,192]{2,1,0:T(8,128)(2,1)}), bf16[16,16,192]{2,1,0:T(8,128)(2,1)S(1)}, u32[]{:S(2)}, u32[]{:S(2)}) %all-to-all-start) | async-done | bytes 98336 | tf_op jit(solution)/shard_map/all_to_all | solution.py:324
  35.5 0.0 copy-start.1
  35.5 0.0 copy-start.2
  35.5 0.0 copy-start.3
  35.6 9.9 %mixer.1 = (f32[16,64,1024]{2,1,0:T(8,128)}, f32[16,2048]{1,0:T(8,128)S(1)}, bf16[16,2048]{1,0:T(8,128)(2,1)S(1)}) custom-call(f32[16,64,1024]{2,1,0:T(8,128)} %state_ref.1, bf16[16,16,192]{2,1,0:T(8,128)(2,1)S(1)} %all-to-all-done.joined_ref, f32[16,1024]{1,0:T(8,128)S(1)} %fusion.15.decay_ref, f32[16,1024]{1,0:T(8,128)S(1)} %fusion.2.removal_ref, ...), custom_call_target="tpu_custom_call" | custom-call | tf_op jit(solution)/shard_map/mixer/pallas_call | solution.py:211
  45.4 0.1 collective-permute-start.18
  45.5 1.2 %collective-permute-start.22 = (bf16[16,2048]{1,0:T(8,128)(2,1)S(1)}, bf16[16,2048]{1,0:T(8,128)(2,1)S(1)}, u32[]{:S(2)}, u32[]{:S(2)}) collective-permute-start(bf16[16,2048]{1,0:T(8,128)(2,1)S(1)} %get-tuple-element.14.refs_0_), channel_id=1, source_target_pairs={{0,8},{1,9},{2,10},{3,11},{4,12},{5,13},{6,14},{7,15},{8,0},{9,1},... | collective-permute-start | bytes 196616 | tf_op jit(solution)/shard_map/ppermute | solution.py:48
  46.7 3.1 %collective-permute-start.26 = (bf16[16,2048]{1,0:T(8,128)(2,1)S(1)}, bf16[16,2048]{1,0:T(8,128)(2,1)S(1)}, u32[]{:S(2)}, u32[]{:S(2)}) collective-permute-start(bf16[16,2048]{1,0:T(8,128)(2,1)S(1)} %get-tuple-element.14.refs_0_), channel_id=1, source_target_pairs={{0,12},{1,13},{2,14},{3,15},{4,8},{5,9},{6,10},{7,11},{8,4},{9,5},... | collective-permute-start | bytes 196616 | tf_op jit(solution)/shard_map/ppermute | solution.py:48
  49.9 0.3 collective-permute-done.18.refs_4_
  50.2 1.8 %collective-permute-start.20 = (bf16[16,2048]{1,0:T(8,128)(2,1)S(1)}, bf16[16,2048]{1,0:T(8,128)(2,1)S(1)}, u32[]{:S(2)}, u32[]{:S(2)}) collective-permute-start(bf16[16,2048]{1,0:T(8,128)(2,1)S(1)} %collective-permute-done.18.refs_4_), channel_id=1, source_target_pairs={{0,2},{1,3},{2,0},{3,1},{4,6},{5,7},{6,4},{7,5},{8,10},{9,11},{10,... | collective-permute-start | bytes 196616 | tf_op jit(solution)/shard_map/ppermute | solution.py:48
  51.9 1.8 %collective-permute-done.22.refs_8_ = bf16[16,2048]{1,0:T(8,128)(2,1)S(1)} collective-permute-done((bf16[16,2048]{1,0:T(8,128)(2,1)S(1)}, bf16[16,2048]{1,0:T(8,128)(2,1)S(1)}, u32[]{:S(2)}, u32[]{:S(2)}) %collective-permute-start.22) | collective-permute-done | bytes 65568 | tf_op jit(solution)/shard_map/ppermute | solution.py:48
  53.7 0.7 collective-permute-start.24
  54.4 1.3 %collective-permute-start.28 = (bf16[16,2048]{1,0:T(8,128)(2,1)S(1)}, bf16[16,2048]{1,0:T(8,128)(2,1)S(1)}, u32[]{:S(2)}, u32[]{:S(2)}) collective-permute-start(bf16[16,2048]{1,0:T(8,128)(2,1)S(1)} %collective-permute-done.26.refs_12_), channel_id=1, source_target_pairs={{0,2},{1,3},{2,0},{3,1},{4,6},{5,7},{6,4},{7,5},{8,10},{9,11},{10,... | collective-permute-start | bytes 196616 | tf_op jit(solution)/shard_map/ppermute | solution.py:48
  55.7 0.5 collective-permute-start.23
  56.2 0.1 collective-permute-start.27
  56.3 1.6 %collective-permute-done.24.refs_10_ = bf16[16,2048]{1,0:T(8,128)(2,1)S(1)} collective-permute-done((bf16[16,2048]{1,0:T(8,128)(2,1)S(1)}, bf16[16,2048]{1,0:T(8,128)(2,1)S(1)}, u32[]{:S(2)}, u32[]{:S(2)}) %collective-permute-start.24) | collective-permute-done | bytes 65568 | tf_op jit(solution)/shard_map/ppermute | solution.py:48
  58.0 0.7 collective-permute-done.28.refs_14_
  58.7 0.5 collective-permute-start.25
  59.2 0.1 collective-permute-start.29
  59.3 0.7 collective-permute-done.21.refs_7_
  59.9 0.2 collective-permute-done.25.refs_11_
  60.1 0.4 collective-permute-done.29.refs_15_
  60.5 0.0 copy-start.7
  60.5 0.0 copy-start.8
  60.5 5.3 %experts.1 = (bf16[2,16,2048]{2,1,0:T(8,128)(2,1)S(1)}, bf16[2,16,2048]{2,1,0:T(8,128)(2,1)S(1)}, bf16[2,16,2048]{2,1,0:T(8,128)(2,1)S(1)}, bf16[2,16,2048]{2,1,...) custom-call(bf16[16,2048]{1,0:T(8,128)(2,1)S(1)} %get-tuple-element., ...), custom_call_target="tpu_custom_call" | custom-call | tf_op jit(solution)/shard_map/experts/pallas_call | solution.py:282
  65.8 0.2 collective-permute-start.39
  66.0 0.4 collective-permute-start.30
  66.4 0.2 collective-permute-start.33
  66.6 0.4 collective-permute-start.36
  66.9 0.3 collective-permute-done.39
  67.3 1.4 %collective-permute-start.40 = (bf16[16,2048]{1,0:T(8,128)(2,1)S(1)}, bf16[16,2048]{1,0:T(8,128)(2,1)S(1)}, u32[]{:S(2)}, u32[]{:S(2)}) collective-permute-start(bf16[16,2048]{1,0:T(8,128)(2,1)S(1)} %slice_bitcast_fusion), channel_id=1, source_target_pairs={{0,2},{1,3},{2,0},{3,1},{4,6},{5,7},{6,4},{7,5},{8,10},{9,11},{10,... | collective-permute-start | bytes 196616 | tf_op jit(solution)/shard_map/ppermute | solution.py:48
  68.7 0.8 collective-permute-start.31
  69.6 1.4 %collective-permute-start.34 = (bf16[16,2048]{1,0:T(8,128)(2,1)S(1)}, bf16[16,2048]{1,0:T(8,128)(2,1)S(1)}, u32[]{:S(2)}, u32[]{:S(2)}) collective-permute-start(bf16[16,2048]{1,0:T(8,128)(2,1)S(1)} %slice_bitcast_fusion.4), channel_id=1, source_target_pairs={{0,2},{1,3},{2,0},{3,1},{4,6},{5,7},{6,4},{7,5},{8,10},{9,11},{10,... | collective-permute-start | bytes 196616 | tf_op jit(solution)/shard_map/ppermute | solution.py:48
  71.0 0.8 collective-permute-start.37
  71.8 2.0 %collective-permute-done.31 = bf16[16,2048]{1,0:T(8,128)(2,1)S(1)} collective-permute-done((bf16[16,2048]{1,0:T(8,128)(2,1)S(1)}, bf16[16,2048]{1,0:T(8,128)(2,1)S(1)}, u32[]{:S(2)}, u32[]{:S(2)}) %collective-permute-start.31) | collective-permute-done | bytes 65568 | tf_op jit(solution)/shard_map/ppermute | solution.py:48
  73.8 1.8 %collective-permute-start.32 = (bf16[16,2048]{1,0:T(8,128)(2,1)S(1)}, bf16[16,2048]{1,0:T(8,128)(2,1)S(1)}, u32[]{:S(2)}, u32[]{:S(2)}) collective-permute-start(bf16[16,2048]{1,0:T(8,128)(2,1)S(1)} %fusion.10), channel_id=1, source_target_pairs={{0,12},{1,13},{2,14},{3,15},{4,8},{5,9},{6,10},{7,11},{8,4},{9,5},... | collective-permute-start | bytes 196616 | tf_op jit(solution)/shard_map/ppermute | solution.py:48
  75.6 0.5 collective-permute-start.35
  76.1 2.3 %collective-permute-start.38 = (bf16[16,2048]{1,0:T(8,128)(2,1)S(1)}, bf16[16,2048]{1,0:T(8,128)(2,1)S(1)}, u32[]{:S(2)}, u32[]{:S(2)}) collective-permute-start(bf16[16,2048]{1,0:T(8,128)(2,1)S(1)} %fusion.8), channel_id=1, source_target_pairs={{0,4},{1,5},{2,6},{3,7},{4,0},{5,1},{6,2},{7,3},{8,12},{9,13},{10,... | collective-permute-start | bytes 196616 | tf_op jit(solution)/shard_map/ppermute | solution.py:48
  78.5 1.7 %collective-permute-done.32 = bf16[16,2048]{1,0:T(8,128)(2,1)S(1)} collective-permute-done((bf16[16,2048]{1,0:T(8,128)(2,1)S(1)}, bf16[16,2048]{1,0:T(8,128)(2,1)S(1)}, u32[]{:S(2)}, u32[]{:S(2)}) %collective-permute-start.32) | collective-permute-done | bytes 65568 | tf_op jit(solution)/shard_map/ppermute | solution.py:48
  80.2 1.4 %collective-permute-done.35 = bf16[16,2048]{1,0:T(8,128)(2,1)S(1)} collective-permute-done((bf16[16,2048]{1,0:T(8,128)(2,1)S(1)}, bf16[16,2048]{1,0:T(8,128)(2,1)S(1)}, u32[]{:S(2)}, u32[]{:S(2)}) %collective-permute-start.35) | collective-permute-done | bytes 65568 | tf_op jit(solution)/shard_map/ppermute | solution.py:48
  81.5 0.7 add_convert_fusion.4
  (57 shorter events, 0.4 us)
Async XLA Ops:
  0.6 16.9 %copy-start = (bf16[2048,128]{1,0:T(8,128)(2,1)S(1)}, bf16[2048,128]{1,0:T(8,128)(2,1)}, u32[]{:S(2)}) copy-start(bf16[2048,128]{1,0:T(8,128)(2,1)} %param.26) | copy-start | bytes 1572868
  0.6 34.9 %copy-start.4 = (bf16[16,2048]{1,0:T(8,128)(2,1)S(1)}, bf16[16,2048]{1,0:T(8,128)(2,1)}, u32[]{:S(2)}) copy-start(bf16[16,2048]{1,0:T(8,128)(2,1)} %hidden_ref.1) | copy-start | bytes 196612
  0.7 34.9 %copy-start.6 = (f32[1024]{0:T(1024)S(1)}, f32[1024]{0:T(1024)}, u32[]{:S(2)}) copy-start(f32[1024]{0:T(1024)} %param.30) | copy-start | bytes 12292
  0.7 34.9 %copy-start.5 = (f32[2048]{0:T(1024)S(1)}, f32[2048]{0:T(1024)}, u32[]{:S(2)}) copy-start(f32[2048]{0:T(1024)} %param.32) | copy-start | bytes 24580
  0.7 8.1 %collective-permute-start.7 = (bf16[16,2048]{1,0:T(8,128)(2,1)}, bf16[16,2048]{1,0:T(8,128)(2,1)S(1)}, u32[]{:S(2)}, u32[]{:S(2)}) collective-permute-start(bf16[16,2048]{1,0:T(8,128)(2,1)} %hidden_ref.1), channel_id=1, source_target_pairs={{0,8},{1,9},{2,10},{3,11},{4,12},{5,13},{6,14},{7,15},{8,0},{9,1},... | collective-permute-start | bytes 196616 | tf_op jit(solution)/shard_map/ppermute | solution.py:48
  4.8 6.6 %collective-permute-start.11 = (bf16[16,2048]{1,0:T(8,128)(2,1)}, bf16[16,2048]{1,0:T(8,128)(2,1)S(1)}, u32[]{:S(2)}, u32[]{:S(2)}) collective-permute-start(bf16[16,2048]{1,0:T(8,128)(2,1)} %hidden_ref.1), channel_id=1, source_target_pairs={{0,12},{1,13},{2,14},{3,15},{4,8},{5,9},{6,10},{7,11},{8,4},{9,5},... | collective-permute-start | bytes 196616 | tf_op jit(solution)/shard_map/ppermute | solution.py:48
  6.2 6.6 %collective-permute-start.3 = (bf16[16,2048]{1,0:T(8,128)(2,1)}, bf16[16,2048]{1,0:T(8,128)(2,1)S(1)}, u32[]{:S(2)}, u32[]{:S(2)}) collective-permute-start(bf16[16,2048]{1,0:T(8,128)(2,1)} %hidden_ref.1), channel_id=1, source_target_pairs={{0,4},{1,5},{2,6},{3,7},{4,0},{5,1},{6,2},{7,3},{8,12},{9,13},{10,... | collective-permute-start | bytes 196616 | tf_op jit(solution)/shard_map/ppermute | solution.py:48
  6.4 7.0 %collective-permute-start.1 = (bf16[16,2048]{1,0:T(8,128)(2,1)}, bf16[16,2048]{1,0:T(8,128)(2,1)S(1)}, u32[]{:S(2)}, u32[]{:S(2)}) collective-permute-start(bf16[16,2048]{1,0:T(8,128)(2,1)} %hidden_ref.1), channel_id=1, source_target_pairs={{0,2},{1,3},{2,0},{3,1},{4,6},{5,7},{6,4},{7,5},{8,10},{9,11},{10,... | collective-permute-start | bytes 196616 | tf_op jit(solution)/shard_map/ppermute | solution.py:48
  7.9 5.5 %collective-permute-start = (bf16[16,2048]{1,0:T(8,128)(2,1)}, bf16[16,2048]{1,0:T(8,128)(2,1)S(1)}, u32[]{:S(2)}, u32[]{:S(2)}) collective-permute-start(bf16[16,2048]{1,0:T(8,128)(2,1)} %hidden_ref.1), channel_id=1, source_target_pairs={{0,1},{1,0},{2,3},{3,2},{4,5},{5,4},{6,7},{7,6},{8,9},{9,8},{10,11... | collective-permute-start | bytes 196616 | tf_op jit(solution)/shard_map/ppermute | solution.py:48
  8.7 6.8 %collective-permute-start.9 = (bf16[16,2048]{1,0:T(8,128)(2,1)S(1)}, bf16[16,2048]{1,0:T(8,128)(2,1)S(1)}, u32[]{:S(2)}, u32[]{:S(2)}) collective-permute-start(bf16[16,2048]{1,0:T(8,128)(2,1)S(1)} %collective-permute-done.7.refs_8_), channel_id=1, source_target_pairs={{0,2},{1,3},{2,0},{3,1},{4,6},{5,7},{6,4},{7,5},{8,10},{9,11},{10,... | collective-permute-start | bytes 196616 | tf_op jit(solution)/shard_map/ppermute | solution.py:48
  11.4 4.3 %collective-permute-start.13 = (bf16[16,2048]{1,0:T(8,128)(2,1)S(1)}, bf16[16,2048]{1,0:T(8,128)(2,1)S(1)}, u32[]{:S(2)}, u32[]{:S(2)}) collective-permute-start(bf16[16,2048]{1,0:T(8,128)(2,1)S(1)} %collective-permute-done.11.refs_12_), channel_id=1, source_target_pairs={{0,2},{1,3},{2,0},{3,1},{4,6},{5,7},{6,4},{7,5},{8,10},{9,11},{10,... | collective-permute-start | bytes 196616 | tf_op jit(solution)/shard_map/ppermute | solution.py:48
  12.7 4.3 %collective-permute-start.5 = (bf16[16,2048]{1,0:T(8,128)(2,1)S(1)}, bf16[16,2048]{1,0:T(8,128)(2,1)S(1)}, u32[]{:S(2)}, u32[]{:S(2)}) collective-permute-start(bf16[16,2048]{1,0:T(8,128)(2,1)S(1)} %collective-permute-done.3.refs_4_), channel_id=1, source_target_pairs={{0,2},{1,3},{2,0},{3,1},{4,6},{5,7},{6,4},{7,5},{8,10},{9,11},{10,... | collective-permute-start | bytes 196616 | tf_op jit(solution)/shard_map/ppermute | solution.py:48
  13.4 3.6 %collective-permute-start.12 = (bf16[16,2048]{1,0:T(8,128)(2,1)S(1)}, bf16[16,2048]{1,0:T(8,128)(2,1)S(1)}, u32[]{:S(2)}, u32[]{:S(2)}) collective-permute-start(bf16[16,2048]{1,0:T(8,128)(2,1)S(1)} %collective-permute-done.11.refs_12_), channel_id=1, source_target_pairs={{0,1},{1,0},{2,3},{3,2},{4,5},{5,4},{6,7},{7,6},{8,9},{9,8},{10,11... | collective-permute-start | bytes 196616 | tf_op jit(solution)/shard_map/ppermute | solution.py:48
  13.4 4.1 %collective-permute-start.4 = (bf16[16,2048]{1,0:T(8,128)(2,1)S(1)}, bf16[16,2048]{1,0:T(8,128)(2,1)S(1)}, u32[]{:S(2)}, u32[]{:S(2)}) collective-permute-start(bf16[16,2048]{1,0:T(8,128)(2,1)S(1)} %collective-permute-done.3.refs_4_), channel_id=1, source_target_pairs={{0,1},{1,0},{2,3},{3,2},{4,5},{5,4},{6,7},{7,6},{8,9},{9,8},{10,11... | collective-permute-start | bytes 196616 | tf_op jit(solution)/shard_map/ppermute | solution.py:48
  15.5 3.4 %collective-permute-start.8 = (bf16[16,2048]{1,0:T(8,128)(2,1)S(1)}, bf16[16,2048]{1,0:T(8,128)(2,1)S(1)}, u32[]{:S(2)}, u32[]{:S(2)}) collective-permute-start(bf16[16,2048]{1,0:T(8,128)(2,1)S(1)} %collective-permute-done.7.refs_8_), channel_id=1, source_target_pairs={{0,1},{1,0},{2,3},{3,2},{4,5},{5,4},{6,7},{7,6},{8,9},{9,8},{10,11... | collective-permute-start | bytes 196616 | tf_op jit(solution)/shard_map/ppermute | solution.py:48
  15.7 3.3 %collective-permute-start.2 = (bf16[16,2048]{1,0:T(8,128)(2,1)S(1)}, bf16[16,2048]{1,0:T(8,128)(2,1)S(1)}, u32[]{:S(2)}, u32[]{:S(2)}) collective-permute-start(bf16[16,2048]{1,0:T(8,128)(2,1)S(1)} %collective-permute-done.1.refs_2_), channel_id=1, source_target_pairs={{0,1},{1,0},{2,3},{3,2},{4,5},{5,4},{6,7},{7,6},{8,9},{9,8},{10,11... | collective-permute-start | bytes 196616 | tf_op jit(solution)/shard_map/ppermute | solution.py:48
  17.0 2.0 %collective-permute-start.10 = (bf16[16,2048]{1,0:T(8,128)(2,1)S(1)}, bf16[16,2048]{1,0:T(8,128)(2,1)S(1)}, u32[]{:S(2)}, u32[]{:S(2)}) collective-permute-start(bf16[16,2048]{1,0:T(8,128)(2,1)S(1)} %collective-permute-done.9.refs_10_), channel_id=1, source_target_pairs={{0,1},{1,0},{2,3},{3,2},{4,5},{5,4},{6,7},{7,6},{8,9},{9,8},{10,11... | collective-permute-start | bytes 196616 | tf_op jit(solution)/shard_map/ppermute | solution.py:48
  17.0 2.0 %collective-permute-start.14 = (bf16[16,2048]{1,0:T(8,128)(2,1)S(1)}, bf16[16,2048]{1,0:T(8,128)(2,1)S(1)}, u32[]{:S(2)}, u32[]{:S(2)}) collective-permute-start(bf16[16,2048]{1,0:T(8,128)(2,1)S(1)} %collective-permute-done.13.refs_14_), channel_id=1, source_target_pairs={{0,1},{1,0},{2,3},{3,2},{4,5},{5,4},{6,7},{7,6},{8,9},{9,8},{10,11... | collective-permute-start | bytes 196616 | tf_op jit(solution)/shard_map/ppermute | solution.py:48
  17.5 1.5 %collective-permute-start.6 = (bf16[16,2048]{1,0:T(8,128)(2,1)S(1)}, bf16[16,2048]{1,0:T(8,128)(2,1)S(1)}, u32[]{:S(2)}, u32[]{:S(2)}) collective-permute-start(bf16[16,2048]{1,0:T(8,128)(2,1)S(1)} %collective-permute-done.5.refs_6_), channel_id=1, source_target_pairs={{0,1},{1,0},{2,3},{3,2},{4,5},{5,4},{6,7},{7,6},{8,9},{9,8},{10,11... | collective-permute-start | bytes 196616 | tf_op jit(solution)/shard_map/ppermute | solution.py:48
  22.0 13.5 %all-to-all-start = ((bf16[16,16,192]{2,1,0:T(8,128)(2,1)}), bf16[16,16,192]{2,1,0:T(8,128)(2,1)S(1)}, u32[]{:S(2)}, u32[]{:S(2)}) async-start(bf16[16,16,192]{2,1,0:T(8,128)(2,1)} %project.1), calls=%async_computation | async-start | bytes 262144 | tf_op jit(solution)/shard_map/all_to_all | solution.py:324
  35.5 24.9 %copy-start.1 = (bf16[2048,704]{0,1:T(8,128)(2,1)S(1)}, bf16[2048,704]{0,1:T(8,128)(2,1)}, u32[]{:S(2)}) copy-start(bf16[2048,704]{0,1:T(8,128)(2,1)} %param.35) | copy-start | bytes 8650756
  35.5 24.9 %copy-start.2 = (bf16[2048,704]{0,1:T(8,128)(2,1)S(1)}, bf16[2048,704]{0,1:T(8,128)(2,1)}, u32[]{:S(2)}) copy-start(bf16[2048,704]{0,1:T(8,128)(2,1)} %param.36) | copy-start | bytes 8650756
  35.5 24.9 %copy-start.3 = (bf16[704,2048]{1,0:T(8,128)(2,1)S(1)}, bf16[704,2048]{1,0:T(8,128)(2,1)}, u32[]{:S(2)}) copy-start(bf16[704,2048]{1,0:T(8,128)(2,1)} %refs_18_.1) | copy-start | bytes 8650756
  45.4 4.7 %collective-permute-start.18 = (bf16[16,2048]{1,0:T(8,128)(2,1)S(1)}, bf16[16,2048]{1,0:T(8,128)(2,1)S(1)}, u32[]{:S(2)}, u32[]{:S(2)}) collective-permute-start(bf16[16,2048]{1,0:T(8,128)(2,1)S(1)} %get-tuple-element.14.refs_0_), channel_id=1, source_target_pairs={{0,4},{1,5},{2,6},{3,7},{4,0},{5,1},{6,2},{7,3},{8,12},{9,13},{10,... | collective-permute-start | bytes 196616 | tf_op jit(solution)/shard_map/ppermute | solution.py:48
  45.5 8.2 %collective-permute-start.22 = (bf16[16,2048]{1,0:T(8,128)(2,1)S(1)}, bf16[16,2048]{1,0:T(8,128)(2,1)S(1)}, u32[]{:S(2)}, u32[]{:S(2)}) collective-permute-start(bf16[16,2048]{1,0:T(8,128)(2,1)S(1)} %get-tuple-element.14.refs_0_), channel_id=1, source_target_pairs={{0,8},{1,9},{2,10},{3,11},{4,12},{5,13},{6,14},{7,15},{8,0},{9,1},... | collective-permute-start | bytes 196616 | tf_op jit(solution)/shard_map/ppermute | solution.py:48
  46.7 7.7 %collective-permute-start.26 = (bf16[16,2048]{1,0:T(8,128)(2,1)S(1)}, bf16[16,2048]{1,0:T(8,128)(2,1)S(1)}, u32[]{:S(2)}, u32[]{:S(2)}) collective-permute-start(bf16[16,2048]{1,0:T(8,128)(2,1)S(1)} %get-tuple-element.14.refs_0_), channel_id=1, source_target_pairs={{0,12},{1,13},{2,14},{3,15},{4,8},{5,9},{6,10},{7,11},{8,4},{9,5},... | collective-permute-start | bytes 196616 | tf_op jit(solution)/shard_map/ppermute | solution.py:48
  49.9 5.8 %collective-permute-start.16 = (bf16[16,2048]{1,0:T(8,128)(2,1)S(1)}, bf16[16,2048]{1,0:T(8,128)(2,1)S(1)}, u32[]{:S(2)}, u32[]{:S(2)}) collective-permute-start(bf16[16,2048]{1,0:T(8,128)(2,1)S(1)} %get-tuple-element.14.refs_0_), channel_id=1, source_target_pairs={{0,2},{1,3},{2,0},{3,1},{4,6},{5,7},{6,4},{7,5},{8,10},{9,11},{10,... | collective-permute-start | bytes 196616 | tf_op jit(solution)/shard_map/ppermute | solution.py:48
  49.9 5.8 %collective-permute-start.15 = (bf16[16,2048]{1,0:T(8,128)(2,1)S(1)}, bf16[16,2048]{1,0:T(8,128)(2,1)S(1)}, u32[]{:S(2)}, u32[]{:S(2)}) collective-permute-start(bf16[16,2048]{1,0:T(8,128)(2,1)S(1)} %get-tuple-element.14.refs_0_), channel_id=1, source_target_pairs={{0,1},{1,0},{2,3},{3,2},{4,5},{5,4},{6,7},{7,6},{8,9},{9,8},{10,11... | collective-permute-start | bytes 196616 | tf_op jit(solution)/shard_map/ppermute | solution.py:48
  50.2 6.1 %collective-permute-start.20 = (bf16[16,2048]{1,0:T(8,128)(2,1)S(1)}, bf16[16,2048]{1,0:T(8,128)(2,1)S(1)}, u32[]{:S(2)}, u32[]{:S(2)}) collective-permute-start(bf16[16,2048]{1,0:T(8,128)(2,1)S(1)} %collective-permute-done.18.refs_4_), channel_id=1, source_target_pairs={{0,2},{1,3},{2,0},{3,1},{4,6},{5,7},{6,4},{7,5},{8,10},{9,11},{10,... | collective-permute-start | bytes 196616 | tf_op jit(solution)/shard_map/ppermute | solution.py:48
  53.7 4.3 %collective-permute-start.24 = (bf16[16,2048]{1,0:T(8,128)(2,1)S(1)}, bf16[16,2048]{1,0:T(8,128)(2,1)S(1)}, u32[]{:S(2)}, u32[]{:S(2)}) collective-permute-start(bf16[16,2048]{1,0:T(8,128)(2,1)S(1)} %collective-permute-done.22.refs_8_), channel_id=1, source_target_pairs={{0,2},{1,3},{2,0},{3,1},{4,6},{5,7},{6,4},{7,5},{8,10},{9,11},{10,... | collective-permute-start | bytes 196616 | tf_op jit(solution)/shard_map/ppermute | solution.py:48
  54.4 4.3 %collective-permute-start.28 = (bf16[16,2048]{1,0:T(8,128)(2,1)S(1)}, bf16[16,2048]{1,0:T(8,128)(2,1)S(1)}, u32[]{:S(2)}, u32[]{:S(2)}) collective-permute-start(bf16[16,2048]{1,0:T(8,128)(2,1)S(1)} %collective-permute-done.26.refs_12_), channel_id=1, source_target_pairs={{0,2},{1,3},{2,0},{3,1},{4,6},{5,7},{6,4},{7,5},{8,10},{9,11},{10,... | collective-permute-start | bytes 196616 | tf_op jit(solution)/shard_map/ppermute | solution.py:48
  55.7 3.0 %collective-permute-start.19 = (bf16[16,2048]{1,0:T(8,128)(2,1)S(1)}, bf16[16,2048]{1,0:T(8,128)(2,1)S(1)}, u32[]{:S(2)}, u32[]{:S(2)}) collective-permute-start(bf16[16,2048]{1,0:T(8,128)(2,1)S(1)} %collective-permute-done.18.refs_4_), channel_id=1, source_target_pairs={{0,1},{1,0},{2,3},{3,2},{4,5},{5,4},{6,7},{7,6},{8,9},{9,8},{10,11... | collective-permute-start | bytes 196616 | tf_op jit(solution)/shard_map/ppermute | solution.py:48
  55.7 3.5 %collective-permute-start.23 = (bf16[16,2048]{1,0:T(8,128)(2,1)S(1)}, bf16[16,2048]{1,0:T(8,128)(2,1)S(1)}, u32[]{:S(2)}, u32[]{:S(2)}) collective-permute-start(bf16[16,2048]{1,0:T(8,128)(2,1)S(1)} %collective-permute-done.22.refs_8_), channel_id=1, source_target_pairs={{0,1},{1,0},{2,3},{3,2},{4,5},{5,4},{6,7},{7,6},{8,9},{9,8},{10,11... | collective-permute-start | bytes 196616 | tf_op jit(solution)/shard_map/ppermute | solution.py:48
  56.2 3.0 %collective-permute-start.27 = (bf16[16,2048]{1,0:T(8,128)(2,1)S(1)}, bf16[16,2048]{1,0:T(8,128)(2,1)S(1)}, u32[]{:S(2)}, u32[]{:S(2)}) collective-permute-start(bf16[16,2048]{1,0:T(8,128)(2,1)S(1)} %collective-permute-done.26.refs_12_), channel_id=1, source_target_pairs={{0,1},{1,0},{2,3},{3,2},{4,5},{5,4},{6,7},{7,6},{8,9},{9,8},{10,11... | collective-permute-start | bytes 196616 | tf_op jit(solution)/shard_map/ppermute | solution.py:48
  58.0 1.3 %collective-permute-start.17 = (bf16[16,2048]{1,0:T(8,128)(2,1)S(1)}, bf16[16,2048]{1,0:T(8,128)(2,1)S(1)}, u32[]{:S(2)}, u32[]{:S(2)}) collective-permute-start(bf16[16,2048]{1,0:T(8,128)(2,1)S(1)} %collective-permute-done.16.refs_2_), channel_id=1, source_target_pairs={{0,1},{1,0},{2,3},{3,2},{4,5},{5,4},{6,7},{7,6},{8,9},{9,8},{10,11... | collective-permute-start | bytes 196616 | tf_op jit(solution)/shard_map/ppermute | solution.py:48
  58.7 1.3 %collective-permute-start.21 = (bf16[16,2048]{1,0:T(8,128)(2,1)S(1)}, bf16[16,2048]{1,0:T(8,128)(2,1)S(1)}, u32[]{:S(2)}, u32[]{:S(2)}) collective-permute-start(bf16[16,2048]{1,0:T(8,128)(2,1)S(1)} %collective-permute-done.20.refs_6_), channel_id=1, source_target_pairs={{0,1},{1,0},{2,3},{3,2},{4,5},{5,4},{6,7},{7,6},{8,9},{9,8},{10,11... | collective-permute-start | bytes 196616 | tf_op jit(solution)/shard_map/ppermute | solution.py:48
  58.7 1.4 %collective-permute-start.25 = (bf16[16,2048]{1,0:T(8,128)(2,1)S(1)}, bf16[16,2048]{1,0:T(8,128)(2,1)S(1)}, u32[]{:S(2)}, u32[]{:S(2)}) collective-permute-start(bf16[16,2048]{1,0:T(8,128)(2,1)S(1)} %collective-permute-done.24.refs_10_), channel_id=1, source_target_pairs={{0,1},{1,0},{2,3},{3,2},{4,5},{5,4},{6,7},{7,6},{8,9},{9,8},{10,11... | collective-permute-start | bytes 196616 | tf_op jit(solution)/shard_map/ppermute | solution.py:48
  59.2 1.3 %collective-permute-start.29 = (bf16[16,2048]{1,0:T(8,128)(2,1)S(1)}, bf16[16,2048]{1,0:T(8,128)(2,1)S(1)}, u32[]{:S(2)}, u32[]{:S(2)}) collective-permute-start(bf16[16,2048]{1,0:T(8,128)(2,1)S(1)} %collective-permute-done.28.refs_14_), channel_id=1, source_target_pairs={{0,1},{1,0},{2,3},{3,2},{4,5},{5,4},{6,7},{7,6},{8,9},{9,8},{10,11... | collective-permute-start | bytes 196616 | tf_op jit(solution)/shard_map/ppermute | solution.py:48
  60.5 18.0 %copy-start.7 = (f32[16,2]{0,1:T(2,128)S(1)}, f32[16,2]{0,1:T(2,128)}, u32[]{:S(2)}) copy-start(f32[16,2]{0,1:T(2,128)} %param.34) | copy-start | bytes 388
  60.5 18.0 %copy-start.8 = (s32[16,2]{0,1:T(2,128)S(1)}, s32[16,2]{0,1:T(2,128)}, u32[]{:S(2)}) copy-start(s32[16,2]{0,1:T(2,128)} %param.33) | copy-start | bytes 388
  65.8 1.4 %collective-permute-start.39 = (bf16[2,16,2048]{2,1,0:T(8,128)(2,1)S(1)}, bf16[2,16,2048]{2,1,0:T(8,128)(2,1)S(1)}, u32[]{:S(2)}, u32[]{:S(2)}) collective-permute-start(bf16[2,16,2048]{2,1,0:T(8,128)(2,1)S(1)} %get-tuple-element.22), channel_id=1, source_target_pairs={{0,1},{1,0},{2,3},{3,2},{4,5},{5,4},{6,7},{7,6},{8,9},{9,8},{10,11... | collective-permute-start | bytes 393224 | tf_op jit(solution)/shard_map/ppermute | solution.py:48
  66.0 2.6 %collective-permute-start.30 = (bf16[2,16,2048]{2,1,0:T(8,128)(2,1)S(1)}, bf16[2,16,2048]{2,1,0:T(8,128)(2,1)S(1)}, u32[]{:S(2)}, u32[]{:S(2)}) collective-permute-start(bf16[2,16,2048]{2,1,0:T(8,128)(2,1)S(1)} %get-tuple-element.16), channel_id=1, source_target_pairs={{0,1},{1,0},{2,3},{3,2},{4,5},{5,4},{6,7},{7,6},{8,9},{9,8},{10,11... | collective-permute-start | bytes 393224 | tf_op jit(solution)/shard_map/ppermute | solution.py:48
  66.4 3.1 %collective-permute-start.33 = (bf16[2,16,2048]{2,1,0:T(8,128)(2,1)S(1)}, bf16[2,16,2048]{2,1,0:T(8,128)(2,1)S(1)}, u32[]{:S(2)}, u32[]{:S(2)}) collective-permute-start(bf16[2,16,2048]{2,1,0:T(8,128)(2,1)S(1)} %get-tuple-element.18), channel_id=1, source_target_pairs={{0,1},{1,0},{2,3},{3,2},{4,5},{5,4},{6,7},{7,6},{8,9},{9,8},{10,11... | collective-permute-start | bytes 393224 | tf_op jit(solution)/shard_map/ppermute | solution.py:48
  66.6 4.4 %collective-permute-start.36 = (bf16[2,16,2048]{2,1,0:T(8,128)(2,1)S(1)}, bf16[2,16,2048]{2,1,0:T(8,128)(2,1)S(1)}, u32[]{:S(2)}, u32[]{:S(2)}) collective-permute-start(bf16[2,16,2048]{2,1,0:T(8,128)(2,1)S(1)} %get-tuple-element.20), channel_id=1, source_target_pairs={{0,1},{1,0},{2,3},{3,2},{4,5},{5,4},{6,7},{7,6},{8,9},{9,8},{10,11... | collective-permute-start | bytes 393224 | tf_op jit(solution)/shard_map/ppermute | solution.py:48
  67.3 11.2 %collective-permute-start.40 = (bf16[16,2048]{1,0:T(8,128)(2,1)S(1)}, bf16[16,2048]{1,0:T(8,128)(2,1)S(1)}, u32[]{:S(2)}, u32[]{:S(2)}) collective-permute-start(bf16[16,2048]{1,0:T(8,128)(2,1)S(1)} %slice_bitcast_fusion), channel_id=1, source_target_pairs={{0,2},{1,3},{2,0},{3,1},{4,6},{5,7},{6,4},{7,5},{8,10},{9,11},{10,... | collective-permute-start | bytes 196616 | tf_op jit(solution)/shard_map/ppermute | solution.py:48
  68.7 5.0 %collective-permute-start.31 = (bf16[16,2048]{1,0:T(8,128)(2,1)S(1)}, bf16[16,2048]{1,0:T(8,128)(2,1)S(1)}, u32[]{:S(2)}, u32[]{:S(2)}) collective-permute-start(bf16[16,2048]{1,0:T(8,128)(2,1)S(1)} %slice_bitcast_fusion.6), channel_id=1, source_target_pairs={{0,2},{1,3},{2,0},{3,1},{4,6},{5,7},{6,4},{7,5},{8,10},{9,11},{10,... | collective-permute-start | bytes 196616 | tf_op jit(solution)/shard_map/ppermute | solution.py:48
  69.6 6.0 %collective-permute-start.34 = (bf16[16,2048]{1,0:T(8,128)(2,1)S(1)}, bf16[16,2048]{1,0:T(8,128)(2,1)S(1)}, u32[]{:S(2)}, u32[]{:S(2)}) collective-permute-start(bf16[16,2048]{1,0:T(8,128)(2,1)S(1)} %slice_bitcast_fusion.4), channel_id=1, source_target_pairs={{0,2},{1,3},{2,0},{3,1},{4,6},{5,7},{6,4},{7,5},{8,10},{9,11},{10,... | collective-permute-start | bytes 196616 | tf_op jit(solution)/shard_map/ppermute | solution.py:48
  71.0 5.1 %collective-permute-start.37 = (bf16[16,2048]{1,0:T(8,128)(2,1)S(1)}, bf16[16,2048]{1,0:T(8,128)(2,1)S(1)}, u32[]{:S(2)}, u32[]{:S(2)}) collective-permute-start(bf16[16,2048]{1,0:T(8,128)(2,1)S(1)} %slice_bitcast_fusion.2), channel_id=1, source_target_pairs={{0,2},{1,3},{2,0},{3,1},{4,6},{5,7},{6,4},{7,5},{8,10},{9,11},{10,... | collective-permute-start | bytes 196616 | tf_op jit(solution)/shard_map/ppermute | solution.py:48
  73.8 6.4 %collective-permute-start.32 = (bf16[16,2048]{1,0:T(8,128)(2,1)S(1)}, bf16[16,2048]{1,0:T(8,128)(2,1)S(1)}, u32[]{:S(2)}, u32[]{:S(2)}) collective-permute-start(bf16[16,2048]{1,0:T(8,128)(2,1)S(1)} %fusion.10), channel_id=1, source_target_pairs={{0,12},{1,13},{2,14},{3,15},{4,8},{5,9},{6,10},{7,11},{8,4},{9,5},... | collective-permute-start | bytes 196616 | tf_op jit(solution)/shard_map/ppermute | solution.py:48
  75.6 5.9 %collective-permute-start.35 = (bf16[16,2048]{1,0:T(8,128)(2,1)S(1)}, bf16[16,2048]{1,0:T(8,128)(2,1)S(1)}, u32[]{:S(2)}, u32[]{:S(2)}) collective-permute-start(bf16[16,2048]{1,0:T(8,128)(2,1)S(1)} %fusion.9), channel_id=1, source_target_pairs={{0,8},{1,9},{2,10},{3,11},{4,12},{5,13},{6,14},{7,15},{8,0},{9,1},... | collective-permute-start | bytes 196616 | tf_op jit(solution)/shard_map/ppermute | solution.py:48
  76.1 5.4 %collective-permute-start.38 = (bf16[16,2048]{1,0:T(8,128)(2,1)S(1)}, bf16[16,2048]{1,0:T(8,128)(2,1)S(1)}, u32[]{:S(2)}, u32[]{:S(2)}) collective-permute-start(bf16[16,2048]{1,0:T(8,128)(2,1)S(1)} %fusion.8), channel_id=1, source_target_pairs={{0,4},{1,5},{2,6},{3,7},{4,0},{5,1},{6,2},{7,3},{8,12},{9,13},{10,... | collective-permute-start | bytes 196616 | tf_op jit(solution)/shard_map/ppermute | solution.py:48
